TPU v7x, 512 devices: a whole 4x8x8 slice. The times are simulated.
512 devices in a mesh: sp: 32 (over z, x), tp: 16 (over y, core).
Axes of the slice: x: 4, y: 8, z: 8, core: 2. Of those that a mesh axis runs over, the one named last changes fastest.
Arguments:
- readout_query_vectors: bfloat16 [8192, 2048], P('sp', 'tp'), may hold values from -6 to 6
- attention_key_vectors: bfloat16 [8192, 2048], P('sp', 'tp'), may hold values from -6 to 6
- attention_content_vectors: bfloat16 [8192, 2048], P('sp', 'tp'), may hold values from -6 to 6
- step_size_preactivation: bfloat16 [8192, 2048], P('sp', 'tp'), may hold values from -16 to 8
- forgetting_preactivation: float32 [8192, 2048], P('sp', 'tp'), may hold values from -22 to 3
- extra_forgetting_bias: float32 [8192, 32], P('sp', 'tp'), may hold values from -0.7 to 0
- subspace_normalizer_gain: float32 [2048], P('tp'), may hold values from 0.1 to 1.9
- skip_connection_stream: bfloat16 [8192, 2048], P('sp'), may hold values from -40 to 40
- blender_projection_matrix: bfloat16 [2048, 2048], P('tp'), may hold values from -0.125 to 0.125
- specialist_prenormal_gain: float32 [2048], replicated, may hold values from 0.1 to 1.9
- cluster_router_chance: float32 [8192], P('sp'), may hold values from 0.4 to 1
- specialist_chance_within_cluster: float32 [8192, 2], P('sp'), may hold values from 0.1 to 1
- chosen_specialist_ids: int32 [8192, 2], P('sp'), may hold values from 0 to 31, all different within a row; in each aligned block of 256 rows (0 to 255, 256 to 511, ...) at most 32 rows name the same one
- specialist_switch_matrix: bfloat16 [32, 2048, 2048], P('sp', None, 'tp'), may hold values from -0.125 to 0.125
- specialist_expansion_matrix: bfloat16 [32, 2048, 2048], P('sp', None, 'tp'), may hold values from -0.125 to 0.125
- specialist_contraction_matrix: bfloat16 [32, 2048, 2048], P('sp', 'tp'), may hold values from -0.375 to 0.375
Outputs:
- layer_out: bfloat16 [8192, 2048], P('sp')
Inputs may be any that keep to these rules, and one draw needn't show every extreme that they name: `chosen_specialist_ids`: in each aligned block of 256 rows every expert is named at most 32 times.
All inputs are finite; a program needn't handle non-finite values.
Results may differ from a plain program's by a relative error of at most 0.022.
Values may be sent and summed in bfloat16 or wider, within the bound.
No kernel may reach another device: no remote copies, remote signals or barrier semaphores. Data moves between devices by JAX's collectives and lax.ppermute only.
A program may use at most 64 MiB of HBM per device.

v0:
```python
import jax
import jax.numpy as jnp
from jax import lax
from jax.experimental import pallas as pl
from jax.experimental.pallas import tpu as pltpu
from jax.sharding import Mesh
from jax.sharding import PartitionSpec as P


SP = ("z", "x")
TP = ("y", "c")
F32 = jnp.float32
BF16 = jnp.bfloat16
SEG = 64
W = 128
DECAY = 0.6065306597126334
INTERPRET = False


def mm(a, b, contract=((1,), (0,)), precision=lax.Precision.HIGHEST):
    return lax.dot_general(
        a, b, (contract, ((), ())), precision=precision, preferred_element_type=F32
    )


def iota(shape, dim):
    return lax.broadcasted_iota(jnp.int32, shape, dim)


def stack_heads(rows):
    first = iota(rows.shape, 1) < SEG
    zero = jnp.zeros_like(rows)
    return jnp.concatenate([jnp.where(first, rows, zero), jnp.where(first, zero, rows)], axis=0)


def flat_heads(stacked):
    half = stacked.shape[0] // 2
    return stacked[:half] + stacked[half:]


def eye128():
    return (iota((W, W), 0) == iota((W, W), 1)).astype(F32)


def same_head_ones():
    return (iota((W, W), 0) // SEG == iota((W, W), 1) // SEG).astype(F32)


def mixer_kernel(q_ref, k_ref, v_ref, s_ref, f_ref, b_ref, pair_ref, map_ref, loc_ref):
    rows = q_ref.shape[0]
    chunks = rows // SEG
    query = q_ref[...].astype(F32)
    key = k_ref[...].astype(F32)
    value = v_ref[...].astype(F32)
    rate = 1.0 / (1.0 + jnp.exp(-s_ref[...].astype(F32)))
    bias = jnp.where(iota((rows, W), 1) < SEG, b_ref[:, 0:1], b_ref[:, 1:2])
    decay = bias - DECAY / (1.0 + jnp.exp(-f_ref[...]))
    removal = key * lax.rsqrt(mm(key * key, same_head_ones()) + 1e-06)
    beta = removal * rate
    row, col = iota((rows, rows), 0), iota((rows, rows), 1)
    below = ((row // SEG == col // SEG) & (row >= col)).astype(F32)
    total = mm(below, decay)

    row, col = iota((W, W), 0), iota((W, W), 1)
    same = row // SEG == col // SEG
    strict = same & (row > col)
    inclusive = same & (row >= col)
    eye = eye128()

    part = []
    for n in range(chunks):
        at = slice(n * SEG, (n + 1) * SEG)
        cum = total[at]
        before = cum - decay[at]
        middle = cum[SEG // 2 - 1 : SEG // 2]
        closing = cum[SEG - 1 : SEG]
        up = jnp.exp(cum - middle)
        down = jnp.exp(middle - cum)
        left = jnp.exp(before - middle)
        opening = jnp.exp(middle)
        ending = jnp.exp(closing - middle)
        alpha = -removal[at] * left
        asked = query[at] * up
        beta_hat = beta[at] * down
        key_hat = key[at] * down
        scores = mm(
            jnp.concatenate([stack_heads(alpha), stack_heads(asked)], axis=0),
            jnp.concatenate([stack_heads(beta_hat), stack_heads(key_hat)], axis=0),
            ((1,), (1,)),
        )
        remove_remove = jnp.where(strict, scores[:W, :W], 0.0)
        remove_write = jnp.where(strict, scores[:W, W:], 0.0)
        read_remove = jnp.where(inclusive, scores[W:, :W], 0.0)
        read_write = jnp.where(inclusive, scores[W:, W:], 0.0)
        part.append(
            dict(
                near=remove_remove,
                write=remove_write,
                read=jnp.concatenate([read_remove, read_write], axis=1),
                read_remove=read_remove,
                alpha=stack_heads(alpha * opening),
                asked=stack_heads(asked * opening),
                value=stack_heads(value[at]),
                bar=jnp.concatenate(
                    [stack_heads(beta_hat * ending), stack_heads(key_hat * ending)], axis=0
                ),
                closing=jnp.exp(closing),
            )
        )
    inverse = [eye + jnp.where(row // 2 == col // 2, p["near"], 0.0) for p in part]
    for level in (4, 8, 16, 32, 64):
        joint = (row // level == col // level) & (row // (level // 2) != col // (level // 2))
        step = [mm(jnp.where(joint, p["near"], 0.0), x) for p, x in zip(part, inverse)]
        inverse = [x + mm(x, s) for x, s in zip(inverse, step)]
    wrote = [mm(p["write"], p["value"]) for p in part]
    solved = [
        mm(x, jnp.concatenate([p["alpha"], w], axis=1)) for x, p, w in zip(inverse, part, wrote)
    ]
    keeps, adds, reads, locals_ = [], [], [], []
    for p, s in zip(part, solved):
        absorb, carried = s[:, :W], s[:, W:]
        keeps.append(mm(absorb, p["bar"][:W], ((0,), (0,))) + eye * p["closing"])
        adds.append(
            mm(jnp.concatenate([carried, p["value"]], axis=0), p["bar"], ((0,), (0,)))
        )
        locals_.append(
            flat_heads(mm(p["read"], jnp.concatenate([carried, p["value"]], axis=0)))
        )
        reads.append(flat_heads(p["asked"] + mm(p["read_remove"], absorb)))
    map_ref[:SEG, :] = reads[0]
    loc_ref[:SEG, :] = locals_[0]
    run = jnp.concatenate([keeps[0], adds[0]], axis=0)
    for n in range(1, chunks):
        at = slice(n * SEG, (n + 1) * SEG)
        both = mm(reads[n], run, ((1,), (1,)))
        map_ref[at, :] = both[:, :W]
        loc_ref[at, :] = locals_[n] + both[:, W:]
        run = mm(run, keeps[n])
        run = jnp.concatenate([run[:W], run[W:] + adds[n]], axis=0)
    pair = jnp.concatenate([flat_heads(run[:W] - eye), flat_heads(run[W:])], axis=0).astype(BF16)
    for n in range(pair_ref.shape[0]):
        pair_ref[n] = pair


def unpack(pair):
    pair = pair.astype(F32)
    return stack_heads(pair[:SEG]), stack_heads(pair[SEG:])


def compose_kernel(pos_ref, got_ref, pair_ref, prefix_ref):
    mine = pos_ref[0]
    eye = eye128()
    change, add = unpack(got_ref[0])
    run = jnp.concatenate([eye + change, add], axis=0)
    prefix = jnp.where(mine > 0, run, jnp.concatenate([eye, jnp.zeros((W, W), F32)], axis=0))
    for n in range(1, got_ref.shape[0]):
        change, add = unpack(got_ref[n])
        run = run + mm(run, change)
        run = jnp.concatenate([run[:W], run[W:] + add], axis=0)
        prefix = jnp.where(n < mine, run, prefix)
    pair = jnp.concatenate([flat_heads(run[:W] - eye), flat_heads(run[W:])], axis=0).astype(BF16)
    for n in range(pair_ref.shape[0]):
        pair_ref[n] = pair
    prefix_ref[...] = prefix


def readout_kernel(pos_ref, got_ref, prefix_ref, map_ref, loc_ref, gain_ref, w_ref, keep_ref, send_ref):
    mine, core = pos_ref[1], pos_ref[3]
    state = jnp.where(mine > 0, unpack(got_ref[0])[1], 0.0)
    for n in range(1, got_ref.shape[0] - 1):
        change, add = unpack(got_ref[n])
        state = jnp.where(n < mine, state + mm(state, change) + add, state)
    state = mm(state, prefix_ref[:W]) + prefix_ref[W:]
    out = loc_ref[...] + mm(map_ref[...], state, ((1,), (1,)))
    ones = same_head_ones()
    centered = out - mm(out, ones) * (1.0 / SEG)
    spread = mm(centered * centered, ones) * (1.0 / SEG)
    mixed = (centered * lax.rsqrt(spread + 0.00064) * gain_ref[...]).astype(BF16)
    for n in range(keep_ref.shape[0]):
        part = jnp.dot(mixed, w_ref[:, n * 2 * W : (n + 1) * 2 * W], preferred_element_type=F32)
        first, second = part[:, :W], part[:, W:]
        keep_ref[n] = jnp.where(core == 0, first, second)
        send_ref[n] = jnp.where(core == 0, second, first).astype(BF16)


def slots_of(ids_ref, experts, capacity):
    tokens = ids_ref.shape[0]
    names = [ids_ref[:, k : k + 1] for k in range(2)]
    hot = [(iota((tokens, experts), 1) == name).astype(F32) for name in names]
    earlier = (iota((tokens, tokens), 0) > iota((tokens, tokens), 1)).astype(BF16)
    ahead = jnp.dot(earlier, (hot[0] + hot[1]).astype(BF16), preferred_element_type=F32)
    ranks = [
        jnp.sum(hot[0] * ahead, axis=1, keepdims=True),
        jnp.sum(hot[1] * (ahead + hot[0]), axis=1, keepdims=True),
    ]
    return [name * capacity + rank.astype(jnp.int32) for name, rank in zip(names, ranks)]


def dispatch_kernel(parts_ref, skip_ref, gain_ref, ids_ref, hid_ref, out_ref):
    hidden = skip_ref[...].astype(F32)
    for n in range(parts_ref.shape[0]):
        hidden = hidden + parts_ref[n].astype(F32)
    hid_ref[...] = hidden
    scaled = (hidden * gain_ref[...]).astype(BF16)
    tokens, places = ids_ref.shape[0], out_ref.shape[0]
    first, second = slots_of(ids_ref, 32, 32)
    lane = iota((tokens, places), 1)
    hot = ((lane == first) | (lane == second)).astype(F32).astype(BF16)
    out_ref[...] = lax.dot_general(
        hot, scaled, (((0,), (0,)), ((), ())), preferred_element_type=F32
    ).astype(BF16)


def expert_kernel(pos_ref, own_ref, other_ref, inv_gain_ref, w0, w1, w2, w3, keep_ref, send_ref):
    core = pos_ref[3]
    ways, rows = own_ref.shape[0], own_ref.shape[1]
    blocks = []
    for n in range(ways):
        own, other = own_ref[n], other_ref[n]
        blocks.append(jnp.where(core == 0, own, other))
        blocks.append(jnp.where(core == 0, other, own))
    data = jnp.concatenate(blocks, axis=1)
    width = data.shape[1]
    squares = jnp.zeros((rows, W), F32)
    for n, block in enumerate(blocks):
        plain = block.astype(F32) * inv_gain_ref[:, n * W : (n + 1) * W]
        squares = squares + plain * plain
    scale = lax.rsqrt(jnp.sum(squares, axis=1, keepdims=True) * (1.0 / width) + 1e-06)
    hidden = []
    for w_ref in (w0, w1, w2, w3):
        both = jnp.concatenate([w_ref[:width], w_ref[width : 2 * width]], axis=1)
        act = jnp.dot(data, both, preferred_element_type=F32) * scale
        gate, up = act[:, :W], act[:, W:]
        hidden.append((gate / (1.0 + jnp.exp(-gate)) * up).astype(BF16))
    hidden = jnp.concatenate(hidden, axis=1)
    for n in range(ways):
        at = 2 * width + 2 * n * W
        pieces = [
            jnp.concatenate([w_ref[at : at + W], w_ref[at + W : at + 2 * W]], axis=1)
            for w_ref in (w0, w1, w2, w3)
        ]
        part = jnp.dot(hidden, jnp.concatenate(pieces, axis=0), preferred_element_type=F32)
        first, second = part[:, :W], part[:, W:]
        keep_ref[n] = jnp.where(core == 0, first, second)
        send_ref[n] = jnp.where(core == 0, second, first).astype(BF16)


def combine_kernel(ret_ref, hid_ref, ids_ref, chance_ref, within_ref, out_ref):
    tokens, places = ids_ref.shape[0], ret_ref.shape[0]
    slots = slots_of(ids_ref, 32, 32)
    lane = iota((tokens, places), 1)
    within = within_ref[...]
    whole = within[:, 0:1] + within[:, 1:2]
    result = hid_ref[...]
    for k in range(2):
        hot = (lane == slots[k]).astype(F32).astype(BF16)
        picked = jnp.dot(hot, ret_ref[...], preferred_element_type=F32)
        result = result + picked * (chance_ref[...] * within[:, k : k + 1] / whole)
    result = result.astype(BF16)
    for n in range(out_ref.shape[0]):
        out_ref[n] = result


def assemble_kernel(pos_ref, own_ref, other_ref, out_ref):
    core = pos_ref[3]
    for n in range(own_ref.shape[0]):
        own, other = own_ref[n], other_ref[n]
        out_ref[:, 2 * n * W : (2 * n + 1) * W] = jnp.where(core == 0, own, other)
        out_ref[:, (2 * n + 1) * W : (2 * n + 2) * W] = jnp.where(core == 0, other, own)


def call(kernel, outs, *args, scalars=0, flops=1_000_000):
    specs = [
        pl.BlockSpec(memory_space=pltpu.SMEM if n < scalars else pltpu.VMEM)
        for n in range(len(args))
    ]
    shapes = [jax.ShapeDtypeStruct(shape, kind) for shape, kind in outs]
    result = pl.pallas_call(
        kernel,
        out_shape=shapes if len(shapes) > 1 else shapes[0],
        in_specs=specs,
        out_specs=[pl.BlockSpec(memory_space=pltpu.VMEM)] * len(shapes)
        if len(shapes) > 1
        else pl.BlockSpec(memory_space=pltpu.VMEM),
        compiler_params=pltpu.CompilerParams(vmem_limit_bytes=40 * 1024 * 1024),
        cost_estimate=pl.CostEstimate(flops=flops, bytes_accessed=1_000_000, transcendentals=0),
        interpret=INTERPRET,
    )(*args)
    return result


def exchange(parts, axes):
    return lax.all_to_all(parts, axes, split_axis=0, concat_axis=0, tiled=True)


def swap_cores(data):
    return lax.ppermute(data, "c", [(0, 1), (1, 0)])


def body(
    queries,
    keys,
    values,
    step_sizes,
    forgetting,
    forgetting_bias,
    head_gain,
    skip,
    blender,
    norm_gain,
    cluster_chance,
    within_chance,
    ids,
    switch,
    expansion,
    contraction,
):
    n_z, n_x, n_y = (lax.axis_size(a) for a in ("z", "x", "y"))
    here = [lax.axis_index(a) for a in ("x", "z", "y", "c")]
    pos = jnp.stack(here).astype(jnp.int32)
    tokens, width = skip.shape
    column = (here[2] * 2 + here[3]) * W

    ring = [(((y + 1) % n_y) * 2, y * 2) for y in range(n_y)]
    ring += [(((y - 1) % n_y) * 2 + 1, y * 2 + 1) for y in range(n_y)]
    pairs, state_map, local = call(
        mixer_kernel,
        [((n_x, W, W), BF16), ((tokens, W), F32), ((tokens, W), F32)],
        queries,
        keys,
        values,
        step_sizes,
        forgetting,
        forgetting_bias,
    )
    pairs, switch, expansion, contraction = lax.optimization_barrier(
        (pairs, switch, expansion, contraction)
    )
    down = contraction[0].reshape(W, width // W, W).transpose(1, 0, 2).reshape(width, W)
    weights = [jnp.concatenate([switch[0], expansion[0], down], axis=0)]
    weights.append(lax.ppermute(weights[-1], TP, ring))
    gathered = exchange(pairs, "x")
    pairs, prefix = call(
        compose_kernel, [((n_z, W, W), BF16), ((2 * W, W), F32)], pos, gathered, scalars=1
    )
    weights.append(lax.ppermute(weights[-1], TP, ring))
    gathered = exchange(pairs, "z")
    keep, send = call(
        readout_kernel,
        [((n_y, tokens, W), F32), ((n_y, tokens, W), BF16)],
        pos,
        gathered,
        prefix,
        state_map,
        local,
        head_gain[None],
        blender,
        scalars=1,
    )
    parts = exchange((keep + swap_cores(send).astype(F32)).astype(BF16), "y")
    parts, weights[2] = lax.optimization_barrier((parts, weights[2]))
    weights.append(lax.ppermute(weights[-1], TP, ring))
    hidden, outgoing = call(
        dispatch_kernel,
        [((tokens, W), F32), ((4 * tokens, W), BF16)],
        parts,
        lax.dynamic_slice_in_dim(skip, column, W, 1),
        lax.dynamic_slice_in_dim(norm_gain, column, W, 0)[None],
        ids,
    )
    arrived = exchange(outgoing.reshape(n_z * n_x, -1, W), SP).reshape(4, tokens, W)
    own = exchange(jnp.concatenate([arrived, arrived], axis=0), "y")
    keep, send = call(
        expert_kernel,
        [((n_y, tokens, W), F32), ((n_y, tokens, W), BF16)],
        pos,
        own,
        swap_cores(own),
        (1.0 / norm_gain)[None],
        *weights,
        scalars=1,
    )
    summed = exchange((keep + swap_cores(send).astype(F32)).astype(BF16), "y")
    summed = (summed[:4].astype(F32) + summed[4:].astype(F32)).astype(BF16)
    returned = exchange(summed.reshape(n_z * n_x, -1, W), SP).reshape(4 * tokens, W)
    copies = call(
        combine_kernel,
        [((n_y, tokens, W), BF16)],
        returned,
        hidden,
        ids,
        cluster_chance[:, None],
        within_chance,
    )
    own = exchange(copies, "y")
    return call(assemble_kernel, [((tokens, width), BF16)], pos, own, swap_cores(own), scalars=1)


def solution(mesh):
    split = Mesh(mesh.devices.reshape(8, 4, 8, 2), ("z", "x", "y", "c"))
    in_specs = (
        P(SP, TP),
        P(SP, TP),
        P(SP, TP),
        P(SP, TP),
        P(SP, TP),
        P(SP, TP),
        P(TP),
        P(SP, None),
        P(TP, None),
        P(),
        P(SP),
        P(SP, None),
        P(SP, None),
        P(SP, None, TP),
        P(SP, None, TP),
        P(SP, TP, None),
    )
    out_specs = P(SP, None)

    return jax.shard_map(body, mesh=split, in_specs=in_specs, out_specs=out_specs, check_vma=False)
```

profile of v0, /device:TPU:1, one launch (start us, length us, event | category | flops | bytes accessed | tf_op | source)
XLA Modules:
  0.0 215.0 jit_solution(3169160985174233747)
XLA Ops:
  0.9 0.9 copy-done.3
  5.2 7.9 %shard_map.154 = (bf16[4,128,128]{2,1,0:T(8,128)(2,1)}, f32[256,128]{1,0:T(8,128)S(1)}, f32[256,128]{1,0:T(8,128)S(1)}) custom-call(bf16[256,128]{1,0:T(8,128)(2,1)S(1)} %copy-done.4, bf16[256,128]{1,0:T(8,128)(2,1)S(1)} %copy-done.5, bf16[256,128]{1,0:T(8,128)(2,1)S(1)} %copy-done.6, bf16[256,128]{1,0:T(8,128)(2,1)S(1)} %copy-done.7, ...), custom_call_target="tpu_custom_call" | custom-call | flops 1000000 | bytes 1000000 | tf_op jit(solution)/shard_map/pallas_call | solution.py:278
  13.0 1.1 copy.28
  14.5 4.2 %collective-permute-start.1 = (bf16[6144,128]{1,0:T(8,128)(2,1)S(1)}, bf16[6144,128]{1,0:T(8,128)(2,1)}, u32[]{:S(2)}, u32[]{:S(2)}) collective-permute-start(bf16[6144,128]{1,0:T(8,128)(2,1)S(1)} %pad_maximum_fusion.w0), channel_id=1, source_target_pairs={{2,0},{4,2},{6,4},{8,6},{10,8},{12,10},{14,12},{0,14},{15,1},{1,3}... | collective-permute-start | bytes 4718600 | tf_op jit(solution)/shard_map/ppermute | solution.py:341
  18.7 4.0 %all-to-all-start = ((bf16[4,128,128]{2,1,0:T(8,128)(2,1)}), bf16[4,128,128]{2,1,0:T(8,128)(2,1)S(1)}, u32[]{:S(2)}, u32[]{:S(2)}) async-start(bf16[4,128,128]{2,1,0:T(8,128)(2,1)} %get-tuple-element.23), calls=%async_computation | async-start | bytes 262144 | tf_op jit(solution)/shard_map/all_to_all | solution.py:293
  22.8 4.8 %all-to-all-done.got_ref = bf16[4,128,128]{2,1,0:T(8,128)(2,1)S(1)} async-done(((bf16[4,128,128]{2,1,0:T(8,128)(2,1)}), bf16[4,128,128]{2,1,0:T(8,128)(2,1)S(1)}, u32[]{:S(2)}, u32[]{:S(2)}) %all-to-all-start) | async-done | bytes 131104 | tf_op jit(solution)/shard_map/all_to_all | solution.py:293
  27.5 1.4 shard_map.155
  28.9 19.3 %all_to_all.40.got_ref = bf16[8,128,128]{2,1,0:T(8,128)(2,1)S(1)} all-to-all(bf16[8,128,128]{2,1,0:T(8,128)(2,1)S(1)} %get-tuple-element.24), channel_id=1, replica_groups=mesh['z'=8,'x'=4,'y'=8,'c'=2] {'z'}, dimensions={0} | all-to-all | bytes 524288 | tf_op jit(solution)/shard_map/all_to_all | solution.py:293
  48.2 3.4 %shard_map.156 = (f32[8,256,128]{2,1,0:T(8,128)S(1)}, bf16[8,256,128]{2,1,0:T(8,128)(2,1)S(1)}) custom-call(s32[4]{0:T(128)S(1)} %pad_add_fusion.pos_ref, bf16[8,128,128]{2,1,0:T(8,128)(2,1)S(1)} %all_to_all.40.got_ref, f32[256,128]{1,0:T(8,128)S(1)} %get-tuple-element.25.prefix_ref, f32[256,128]{1,0:T(8,128)S(1)} %get-tuple-element.26.map_ref, ...), custom_call_target="tpu_custom_call" | custom-call | flops 1000000 | bytes 1000000 | tf_op jit(solution)/shard_map/pallas_call | solution.py:278
  51.6 7.5 %collective-permute-start = (bf16[8,256,128]{2,1,0:T(8,128)(2,1)S(1)}, bf16[8,256,128]{2,1,0:T(8,128)(2,1)S(1)}, u32[]{:S(2)}, u32[]{:S(2)}) collective-permute-start(bf16[8,256,128]{2,1,0:T(8,128)(2,1)S(1)} %get-tuple-element.29), channel_id=1, source_target_pairs={{0,1},{1,0},{2,3},{3,2},{4,5},{5,4},{6,7},{7,6},{8,9},{9,8},{10,11... | collective-permute-start | bytes 1572872 | tf_op jit(solution)/shard_map/ppermute | solution.py:297
  59.1 1.9 collective-permute-start.2
  61.1 0.9 add_convert_fusion.1
  62.0 5.1 %all-to-all-start.2 = ((bf16[8,256,128]{2,1,0:T(8,128)(2,1)}), bf16[8,256,128]{2,1,0:T(8,128)(2,1)S(1)}, u32[]{:S(2)}, u32[]{:S(2)}) async-start(bf16[8,256,128]{2,1,0:T(8,128)(2,1)} %add_convert_fusion.1), calls=%async_computation.2 | async-start | bytes 1048576 | tf_op jit(solution)/shard_map/all_to_all | solution.py:293
  67.3 25.8 %all-to-all-done.2.parts_ref = bf16[8,256,128]{2,1,0:T(8,128)(2,1)S(1)} async-done(((bf16[8,256,128]{2,1,0:T(8,128)(2,1)}), bf16[8,256,128]{2,1,0:T(8,128)(2,1)S(1)}, u32[]{:S(2)}, u32[]{:S(2)}) %all-to-all-start.2) | async-done | bytes 524320 | tf_op jit(solution)/shard_map/all_to_all | solution.py:293
  93.1 0.9 shard_map.157
  94.7 3.9 %all-to-all-start.3 = ((bf16[32,32,128]{2,1,0:T(8,128)(2,1)}), bf16[32,32,128]{2,1,0:T(8,128)(2,1)S(1)}, u32[]{:S(2)}, u32[]{:S(2)}) async-start(bf16[32,32,128]{2,1,0:T(8,128)(2,1)} %bitcast.22), calls=%async_computation.3 | async-start | bytes 524288 | tf_op jit(solution)/shard_map/all_to_all | solution.py:293
  98.6 2.1 collective-permute-start.4
  100.7 9.0 %all-to-all-done.3 = bf16[32,32,128]{2,1,0:T(8,128)(2,1)S(1)} async-done(((bf16[32,32,128]{2,1,0:T(8,128)(2,1)}), bf16[32,32,128]{2,1,0:T(8,128)(2,1)S(1)}, u32[]{:S(2)}, u32[]{:S(2)}) %all-to-all-start.3) | async-done | bytes 262176 | tf_op jit(solution)/shard_map/all_to_all | solution.py:293
  109.7 23.3 %all_to_all.41.own_ref = bf16[8,256,128]{2,1,0:T(8,128)(2,1)S(1)} all-to-all(bf16[8,256,128]{2,1,0:T(8,128)(2,1)S(1)} %pad_maximum_fusion.1), channel_id=1, replica_groups=mesh['z'=8,'x'=4,'y'=8,'c'=2] {'y'}, dimensions={0} | all-to-all | bytes 1048576 | tf_op jit(solution)/shard_map/all_to_all | solution.py:293
  133.0 3.7 %collective-permute-start.3 = (bf16[8,256,128]{2,1,0:T(8,128)(2,1)S(1)}, bf16[8,256,128]{2,1,0:T(8,128)(2,1)S(1)}, u32[]{:S(2)}, u32[]{:S(2)}) collective-permute-start(bf16[8,256,128]{2,1,0:T(8,128)(2,1)S(1)} %all_to_all.41.own_ref), channel_id=1, source_target_pairs={{0,1},{1,0},{2,3},{3,2},{4,5},{5,4},{6,7},{7,6},{8,9},{9,8},{10,11... | collective-permute-start | bytes 1572872 | tf_op jit(solution)/shard_map/ppermute | solution.py:297
  136.8 1.5 collective-permute-done.3.other_ref
  138.3 4.2 %shard_map.158 = (f32[8,256,128]{2,1,0:T(8,128)S(1)}, bf16[8,256,128]{2,1,0:T(8,128)(2,1)S(1)}) custom-call(s32[4]{0:T(128)S(1)} %pad_add_fusion.pos_ref, bf16[8,256,128]{2,1,0:T(8,128)(2,1)S(1)} %all_to_all.41.own_ref, bf16[8,256,128]{2,1,0:T(8,128)(2,1)S(1)} %collective-permute-done.3.other_ref, f32[1,2048]{1,0:T(1,128)S(1)} %bitcast.23, ...), custom_call_target="tpu_custom_call" | custom-call | flops 1000000 | bytes 1000000 | tf_op jit(solution)/shard_map/pallas_call | solution.py:278
  142.5 2.3 %collective-permute-start.5 = (bf16[8,256,128]{2,1,0:T(8,128)(2,1)S(1)}, bf16[8,256,128]{2,1,0:T(8,128)(2,1)S(1)}, u32[]{:S(2)}, u32[]{:S(2)}) collective-permute-start(bf16[8,256,128]{2,1,0:T(8,128)(2,1)S(1)} %get-tuple-element.37), channel_id=1, source_target_pairs={{0,1},{1,0},{2,3},{3,2},{4,5},{5,4},{6,7},{7,6},{8,9},{9,8},{10,11... | collective-permute-start | bytes 1572872 | tf_op jit(solution)/shard_map/ppermute | solution.py:297
  144.8 1.5 collective-permute-done.5
  146.5 20.8 %all_to_all.42 = bf16[8,256,128]{2,1,0:T(8,128)(2,1)S(1)} all-to-all(bf16[8,256,128]{2,1,0:T(8,128)(2,1)S(1)} %add_convert_fusion), channel_id=1, replica_groups=mesh['z'=8,'x'=4,'y'=8,'c'=2] {'y'}, dimensions={0} | all-to-all | bytes 1048576 | tf_op jit(solution)/shard_map/all_to_all | solution.py:293
  168.1 9.5 %all-to-all-start.6 = ((bf16[32,32,128]{2,1,0:T(8,128)(2,1)}), bf16[32,32,128]{2,1,0:T(8,128)(2,1)S(1)}, u32[]{:S(2)}, u32[]{:S(2)}) async-start(bf16[32,32,128]{2,1,0:T(8,128)(2,1)} %bitcast.13), calls=%async_computation.6 | async-start | bytes 524288 | tf_op jit(solution)/shard_map/all_to_all | solution.py:293
  177.9 10.1 %all-to-all-done.6 = bf16[32,32,128]{2,1,0:T(8,128)(2,1)S(1)} async-done(((bf16[32,32,128]{2,1,0:T(8,128)(2,1)}), bf16[32,32,128]{2,1,0:T(8,128)(2,1)S(1)}, u32[]{:S(2)}, u32[]{:S(2)}) %all-to-all-start.6) | async-done | bytes 262176 | tf_op jit(solution)/shard_map/all_to_all | solution.py:293
  188.0 1.0 shard_map.159
  189.0 15.4 %all_to_all.43.own_ref = bf16[8,256,128]{2,1,0:T(8,128)(2,1)S(1)} all-to-all(bf16[8,256,128]{2,1,0:T(8,128)(2,1)S(1)} %shard_map.159), channel_id=1, replica_groups=mesh['z'=8,'x'=4,'y'=8,'c'=2] {'y'}, dimensions={0} | all-to-all | bytes 1048576 | tf_op jit(solution)/shard_map/all_to_all | solution.py:293
  204.4 7.3 %collective-permute-start.6 = (bf16[8,256,128]{2,1,0:T(8,128)(2,1)S(1)}, bf16[8,256,128]{2,1,0:T(8,128)(2,1)S(1)}, u32[]{:S(2)}, u32[]{:S(2)}) collective-permute-start(bf16[8,256,128]{2,1,0:T(8,128)(2,1)S(1)} %all_to_all.43.own_ref), channel_id=1, source_target_pairs={{0,1},{1,0},{2,3},{3,2},{4,5},{5,4},{6,7},{7,6},{8,9},{9,8},{10,11... | collective-permute-start | bytes 1572872 | tf_op jit(solution)/shard_map/ppermute | solution.py:297
  211.8 1.5 collective-permute-done.6.other_ref
  213.3 1.7 shard_map.160
  (46 shorter events, 6.8 us)
Async XLA Ops:
  0.0 67.3 %copy-start = (bf16[256,2048]{1,0:T(8,128)(2,1)S(1)}, bf16[256,2048]{1,0:T(8,128)(2,1)}, u32[]{:S(2)}) copy-start(bf16[256,2048]{1,0:T(8,128)(2,1)} %param.23) | copy-start | bytes 3145732
  0.9 0.9 copy-start.3
  1.8 0.8 copy-start.4
  2.7 0.8 copy-start.5
  3.5 0.8 copy-start.6
  4.3 0.8 copy-start.7
  5.2 9.2 %copy-start.9 = (bf16[1,2048,128]{2,1,0:T(8,128)(2,1)S(1)}, bf16[1,2048,128]{2,1,0:T(8,128)(2,1)}, u32[]{:S(2)}) copy-start(bf16[1,2048,128]{2,1,0:T(8,128)(2,1)} %param.30) | copy-start | bytes 1572868
  5.2 9.2 %copy-start.10 = (bf16[1,2048,128]{2,1,0:T(8,128)(2,1)S(1)}, bf16[1,2048,128]{2,1,0:T(8,128)(2,1)}, u32[]{:S(2)}) copy-start(bf16[1,2048,128]{2,1,0:T(8,128)(2,1)} %param.29) | copy-start | bytes 1572868
  14.4 33.8 %copy-start.1 = (bf16[128,2048]{1,0:T(8,128)(2,1)S(1)}, bf16[128,2048]{1,0:T(8,128)(2,1)}, u32[]{:S(2)}) copy-start(bf16[128,2048]{1,0:T(8,128)(2,1)} %w_ref.1) | copy-start | bytes 1572868
  14.4 33.8 %copy-start.8 = (f32[128]{0:T(128)S(1)}, f32[128]{0:T(128)}, u32[]{:S(2)}) copy-start(f32[128]{0:T(128)} %param.22) | copy-start | bytes 1540
  14.5 44.6 %collective-permute-start.1 = (bf16[6144,128]{1,0:T(8,128)(2,1)S(1)}, bf16[6144,128]{1,0:T(8,128)(2,1)}, u32[]{:S(2)}, u32[]{:S(2)}) collective-permute-start(bf16[6144,128]{1,0:T(8,128)(2,1)S(1)} %pad_maximum_fusion.w0), channel_id=1, source_target_pairs={{2,0},{4,2},{6,4},{8,6},{10,8},{12,10},{14,12},{0,14},{15,1},{1,3}... | collective-permute-start | bytes 4718600 | tf_op jit(solution)/shard_map/ppermute | solution.py:341
  18.7 8.9 %all-to-all-start = ((bf16[4,128,128]{2,1,0:T(8,128)(2,1)}), bf16[4,128,128]{2,1,0:T(8,128)(2,1)S(1)}, u32[]{:S(2)}, u32[]{:S(2)}) async-start(bf16[4,128,128]{2,1,0:T(8,128)(2,1)} %get-tuple-element.23), calls=%async_computation | async-start | bytes 262144 | tf_op jit(solution)/shard_map/all_to_all | solution.py:293
  51.6 9.5 %collective-permute-start = (bf16[8,256,128]{2,1,0:T(8,128)(2,1)S(1)}, bf16[8,256,128]{2,1,0:T(8,128)(2,1)S(1)}, u32[]{:S(2)}, u32[]{:S(2)}) collective-permute-start(bf16[8,256,128]{2,1,0:T(8,128)(2,1)S(1)} %get-tuple-element.29), channel_id=1, source_target_pairs={{0,1},{1,0},{2,3},{3,2},{4,5},{5,4},{6,7},{7,6},{8,9},{9,8},{10,11... | collective-permute-start | bytes 1572872 | tf_op jit(solution)/shard_map/ppermute | solution.py:297
  59.1 34.0 %collective-permute-start.2 = (bf16[6144,128]{1,0:T(8,128)(2,1)}, bf16[6144,128]{1,0:T(8,128)(2,1)}, u32[]{:S(2)}, u32[]{:S(2)}) collective-permute-start(bf16[6144,128]{1,0:T(8,128)(2,1)} %collective-permute-done.1.w1), channel_id=1, source_target_pairs={{2,0},{4,2},{6,4},{8,6},{10,8},{12,10},{14,12},{0,14},{15,1},{1,3}... | collective-permute-start | bytes 4718600 | tf_op jit(solution)/shard_map/ppermute | solution.py:346
  61.0 6.0 %copy-start.12 = (s32[256,2]{0,1:T(2,128)S(1)}, s32[256,2]{0,1:T(2,128)}, u32[]{:S(2)}) copy-start(s32[256,2]{0,1:T(2,128)} %param.28) | copy-start | bytes 6148
  61.0 6.2 %copy-start.11 = (f32[2048]{0:T(1024)S(1)}, f32[2048]{0:T(1024)}, u32[]{:S(2)}) copy-start(f32[2048]{0:T(1024)} %param.25) | copy-start | bytes 24580
  62.0 31.1 %all-to-all-start.2 = ((bf16[8,256,128]{2,1,0:T(8,128)(2,1)}), bf16[8,256,128]{2,1,0:T(8,128)(2,1)S(1)}, u32[]{:S(2)}, u32[]{:S(2)}) async-start(bf16[8,256,128]{2,1,0:T(8,128)(2,1)} %add_convert_fusion.1), calls=%async_computation.2 | async-start | bytes 1048576 | tf_op jit(solution)/shard_map/all_to_all | solution.py:293
  94.0 0.7 copy-start.2
  94.7 15.0 %all-to-all-start.3 = ((bf16[32,32,128]{2,1,0:T(8,128)(2,1)}), bf16[32,32,128]{2,1,0:T(8,128)(2,1)S(1)}, u32[]{:S(2)}, u32[]{:S(2)}) async-start(bf16[32,32,128]{2,1,0:T(8,128)(2,1)} %bitcast.22), calls=%async_computation.3 | async-start | bytes 524288 | tf_op jit(solution)/shard_map/all_to_all | solution.py:293
  98.6 38.2 %collective-permute-start.4 = (bf16[6144,128]{1,0:T(8,128)(2,1)}, bf16[6144,128]{1,0:T(8,128)(2,1)}, u32[]{:S(2)}, u32[]{:S(2)}) collective-permute-start(bf16[6144,128]{1,0:T(8,128)(2,1)} %collective-permute-done.2.w2), channel_id=1, source_target_pairs={{2,0},{4,2},{6,4},{8,6},{10,8},{12,10},{14,12},{0,14},{15,1},{1,3}... | collective-permute-start | bytes 4718600 | tf_op jit(solution)/shard_map/ppermute | solution.py:362
  133.0 5.2 %collective-permute-start.3 = (bf16[8,256,128]{2,1,0:T(8,128)(2,1)S(1)}, bf16[8,256,128]{2,1,0:T(8,128)(2,1)S(1)}, u32[]{:S(2)}, u32[]{:S(2)}) collective-permute-start(bf16[8,256,128]{2,1,0:T(8,128)(2,1)S(1)} %all_to_all.41.own_ref), channel_id=1, source_target_pairs={{0,1},{1,0},{2,3},{3,2},{4,5},{5,4},{6,7},{7,6},{8,9},{9,8},{10,11... | collective-permute-start | bytes 1572872 | tf_op jit(solution)/shard_map/ppermute | solution.py:297
  142.5 3.8 %collective-permute-start.5 = (bf16[8,256,128]{2,1,0:T(8,128)(2,1)S(1)}, bf16[8,256,128]{2,1,0:T(8,128)(2,1)S(1)}, u32[]{:S(2)}, u32[]{:S(2)}) collective-permute-start(bf16[8,256,128]{2,1,0:T(8,128)(2,1)S(1)} %get-tuple-element.37), channel_id=1, source_target_pairs={{0,1},{1,0},{2,3},{3,2},{4,5},{5,4},{6,7},{7,6},{8,9},{9,8},{10,11... | collective-permute-start | bytes 1572872 | tf_op jit(solution)/shard_map/ppermute | solution.py:297
  146.4 31.1 %copy-start.14 = (f32[256]{0:T(256)S(1)}, f32[256]{0:T(256)}, u32[]{:S(2)}) copy-start(f32[256]{0:T(256)} %param.26) | copy-start | bytes 3076
  146.4 31.3 %copy-start.13 = (f32[256,2]{0,1:T(2,128)S(1)}, f32[256,2]{0,1:T(2,128)}, u32[]{:S(2)}) copy-start(f32[256,2]{0,1:T(2,128)} %param.27) | copy-start | bytes 6148
  168.1 19.9 %all-to-all-start.6 = ((bf16[32,32,128]{2,1,0:T(8,128)(2,1)}), bf16[32,32,128]{2,1,0:T(8,128)(2,1)S(1)}, u32[]{:S(2)}, u32[]{:S(2)}) async-start(bf16[32,32,128]{2,1,0:T(8,128)(2,1)} %bitcast.13), calls=%async_computation.6 | async-start | bytes 524288 | tf_op jit(solution)/shard_map/all_to_all | solution.py:293
  204.4 8.8 %collective-permute-start.6 = (bf16[8,256,128]{2,1,0:T(8,128)(2,1)S(1)}, bf16[8,256,128]{2,1,0:T(8,128)(2,1)S(1)}, u32[]{:S(2)}, u32[]{:S(2)}) collective-permute-start(bf16[8,256,128]{2,1,0:T(8,128)(2,1)S(1)} %all_to_all.43.own_ref), channel_id=1, source_target_pairs={{0,1},{1,0},{2,3},{3,2},{4,5},{5,4},{6,7},{7,6},{8,9},{9,8},{10,11... | collective-permute-start | bytes 1572872 | tf_op jit(solution)/shard_map/ppermute | solution.py:297
where the time goes:
time: 216 us; the launch traced here: 215 us
  blocking collectives  78.9 us (37%)
  waiting for transfers between devices  54.1 us (25%)
  starting transfers between devices  51.5 us (24%)
  Pallas kernels  20.5 us (9%)
  local copies, waits for them, and re-layouts  7.68 us (4%)
    all_to_all x4, blocking collectives, exchange(): return lax.all_to_all(parts, axes, split_axis=0, concat_axis=0, tiled=True)  78.9 us
    all_to_all x4, waiting for transfers between devices, exchange(): return lax.all_to_all(parts, axes, split_axis=0, concat_axis=0, tiled=True)  49.6 us
    all_to_all x4, starting transfers between devices, exchange(): return lax.all_to_all(parts, axes, split_axis=0, concat_axis=0, tiled=True)  22.5 us
    ppermute x4, starting transfers between devices, swap_cores(): return lax.ppermute(data, 'c', [(0, 1), (1, 0)])  20.8 us
    pallas_call x7, Pallas kernels, call(): pl.pallas_call(kernel, out_shape=shapes if len(shapes) > 1 else shapes[0]...  20.5 us
    ppermute x3, starting transfers between devices, body(): weights.append(lax.ppermute(weights[-1], TP, ring))  8.18 us
    unnamed x34, local copies, waits for them, and re-layouts  7.31 us
    ppermute x4, waiting for transfers between devices, swap_cores(): return lax.ppermute(data, 'c', [(0, 1), (1, 0)])  4.52 us
  transfers between devices with their start and end apart: 11, of which 7 were waited for; matrix products, arithmetic and copies ran while one was open for 1% of the time, Pallas kernels for 2%

commit v1 on v0

--- a/solution.py
+++ b/solution.py
@@ -46,14 +46,50 @@
     return (iota((W, W), 0) // SEG == iota((W, W), 1) // SEG).astype(F32)
 
 
-def mixer_kernel(q_ref, k_ref, v_ref, s_ref, f_ref, b_ref, pair_ref, map_ref, loc_ref):
+def pack_kernel(switch_ref, expansion_ref, contraction_ref, out_ref, sems):
+    depth = switch_ref.shape[1]
+    copies = [
+        pltpu.make_async_copy(switch_ref.at[0], out_ref.at[pl.ds(0, depth)], sems.at[0]),
+        pltpu.make_async_copy(expansion_ref.at[0], out_ref.at[pl.ds(depth, depth)], sems.at[1]),
+    ]
+    for n in range(depth // W):
+        copies.append(
+            pltpu.make_async_copy(
+                contraction_ref.at[0, :, pl.ds(n * W, W)],
+                out_ref.at[pl.ds(2 * depth + n * W, W)],
+                sems.at[2 + n],
+            )
+        )
+    for copy in copies:
+        copy.start()
+    for copy in copies:
+        copy.wait()
+
+
+def columns_of(rows):
+    spare = jnp.zeros((6, rows.shape[1]), rows.dtype)
+    return jnp.concatenate([rows, spare], axis=0).T
+
+
+def mixer_kernel(*refs):
+    pair_ref, map_ref, loc_ref = refs[6:9]
+    held, sems = refs[9:15], refs[15]
+    copies = [
+        pltpu.make_async_copy(refs[n], held[n], sems.at[n]) for n in range(len(held))
+    ]
+    for copy in copies:
+        copy.start()
+    for copy in copies:
+        copy.wait()
+    q_ref, k_ref, v_ref, s_ref, f_ref, b_ref = held
+    bias_columns = columns_of(b_ref[...])
     rows = q_ref.shape[0]
     chunks = rows // SEG
     query = q_ref[...].astype(F32)
     key = k_ref[...].astype(F32)
     value = v_ref[...].astype(F32)
     rate = 1.0 / (1.0 + jnp.exp(-s_ref[...].astype(F32)))
-    bias = jnp.where(iota((rows, W), 1) < SEG, b_ref[:, 0:1], b_ref[:, 1:2])
+    bias = jnp.where(iota((rows, W), 1) < SEG, bias_columns[:, 0:1], bias_columns[:, 1:2])
     decay = bias - DECAY / (1.0 + jnp.exp(-f_ref[...]))
     removal = key * lax.rsqrt(mm(key * key, same_head_ones()) + 1e-06)
     beta = removal * rate
@@ -179,13 +215,14 @@
     for n in range(keep_ref.shape[0]):
         part = jnp.dot(mixed, w_ref[:, n * 2 * W : (n + 1) * 2 * W], preferred_element_type=F32)
         first, second = part[:, :W], part[:, W:]
-        keep_ref[n] = jnp.where(core == 0, first, second)
+        keep_ref[n] = jnp.where(core == 0, first, second).astype(BF16)
         send_ref[n] = jnp.where(core == 0, second, first).astype(BF16)
 
 
 def slots_of(ids_ref, experts, capacity):
-    tokens = ids_ref.shape[0]
-    names = [ids_ref[:, k : k + 1] for k in range(2)]
+    tokens = ids_ref.shape[1]
+    named = columns_of(ids_ref[...].astype(F32)).astype(jnp.int32)
+    names = [named[:, k : k + 1] for k in range(2)]
     hot = [(iota((tokens, experts), 1) == name).astype(F32) for name in names]
     earlier = (iota((tokens, tokens), 0) > iota((tokens, tokens), 1)).astype(BF16)
     ahead = jnp.dot(earlier, (hot[0] + hot[1]).astype(BF16), preferred_element_type=F32)
@@ -196,13 +233,14 @@
     return [name * capacity + rank.astype(jnp.int32) for name, rank in zip(names, ranks)]
 
 
-def dispatch_kernel(parts_ref, skip_ref, gain_ref, ids_ref, hid_ref, out_ref):
+def dispatch_kernel(pos_ref, parts_ref, skip_ref, gain_ref, ids_ref, hid_ref, out_ref):
     hidden = skip_ref[...].astype(F32)
     for n in range(parts_ref.shape[0]):
         hidden = hidden + parts_ref[n].astype(F32)
     hid_ref[...] = hidden
-    scaled = (hidden * gain_ref[...]).astype(BF16)
-    tokens, places = ids_ref.shape[0], out_ref.shape[0]
+    column = pl.multiple_of((pos_ref[2] * 2 + pos_ref[3]) * W, W)
+    scaled = (hidden * gain_ref[:, pl.ds(column, W)]).astype(BF16)
+    tokens, places = ids_ref.shape[1], out_ref.shape[0]
     first, second = slots_of(ids_ref, 32, 32)
     lane = iota((tokens, places), 1)
     hot = ((lane == first) | (lane == second)).astype(F32).astype(BF16)
@@ -211,7 +249,7 @@
     ).astype(BF16)
 
 
-def expert_kernel(pos_ref, own_ref, other_ref, inv_gain_ref, w0, w1, w2, w3, keep_ref, send_ref):
+def expert_kernel(pos_ref, own_ref, other_ref, gain_ref, w0, w1, w2, w3, keep_ref, send_ref):
     core = pos_ref[3]
     ways, rows = own_ref.shape[0], own_ref.shape[1]
     blocks = []
@@ -223,7 +261,7 @@
     width = data.shape[1]
     squares = jnp.zeros((rows, W), F32)
     for n, block in enumerate(blocks):
-        plain = block.astype(F32) * inv_gain_ref[:, n * W : (n + 1) * W]
+        plain = block.astype(F32) * (1.0 / gain_ref[:, n * W : (n + 1) * W])
         squares = squares + plain * plain
     scale = lax.rsqrt(jnp.sum(squares, axis=1, keepdims=True) * (1.0 / width) + 1e-06)
     hidden = []
@@ -241,21 +279,21 @@
         ]
         part = jnp.dot(hidden, jnp.concatenate(pieces, axis=0), preferred_element_type=F32)
         first, second = part[:, :W], part[:, W:]
-        keep_ref[n] = jnp.where(core == 0, first, second)
+        keep_ref[n] = jnp.where(core == 0, first, second).astype(BF16)
         send_ref[n] = jnp.where(core == 0, second, first).astype(BF16)
 
 
 def combine_kernel(ret_ref, hid_ref, ids_ref, chance_ref, within_ref, out_ref):
-    tokens, places = ids_ref.shape[0], ret_ref.shape[0]
+    tokens, places = ids_ref.shape[1], ret_ref.shape[0]
     slots = slots_of(ids_ref, 32, 32)
     lane = iota((tokens, places), 1)
     within = within_ref[...]
-    whole = within[:, 0:1] + within[:, 1:2]
+    shares = columns_of(chance_ref[...] * within / jnp.sum(within, axis=0, keepdims=True))
     result = hid_ref[...]
     for k in range(2):
         hot = (lane == slots[k]).astype(F32).astype(BF16)
         picked = jnp.dot(hot, ret_ref[...], preferred_element_type=F32)
-        result = result + picked * (chance_ref[...] * within[:, k : k + 1] / whole)
+        result = result + picked * shares[:, k : k + 1]
     result = result.astype(BF16)
     for n in range(out_ref.shape[0]):
         out_ref[n] = result
@@ -269,9 +307,11 @@
         out_ref[:, (2 * n + 1) * W : (2 * n + 2) * W] = jnp.where(core == 0, other, own)
 
 
-def call(kernel, outs, *args, scalars=0, flops=1_000_000):
+def call(kernel, outs, *args, scalars=0, flops=2_000_000_000, far=(), scratch=(), grant=40 << 20):
     specs = [
-        pl.BlockSpec(memory_space=pltpu.SMEM if n < scalars else pltpu.VMEM)
+        pl.BlockSpec(
+            memory_space=pltpu.SMEM if n < scalars else pltpu.HBM if n in far else pltpu.VMEM
+        )
         for n in range(len(args))
     ]
     shapes = [jax.ShapeDtypeStruct(shape, kind) for shape, kind in outs]
@@ -279,10 +319,11 @@
         kernel,
         out_shape=shapes if len(shapes) > 1 else shapes[0],
         in_specs=specs,
+        scratch_shapes=list(scratch),
         out_specs=[pl.BlockSpec(memory_space=pltpu.VMEM)] * len(shapes)
         if len(shapes) > 1
         else pl.BlockSpec(memory_space=pltpu.VMEM),
-        compiler_params=pltpu.CompilerParams(vmem_limit_bytes=40 * 1024 * 1024),
+        compiler_params=pltpu.CompilerParams(vmem_limit_bytes=grant),
         cost_estimate=pl.CostEstimate(flops=flops, bytes_accessed=1_000_000, transcendentals=0),
         interpret=INTERPRET,
     )(*args)
@@ -319,10 +360,22 @@
     here = [lax.axis_index(a) for a in ("x", "z", "y", "c")]
     pos = jnp.stack(here).astype(jnp.int32)
     tokens, width = skip.shape
-    column = (here[2] * 2 + here[3]) * W
 
     ring = [(((y + 1) % n_y) * 2, y * 2) for y in range(n_y)]
     ring += [(((y - 1) % n_y) * 2 + 1, y * 2 + 1) for y in range(n_y)]
+    weights = [
+        call(
+            pack_kernel,
+            [((3 * width, W), BF16)],
+            switch,
+            expansion,
+            contraction,
+            far=(0, 1, 2),
+            scratch=[pltpu.SemaphoreType.DMA((2 + width // W,))],
+            grant=67043328,
+        )
+    ]
+    weights.append(lax.ppermute(weights[-1], TP, ring))
     pairs, state_map, local = call(
         mixer_kernel,
         [((n_x, W, W), BF16), ((tokens, W), F32), ((tokens, W), F32)],
@@ -331,23 +384,28 @@
         values,
         step_sizes,
         forgetting,
-        forgetting_bias,
-    )
-    pairs, switch, expansion, contraction = lax.optimization_barrier(
-        (pairs, switch, expansion, contraction)
-    )
-    down = contraction[0].reshape(W, width // W, W).transpose(1, 0, 2).reshape(width, W)
-    weights = [jnp.concatenate([switch[0], expansion[0], down], axis=0)]
-    weights.append(lax.ppermute(weights[-1], TP, ring))
+        forgetting_bias.T,
+        far=range(6),
+        scratch=[pltpu.VMEM((tokens, W), BF16)] * 4
+        + [
+            pltpu.VMEM((tokens, W), F32),
+            pltpu.VMEM((2, tokens), F32),
+            pltpu.SemaphoreType.DMA((6,)),
+        ],
+        grant=67043328,
+    )
+    own_skip = lax.dynamic_slice_in_dim(skip, (here[2] * 2 + here[3]) * W, W, 1)
+    pairs, own_skip = lax.optimization_barrier((pairs, own_skip))
     gathered = exchange(pairs, "x")
     pairs, prefix = call(
         compose_kernel, [((n_z, W, W), BF16), ((2 * W, W), F32)], pos, gathered, scalars=1
     )
+    pairs, weights[1] = lax.optimization_barrier((pairs, weights[1]))
     weights.append(lax.ppermute(weights[-1], TP, ring))
     gathered = exchange(pairs, "z")
     keep, send = call(
         readout_kernel,
-        [((n_y, tokens, W), F32), ((n_y, tokens, W), BF16)],
+        [((n_y, tokens, W), BF16), ((n_y, tokens, W), BF16)],
         pos,
         gathered,
         prefix,
@@ -357,30 +415,34 @@
         blender,
         scalars=1,
     )
-    parts = exchange((keep + swap_cores(send).astype(F32)).astype(BF16), "y")
+    branch = (keep.astype(F32) + swap_cores(send).astype(F32)).astype(BF16)
+    branch, weights[2] = lax.optimization_barrier((branch, weights[2]))
+    parts = exchange(branch, "y")
     parts, weights[2] = lax.optimization_barrier((parts, weights[2]))
     weights.append(lax.ppermute(weights[-1], TP, ring))
     hidden, outgoing = call(
         dispatch_kernel,
         [((tokens, W), F32), ((4 * tokens, W), BF16)],
+        pos,
         parts,
-        lax.dynamic_slice_in_dim(skip, column, W, 1),
-        lax.dynamic_slice_in_dim(norm_gain, column, W, 0)[None],
-        ids,
+        own_skip,
+        norm_gain[None],
+        ids.T,
+        scalars=1,
     )
     arrived = exchange(outgoing.reshape(n_z * n_x, -1, W), SP).reshape(4, tokens, W)
     own = exchange(jnp.concatenate([arrived, arrived], axis=0), "y")
     keep, send = call(
         expert_kernel,
-        [((n_y, tokens, W), F32), ((n_y, tokens, W), BF16)],
+        [((n_y, tokens, W), BF16), ((n_y, tokens, W), BF16)],
         pos,
         own,
         swap_cores(own),
-        (1.0 / norm_gain)[None],
+        norm_gain[None],
         *weights,
         scalars=1,
     )
-    summed = exchange((keep + swap_cores(send).astype(F32)).astype(BF16), "y")
+    summed = exchange((keep.astype(F32) + swap_cores(send).astype(F32)).astype(BF16), "y")
     summed = (summed[:4].astype(F32) + summed[4:].astype(F32)).astype(BF16)
     returned = exchange(summed.reshape(n_z * n_x, -1, W), SP).reshape(4 * tokens, W)
     copies = call(
@@ -388,9 +450,9 @@
         [((n_y, tokens, W), BF16)],
         returned,
         hidden,
-        ids,
-        cluster_chance[:, None],
-        within_chance,
+        ids.T,
+        cluster_chance[None],
+        within_chance.T,
     )
     own = exchange(copies, "y")
     return call(assemble_kernel, [((tokens, width), BF16)], pos, own, swap_cores(own), scalars=1)

time: 216 us -> 206 us (0.954)
  blocking collectives: 78.9 us -> 119 us
  waiting for transfers between devices: 54.1 us -> 19.3 us
  starting transfers between devices: 51.5 us -> 37.7 us
  local copies, waits for them, and re-layouts: 7.68 us -> 1.52 us
  Pallas kernels: 20.5 us -> 25.6 us
    all_to_all x4 -> x6, blocking collectives: 78.9 us -> 119 us  [exchange(): return lax.all_to_all(parts, axes, split_axis=0, concat_axis=0, tiled=True)]
    all_to_all x4 -> x2, waiting for transfers between devices: 49.6 us -> 13.3 us  [exchange(): return lax.all_to_all(parts, axes, split_axis=0, concat_axis=0, tiled=True)]
    all_to_all x4 -> x2, starting transfers between devices: 22.5 us -> 8.76 us  [exchange(): return lax.all_to_all(parts, axes, split_axis=0, concat_axis=0, tiled=True)]
    unnamed x34 -> x20, local copies, waits for them, and re-layouts: 7.31 us -> 0.05 us
    pallas_call x7 -> x8, Pallas kernels: 20.5 us -> 25.6 us  [call(): pl.pallas_call(kernel, out_shape=shapes if len(shapes) > 1 else shapes[0]...]
  transfers between devices with their start and end apart: 11 -> 9, of which waited for: 7 -> 6; matrix products, arithmetic and copies ran while one was open for 1% -> 1% of each run, Pallas kernels for 2% -> 7%
where the time goes in v1:
time: 206 us; the launch traced here: 205 us
  blocking collectives  119 us (58%)
  starting transfers between devices  37.7 us (18%)
  Pallas kernels  25.6 us (12%)
  waiting for transfers between devices  19.3 us (9%)
    all_to_all x6, blocking collectives, exchange(): return lax.all_to_all(parts, axes, split_axis=0, concat_axis=0, tiled=True)  119 us
    pallas_call x8, Pallas kernels, call(): pl.pallas_call(kernel, out_shape=shapes if len(shapes) > 1 else shapes[0]...  25.6 us
    ppermute x4, starting transfers between devices, swap_cores(): return lax.ppermute(data, 'c', [(0, 1), (1, 0)])  19.8 us
    all_to_all x2, waiting for transfers between devices, exchange(): return lax.all_to_all(parts, axes, split_axis=0, concat_axis=0, tiled=True)  13.3 us
    ppermute x3, starting transfers between devices, body(): weights.append(lax.ppermute(weights[-1], TP, ring))  9.15 us
    all_to_all x2, starting transfers between devices, exchange(): return lax.all_to_all(parts, axes, split_axis=0, concat_axis=0, tiled=True)  8.76 us
    ppermute x4, waiting for transfers between devices, swap_cores(): return lax.ppermute(data, 'c', [(0, 1), (1, 0)])  6.05 us
  transfers between devices with their start and end apart: 9, of which 6 were waited for; matrix products, arithmetic and copies ran while one was open for 1% of the time, Pallas kernels for 7%

profile of v1, /device:TPU:1, one launch (start us, length us, event | category | flops | bytes accessed | tf_op | source)
XLA Modules:
  0.0 205.0 jit_solution(10068659797085350819)
XLA Ops:
  0.0 2.6 %shard_map.156.w0 = bf16[6144,128]{1,0:T(8,128)(2,1)} custom-call(bf16[1,2048,128]{2,1,0:T(8,128)(2,1)} %switch_ref.1, bf16[1,2048,128]{2,1,0:T(8,128)(2,1)} %expansion_ref.1, bf16[1,128,2048]{2,1,0:T(8,128)(2,1)} %contraction_ref.1), custom_call_target="tpu_custom_call" | custom-call | flops 2000000000 | bytes 1000000 | tf_op jit(solution)/shard_map/pallas_call | solution.py:318
  2.6 4.0 %collective-permute-start = (bf16[6144,128]{1,0:T(8,128)(2,1)}, bf16[6144,128]{1,0:T(8,128)(2,1)}, u32[]{:S(2)}, u32[]{:S(2)}) collective-permute-start(bf16[6144,128]{1,0:T(8,128)(2,1)} %shard_map.156.w0), channel_id=1, source_target_pairs={{2,0},{4,2},{6,4},{8,6},{10,8},{12,10},{14,12},{0,14},{15,1},{1,3}... | collective-permute-start | bytes 4718600 | tf_op jit(solution)/shard_map/ppermute | solution.py:378
  6.6 1.5 constant_dynamic-slice_fusion.skip_ref
  8.1 9.1 %shard_map.154 = (bf16[4,128,128]{2,1,0:T(8,128)(2,1)}, f32[256,128]{1,0:T(8,128)}, f32[256,128]{1,0:T(8,128)}) custom-call(bf16[256,128]{1,0:T(8,128)(2,1)} %refs_0_.1, bf16[256,128]{1,0:T(8,128)(2,1)} %refs_1_.1, bf16[256,128]{1,0:T(8,128)(2,1)} %refs_2_.1, bf16[256,128]{1,0:T(8,128)(2,1)} %refs_3_.1, f32[256,128]{1,0:T(8,128)} %refs_4_.1, f32[2,256]{1,0:T(2,128)} %bitcast.23), custom_call_target="tpu_custom_call" | custom-call | flops 2000000000 | bytes 1000000 | tf_op jit(solution)/shard_map/pallas_call | solution.py:318
  17.3 4.0 %all-to-all-start = ((bf16[4,128,128]{2,1,0:T(8,128)(2,1)}), bf16[4,128,128]{2,1,0:T(8,128)(2,1)S(1)}, u32[]{:S(2)}, u32[]{:S(2)}) async-start(bf16[4,128,128]{2,1,0:T(8,128)(2,1)} %get-tuple-element.25), calls=%async_computation | async-start | bytes 262144 | tf_op jit(solution)/shard_map/all_to_all | solution.py:334
  21.4 4.7 %all-to-all-done.got_ref = bf16[4,128,128]{2,1,0:T(8,128)(2,1)S(1)} async-done(((bf16[4,128,128]{2,1,0:T(8,128)(2,1)}), bf16[4,128,128]{2,1,0:T(8,128)(2,1)S(1)}, u32[]{:S(2)}, u32[]{:S(2)}) %all-to-all-start) | async-done | bytes 131104 | tf_op jit(solution)/shard_map/all_to_all | solution.py:334
  26.1 1.4 shard_map.155
  27.5 3.2 %collective-permute-start.2 = (bf16[6144,128]{1,0:T(8,128)(2,1)}, bf16[6144,128]{1,0:T(8,128)(2,1)S(1)}, u32[]{:S(2)}, u32[]{:S(2)}) collective-permute-start(bf16[6144,128]{1,0:T(8,128)(2,1)} %collective-permute-done.w1), channel_id=1, source_target_pairs={{2,0},{4,2},{6,4},{8,6},{10,8},{12,10},{14,12},{0,14},{15,1},{1,3}... | collective-permute-start | bytes 4718600 | tf_op jit(solution)/shard_map/ppermute | solution.py:404
  30.7 19.4 %all_to_all.40.got_ref = bf16[8,128,128]{2,1,0:T(8,128)(2,1)S(1)} all-to-all(bf16[8,128,128]{2,1,0:T(8,128)(2,1)S(1)} %get-tuple-element.27), channel_id=1, replica_groups=mesh['z'=8,'x'=4,'y'=8,'c'=2] {'z'}, dimensions={0} | all-to-all | bytes 524288 | tf_op jit(solution)/shard_map/all_to_all | solution.py:334
  50.2 3.4 %shard_map.157 = (bf16[8,256,128]{2,1,0:T(8,128)(2,1)S(1)}, bf16[8,256,128]{2,1,0:T(8,128)(2,1)S(1)}) custom-call(s32[4]{0:T(128)S(1)} %pad_add_fusion.pos_ref, bf16[8,128,128]{2,1,0:T(8,128)(2,1)S(1)} %all_to_all.40.got_ref, f32[256,128]{1,0:T(8,128)S(1)} %get-tuple-element.28.prefix_ref, f32[256,128]{1,0:T(8,128)S(1)} %copy-done.8, ...), custom_call_target="tpu_custom_call" | custom-call | flops 2000000000 | bytes 1000000 | tf_op jit(solution)/shard_map/pallas_call | solution.py:318
  53.6 7.5 %collective-permute-start.1 = (bf16[8,256,128]{2,1,0:T(8,128)(2,1)S(1)}, bf16[8,256,128]{2,1,0:T(8,128)(2,1)S(1)}, u32[]{:S(2)}, u32[]{:S(2)}) collective-permute-start(bf16[8,256,128]{2,1,0:T(8,128)(2,1)S(1)} %get-tuple-element.32), channel_id=1, source_target_pairs={{0,1},{1,0},{2,3},{3,2},{4,5},{5,4},{6,7},{7,6},{8,9},{9,8},{10,11... | collective-permute-start | bytes 1572872 | tf_op jit(solution)/shard_map/ppermute | solution.py:338
  61.1 1.5 collective-permute-done.1
  62.6 0.1 add_convert_fusion.1
  62.8 19.7 %all_to_all.41.parts_ref = bf16[8,256,128]{2,1,0:T(8,128)(2,1)S(1)} all-to-all(bf16[8,256,128]{2,1,0:T(8,128)(2,1)S(1)} %add_convert_fusion.1), channel_id=1, replica_groups=mesh['z'=8,'x'=4,'y'=8,'c'=2] {'y'}, dimensions={0} | all-to-all | bytes 1048576 | tf_op jit(solution)/shard_map/all_to_all | solution.py:334
  82.5 2.3 %shard_map.158 = (f32[256,128]{1,0:T(8,128)S(1)}, bf16[1024,128]{1,0:T(8,128)(2,1)}) custom-call(s32[4]{0:T(128)S(1)} %pad_add_fusion.pos_ref, bf16[8,256,128]{2,1,0:T(8,128)(2,1)S(1)} %all_to_all.41.parts_ref, bf16[256,128]{1,0:T(8,128)(2,1)S(1)} %copy-done, f32[1,2048]{1,0:T(1,128)S(1)} %bitcast.15, s32[2,256]{1,0:T(2,128)S(1)} %bitcast.17), custom_call_target="tpu_custom_call" | custom-call | flops 2000000000 | bytes 1000000 | tf_op jit(solution)/shard_map/pallas_call | solution.py:318
  84.8 4.7 %all-to-all-start.3 = ((bf16[32,32,128]{2,1,0:T(8,128)(2,1)}), bf16[32,32,128]{2,1,0:T(8,128)(2,1)}, u32[]{:S(2)}, u32[]{:S(2)}) async-start(bf16[32,32,128]{2,1,0:T(8,128)(2,1)} %bitcast.8), calls=%async_computation.3 | async-start | bytes 524288 | tf_op jit(solution)/shard_map/all_to_all | solution.py:334
  89.6 1.9 collective-permute-start.4
  91.5 8.5 %all-to-all-done.3 = bf16[32,32,128]{2,1,0:T(8,128)(2,1)} async-done(((bf16[32,32,128]{2,1,0:T(8,128)(2,1)}), bf16[32,32,128]{2,1,0:T(8,128)(2,1)}, u32[]{:S(2)}, u32[]{:S(2)}) %all-to-all-start.3) | async-done | bytes 262176 | tf_op jit(solution)/shard_map/all_to_all | solution.py:334
  100.0 1.1 pad_maximum_fusion
  101.1 22.2 %all_to_all.42.own_ref = bf16[8,256,128]{2,1,0:T(8,128)(2,1)S(1)} all-to-all(bf16[8,256,128]{2,1,0:T(8,128)(2,1)S(1)} %pad_maximum_fusion), channel_id=1, replica_groups=mesh['z'=8,'x'=4,'y'=8,'c'=2] {'y'}, dimensions={0} | all-to-all | bytes 1048576 | tf_op jit(solution)/shard_map/all_to_all | solution.py:334
  123.3 2.7 %collective-permute-start.3 = (bf16[8,256,128]{2,1,0:T(8,128)(2,1)S(1)}, bf16[8,256,128]{2,1,0:T(8,128)(2,1)S(1)}, u32[]{:S(2)}, u32[]{:S(2)}) collective-permute-start(bf16[8,256,128]{2,1,0:T(8,128)(2,1)S(1)} %all_to_all.42.own_ref), channel_id=1, source_target_pairs={{0,1},{1,0},{2,3},{3,2},{4,5},{5,4},{6,7},{7,6},{8,9},{9,8},{10,11... | collective-permute-start | bytes 1572872 | tf_op jit(solution)/shard_map/ppermute | solution.py:338
  126.0 1.5 collective-permute-done.3.other_ref
  127.5 3.8 %shard_map.159 = (bf16[8,256,128]{2,1,0:T(8,128)(2,1)S(1)}, bf16[8,256,128]{2,1,0:T(8,128)(2,1)S(1)}) custom-call(s32[4]{0:T(128)S(1)} %pad_add_fusion.pos_ref, bf16[8,256,128]{2,1,0:T(8,128)(2,1)S(1)} %all_to_all.42.own_ref, bf16[8,256,128]{2,1,0:T(8,128)(2,1)S(1)} %collective-permute-done.3.other_ref, f32[1,2048]{1,0:T(1,128)S(1)} %bitcast.16, ...), custom_call_target="tpu_custom_call" | custom-call | flops 2000000000 | bytes 1000000 | tf_op jit(solution)/shard_map/pallas_call | solution.py:318
  131.3 2.3 %collective-permute-start.5 = (bf16[8,256,128]{2,1,0:T(8,128)(2,1)S(1)}, bf16[8,256,128]{2,1,0:T(8,128)(2,1)S(1)}, u32[]{:S(2)}, u32[]{:S(2)}) collective-permute-start(bf16[8,256,128]{2,1,0:T(8,128)(2,1)S(1)} %get-tuple-element.41), channel_id=1, source_target_pairs={{0,1},{1,0},{2,3},{3,2},{4,5},{5,4},{6,7},{7,6},{8,9},{9,8},{10,11... | collective-permute-start | bytes 1572872 | tf_op jit(solution)/shard_map/ppermute | solution.py:338
  133.6 1.5 collective-permute-done.5
  135.3 22.7 %all_to_all.43 = bf16[8,256,128]{2,1,0:T(8,128)(2,1)S(1)} all-to-all(bf16[8,256,128]{2,1,0:T(8,128)(2,1)S(1)} %add_convert_fusion), channel_id=1, replica_groups=mesh['z'=8,'x'=4,'y'=8,'c'=2] {'y'}, dimensions={0} | all-to-all | bytes 1048576 | tf_op jit(solution)/shard_map/all_to_all | solution.py:334
  158.1 19.6 %all_to_all.44 = bf16[32,32,128]{2,1,0:T(8,128)(2,1)S(1)} all-to-all(bf16[32,32,128]{2,1,0:T(8,128)(2,1)S(1)} %bitcast.22), channel_id=1, replica_groups=mesh['z'=8,'x'=4,'y'=8,'c'=2] {'z','x'}, dimensions={0} | all-to-all | bytes 524288 | tf_op jit(solution)/shard_map/all_to_all | solution.py:334
  177.8 1.2 shard_map.160
  179.0 15.4 %all_to_all.45.own_ref = bf16[8,256,128]{2,1,0:T(8,128)(2,1)S(1)} all-to-all(bf16[8,256,128]{2,1,0:T(8,128)(2,1)S(1)} %shard_map.160), channel_id=1, replica_groups=mesh['z'=8,'x'=4,'y'=8,'c'=2] {'y'}, dimensions={0} | all-to-all | bytes 1048576 | tf_op jit(solution)/shard_map/all_to_all | solution.py:334
  194.4 7.3 %collective-permute-start.6 = (bf16[8,256,128]{2,1,0:T(8,128)(2,1)S(1)}, bf16[8,256,128]{2,1,0:T(8,128)(2,1)S(1)}, u32[]{:S(2)}, u32[]{:S(2)}) collective-permute-start(bf16[8,256,128]{2,1,0:T(8,128)(2,1)S(1)} %all_to_all.45.own_ref), channel_id=1, source_target_pairs={{0,1},{1,0},{2,3},{3,2},{4,5},{5,4},{6,7},{7,6},{8,9},{9,8},{10,11... | collective-permute-start | bytes 1572872 | tf_op jit(solution)/shard_map/ppermute | solution.py:338
  201.8 1.5 collective-permute-done.6.other_ref
  203.3 1.7 shard_map.161
  (26 shorter events, 0.3 us)
Async XLA Ops:
  2.6 24.9 %collective-permute-start = (bf16[6144,128]{1,0:T(8,128)(2,1)}, bf16[6144,128]{1,0:T(8,128)(2,1)}, u32[]{:S(2)}, u32[]{:S(2)}) collective-permute-start(bf16[6144,128]{1,0:T(8,128)(2,1)} %shard_map.156.w0), channel_id=1, source_target_pairs={{2,0},{4,2},{6,4},{8,6},{10,8},{12,10},{14,12},{0,14},{15,1},{1,3}... | collective-permute-start | bytes 4718600 | tf_op jit(solution)/shard_map/ppermute | solution.py:378
  17.3 8.9 %all-to-all-start = ((bf16[4,128,128]{2,1,0:T(8,128)(2,1)}), bf16[4,128,128]{2,1,0:T(8,128)(2,1)S(1)}, u32[]{:S(2)}, u32[]{:S(2)}) async-start(bf16[4,128,128]{2,1,0:T(8,128)(2,1)} %get-tuple-element.25), calls=%async_computation | async-start | bytes 262144 | tf_op jit(solution)/shard_map/all_to_all | solution.py:334
  21.4 28.8 %copy-start.2 = (bf16[128,2048]{1,0:T(8,128)(2,1)S(1)}, bf16[128,2048]{1,0:T(8,128)(2,1)}, u32[]{:S(2)}) copy-start(bf16[128,2048]{1,0:T(8,128)(2,1)} %w_ref.1) | copy-start | bytes 1572868
  21.4 28.8 %copy-start.7 = (f32[128]{0:T(128)S(1)}, f32[128]{0:T(128)}, u32[]{:S(2)}) copy-start(f32[128]{0:T(128)} %param.22) | copy-start | bytes 1540
  21.4 28.8 %copy-start.8 = (f32[256,128]{1,0:T(8,128)S(1)}, f32[256,128]{1,0:T(8,128)}, u32[]{:S(2)}) copy-start(f32[256,128]{1,0:T(8,128)} %get-tuple-element.29.map_ref) | copy-start | bytes 393220
  21.4 28.8 %copy-start.9 = (f32[256,128]{1,0:T(8,128)S(1)}, f32[256,128]{1,0:T(8,128)}, u32[]{:S(2)}) copy-start(f32[256,128]{1,0:T(8,128)} %get-tuple-element.30.loc_ref) | copy-start | bytes 393220
  27.5 35.3 %collective-permute-start.2 = (bf16[6144,128]{1,0:T(8,128)(2,1)}, bf16[6144,128]{1,0:T(8,128)(2,1)S(1)}, u32[]{:S(2)}, u32[]{:S(2)}) collective-permute-start(bf16[6144,128]{1,0:T(8,128)(2,1)} %collective-permute-done.w1), channel_id=1, source_target_pairs={{2,0},{4,2},{6,4},{8,6},{10,8},{12,10},{14,12},{0,14},{15,1},{1,3}... | collective-permute-start | bytes 4718600 | tf_op jit(solution)/shard_map/ppermute | solution.py:404
  53.5 28.9 %copy-start = (bf16[256,128]{1,0:T(8,128)(2,1)S(1)}, bf16[256,128]{1,0:T(8,128)(2,1)}, u32[]{:S(2)}) copy-start(bf16[256,128]{1,0:T(8,128)(2,1)} %constant_dynamic-slice_fusion.skip_ref) | copy-start | bytes 196612
  53.6 28.9 %copy-start.3 = (f32[2048]{0:T(1024)S(1)}, f32[2048]{0:T(1024)}, u32[]{:S(2)}) copy-start(f32[2048]{0:T(1024)} %param.25) | copy-start | bytes 24580
  53.6 28.9 %copy-start.4 = (s32[256,2]{0,1:T(2,128)S(1)}, s32[256,2]{0,1:T(2,128)}, u32[]{:S(2)}) copy-start(s32[256,2]{0,1:T(2,128)} %param.28) | copy-start | bytes 6148
  53.6 9.1 %collective-permute-start.1 = (bf16[8,256,128]{2,1,0:T(8,128)(2,1)S(1)}, bf16[8,256,128]{2,1,0:T(8,128)(2,1)S(1)}, u32[]{:S(2)}, u32[]{:S(2)}) collective-permute-start(bf16[8,256,128]{2,1,0:T(8,128)(2,1)S(1)} %get-tuple-element.32), channel_id=1, source_target_pairs={{0,1},{1,0},{2,3},{3,2},{4,5},{5,4},{6,7},{7,6},{8,9},{9,8},{10,11... | collective-permute-start | bytes 1572872 | tf_op jit(solution)/shard_map/ppermute | solution.py:338
  84.8 42.7 %copy-start.1 = (bf16[6144,128]{1,0:T(8,128)(2,1)S(1)}, bf16[6144,128]{1,0:T(8,128)(2,1)}, u32[]{:S(2)}) copy-start(bf16[6144,128]{1,0:T(8,128)(2,1)} %shard_map.156.w0) | copy-start | bytes 4718596
  84.8 15.2 %all-to-all-start.3 = ((bf16[32,32,128]{2,1,0:T(8,128)(2,1)}), bf16[32,32,128]{2,1,0:T(8,128)(2,1)}, u32[]{:S(2)}, u32[]{:S(2)}) async-start(bf16[32,32,128]{2,1,0:T(8,128)(2,1)} %bitcast.8), calls=%async_computation.3 | async-start | bytes 524288 | tf_op jit(solution)/shard_map/all_to_all | solution.py:334
  89.6 36.4 %collective-permute-start.4 = (bf16[6144,128]{1,0:T(8,128)(2,1)S(1)}, bf16[6144,128]{1,0:T(8,128)(2,1)}, u32[]{:S(2)}, u32[]{:S(2)}) collective-permute-start(bf16[6144,128]{1,0:T(8,128)(2,1)S(1)} %collective-permute-done.2.w2), channel_id=1, source_target_pairs={{2,0},{4,2},{6,4},{8,6},{10,8},{12,10},{14,12},{0,14},{15,1},{1,3}... | collective-permute-start | bytes 4718600 | tf_op jit(solution)/shard_map/ppermute | solution.py:422
  123.3 4.2 %collective-permute-start.3 = (bf16[8,256,128]{2,1,0:T(8,128)(2,1)S(1)}, bf16[8,256,128]{2,1,0:T(8,128)(2,1)S(1)}, u32[]{:S(2)}, u32[]{:S(2)}) collective-permute-start(bf16[8,256,128]{2,1,0:T(8,128)(2,1)S(1)} %all_to_all.42.own_ref), channel_id=1, source_target_pairs={{0,1},{1,0},{2,3},{3,2},{4,5},{5,4},{6,7},{7,6},{8,9},{9,8},{10,11... | collective-permute-start | bytes 1572872 | tf_op jit(solution)/shard_map/ppermute | solution.py:338
  131.3 3.8 %collective-permute-start.5 = (bf16[8,256,128]{2,1,0:T(8,128)(2,1)S(1)}, bf16[8,256,128]{2,1,0:T(8,128)(2,1)S(1)}, u32[]{:S(2)}, u32[]{:S(2)}) collective-permute-start(bf16[8,256,128]{2,1,0:T(8,128)(2,1)S(1)} %get-tuple-element.41), channel_id=1, source_target_pairs={{0,1},{1,0},{2,3},{3,2},{4,5},{5,4},{6,7},{7,6},{8,9},{9,8},{10,11... | collective-permute-start | bytes 1572872 | tf_op jit(solution)/shard_map/ppermute | solution.py:338
  135.3 42.5 %copy-start.5 = (f32[256,2]{0,1:T(2,128)S(1)}, f32[256,2]{0,1:T(2,128)}, u32[]{:S(2)}) copy-start(f32[256,2]{0,1:T(2,128)} %param.27) | copy-start | bytes 6148
  135.3 42.5 %copy-start.6 = (f32[256]{0:T(256)S(1)}, f32[256]{0:T(256)}, u32[]{:S(2)}) copy-start(f32[256]{0:T(256)} %param.26) | copy-start | bytes 3076
  194.4 8.8 %collective-permute-start.6 = (bf16[8,256,128]{2,1,0:T(8,128)(2,1)S(1)}, bf16[8,256,128]{2,1,0:T(8,128)(2,1)S(1)}, u32[]{:S(2)}, u32[]{:S(2)}) collective-permute-start(bf16[8,256,128]{2,1,0:T(8,128)(2,1)S(1)} %all_to_all.45.own_ref), channel_id=1, source_target_pairs={{0,1},{1,0},{2,3},{3,2},{4,5},{5,4},{6,7},{7,6},{8,9},{9,8},{10,11... | collective-permute-start | bytes 1572872 | tf_op jit(solution)/shard_map/ppermute | solution.py:338

commit v2 on v1

--- a/solution.py
+++ b/solution.py
@@ -240,28 +240,30 @@
     hid_ref[...] = hidden
     column = pl.multiple_of((pos_ref[2] * 2 + pos_ref[3]) * W, W)
     scaled = (hidden * gain_ref[:, pl.ds(column, W)]).astype(BF16)
-    tokens, places = ids_ref.shape[1], out_ref.shape[0]
+    tokens, places = ids_ref.shape[1], out_ref.shape[0] * out_ref.shape[1] // 2
     first, second = slots_of(ids_ref, 32, 32)
     lane = iota((tokens, places), 1)
     hot = ((lane == first) | (lane == second)).astype(F32).astype(BF16)
-    out_ref[...] = lax.dot_general(
-        hot, scaled, (((0,), (0,)), ((), ())), preferred_element_type=F32
-    ).astype(BF16)
+    rows = lax.dot_general(hot, scaled, (((0,), (0,)), ((), ())), preferred_element_type=F32)
+    rows = rows.astype(BF16).reshape(32, 32, W)
+    out_ref[:, :32, :] = rows
+    out_ref[:, 32:, :] = rows
 
 
 def expert_kernel(pos_ref, own_ref, other_ref, gain_ref, w0, w1, w2, w3, keep_ref, send_ref):
     core = pos_ref[3]
-    ways, rows = own_ref.shape[0], own_ref.shape[1]
+    sources, ways, lines, _ = own_ref.shape
+    rows, width = sources * lines, gain_ref.shape[1]
     blocks = []
     for n in range(ways):
-        own, other = own_ref[n], other_ref[n]
+        own = own_ref[:, n].astype(F32).reshape(rows, W)
+        other = other_ref[:, n].astype(F32).reshape(rows, W)
         blocks.append(jnp.where(core == 0, own, other))
         blocks.append(jnp.where(core == 0, other, own))
-    data = jnp.concatenate(blocks, axis=1)
-    width = data.shape[1]
+    data = jnp.concatenate([block.astype(BF16) for block in blocks], axis=1)
     squares = jnp.zeros((rows, W), F32)
     for n, block in enumerate(blocks):
-        plain = block.astype(F32) * (1.0 / gain_ref[:, n * W : (n + 1) * W])
+        plain = block * (1.0 / gain_ref[:, n * W : (n + 1) * W])
         squares = squares + plain * plain
     scale = lax.rsqrt(jnp.sum(squares, axis=1, keepdims=True) * (1.0 / width) + 1e-06)
     hidden = []
@@ -279,12 +281,17 @@
         ]
         part = jnp.dot(hidden, jnp.concatenate(pieces, axis=0), preferred_element_type=F32)
         first, second = part[:, :W], part[:, W:]
-        keep_ref[n] = jnp.where(core == 0, first, second).astype(BF16)
-        send_ref[n] = jnp.where(core == 0, second, first).astype(BF16)
+        keep = jnp.where(core == 0, first, second).reshape(sources, lines, W)
+        send = jnp.where(core == 0, second, first).reshape(sources, lines, W)
+        keep_ref[:, n] = keep.astype(BF16)
+        send_ref[:, n] = send.astype(BF16)
 
 
 def combine_kernel(ret_ref, hid_ref, ids_ref, chance_ref, within_ref, out_ref):
-    tokens, places = ids_ref.shape[1], ret_ref.shape[0]
+    half = ret_ref.shape[1] // 2
+    rows = ret_ref[:, :half].astype(F32) + ret_ref[:, half:].astype(F32)
+    rows = rows.reshape(-1, W).astype(BF16)
+    tokens, places = ids_ref.shape[1], rows.shape[0]
     slots = slots_of(ids_ref, 32, 32)
     lane = iota((tokens, places), 1)
     within = within_ref[...]
@@ -292,7 +299,7 @@
     result = hid_ref[...]
     for k in range(2):
         hot = (lane == slots[k]).astype(F32).astype(BF16)
-        picked = jnp.dot(hot, ret_ref[...], preferred_element_type=F32)
+        picked = jnp.dot(hot, rows, preferred_element_type=F32)
         result = result + picked * shares[:, k : k + 1]
     result = result.astype(BF16)
     for n in range(out_ref.shape[0]):
@@ -395,8 +402,8 @@
         grant=67043328,
     )
     own_skip = lax.dynamic_slice_in_dim(skip, (here[2] * 2 + here[3]) * W, W, 1)
-    pairs, own_skip = lax.optimization_barrier((pairs, own_skip))
     gathered = exchange(pairs, "x")
+    gathered, own_skip = lax.optimization_barrier((gathered, own_skip))
     pairs, prefix = call(
         compose_kernel, [((n_z, W, W), BF16), ((2 * W, W), F32)], pos, gathered, scalars=1
     )
@@ -422,7 +429,7 @@
     weights.append(lax.ppermute(weights[-1], TP, ring))
     hidden, outgoing = call(
         dispatch_kernel,
-        [((tokens, W), F32), ((4 * tokens, W), BF16)],
+        [((tokens, W), F32), ((n_z * n_x, 64, W), BF16)],
         pos,
         parts,
         own_skip,
@@ -430,11 +437,11 @@
         ids.T,
         scalars=1,
     )
-    arrived = exchange(outgoing.reshape(n_z * n_x, -1, W), SP).reshape(4, tokens, W)
-    own = exchange(jnp.concatenate([arrived, arrived], axis=0), "y")
+    own = exchange(outgoing.reshape(n_z * n_x * n_y, 8, W), ("z", "x", "y"))
+    own = own.reshape(n_z * n_x, n_y, 8, W)
     keep, send = call(
         expert_kernel,
-        [((n_y, tokens, W), BF16), ((n_y, tokens, W), BF16)],
+        [((n_z * n_x, n_y, 8, W), BF16), ((n_z * n_x, n_y, 8, W), BF16)],
         pos,
         own,
         swap_cores(own),
@@ -442,9 +449,9 @@
         *weights,
         scalars=1,
     )
-    summed = exchange((keep.astype(F32) + swap_cores(send).astype(F32)).astype(BF16), "y")
-    summed = (summed[:4].astype(F32) + summed[4:].astype(F32)).astype(BF16)
-    returned = exchange(summed.reshape(n_z * n_x, -1, W), SP).reshape(4 * tokens, W)
+    summed = (keep.astype(F32) + swap_cores(send).astype(F32)).astype(BF16)
+    returned = exchange(summed.reshape(n_z * n_x * n_y, 8, W), ("z", "x", "y"))
+    returned = returned.reshape(n_z * n_x, n_y, 8, W)
     copies = call(
         combine_kernel,
         [((n_y, tokens, W), BF16)],

time: 206 us -> 193 us (0.937)
  waiting for transfers between devices: 19.3 us -> 10.6 us
  starting transfers between devices: 37.7 us -> 30.2 us
  blocking collectives: 119 us -> 126 us
    all_to_all x2 -> x1, waiting for transfers between devices: 13.3 us -> 3.89 us  [exchange(): return lax.all_to_all(parts, axes, split_axis=0, concat_axis=0, tiled=True)]
    all_to_all x6 -> x5, blocking collectives: 119 us -> 126 us  [exchange(): return lax.all_to_all(parts, axes, split_axis=0, concat_axis=0, tiled=True)]
    all_to_all x2 -> x1, starting transfers between devices: 8.76 us -> 4.02 us  [exchange(): return lax.all_to_all(parts, axes, split_axis=0, concat_axis=0, tiled=True)]
    ppermute x4, starting transfers between devices: 19.8 us -> 17.6 us  [swap_cores(): return lax.ppermute(data, 'c', [(0, 1), (1, 0)])]
  transfers between devices with their start and end apart: 9 -> 8, of which waited for: 6 -> 6; matrix products, arithmetic and copies ran while one was open for 1% -> 1% of each run, Pallas kernels for 7% -> 8%
where the time goes in v2:
time: 193 us; the launch traced here: 192 us
  blocking collectives  126 us (65%)
  starting transfers between devices  30.2 us (16%)
  Pallas kernels  24.5 us (13%)
  waiting for transfers between devices  10.6 us (5%)
    all_to_all x5, blocking collectives, exchange(): return lax.all_to_all(parts, axes, split_axis=0, concat_axis=0, tiled=True)  126 us
    pallas_call x8, Pallas kernels, call(): pl.pallas_call(kernel, out_shape=shapes if len(shapes) > 1 else shapes[0]...  24.5 us
    ppermute x4, starting transfers between devices, swap_cores(): return lax.ppermute(data, 'c', [(0, 1), (1, 0)])  17.6 us
    ppermute x3, starting transfers between devices, body(): weights.append(lax.ppermute(weights[-1], TP, ring))  8.55 us
    ppermute x4, waiting for transfers between devices, swap_cores(): return lax.ppermute(data, 'c', [(0, 1), (1, 0)])  6.07 us
    all_to_all x1, starting transfers between devices, exchange(): return lax.all_to_all(parts, axes, split_axis=0, concat_axis=0, tiled=True)  4.02 us
    all_to_all x1, waiting for transfers between devices, exchange(): return lax.all_to_all(parts, axes, split_axis=0, concat_axis=0, tiled=True)  3.89 us
  transfers between devices with their start and end apart: 8, of which 6 were waited for; matrix products, arithmetic and copies ran while one was open for 1% of the time, Pallas kernels for 8%

profile of v2, /device:TPU:1, one launch (start us, length us, event | category | flops | bytes accessed | tf_op | source)
XLA Modules:
  0.0 192.5 jit_solution(9884112152463296289)
XLA Ops:
  0.0 2.6 %shard_map.156.w0 = bf16[6144,128]{1,0:T(8,128)(2,1)} custom-call(bf16[1,2048,128]{2,1,0:T(8,128)(2,1)} %switch_ref.1, bf16[1,2048,128]{2,1,0:T(8,128)(2,1)} %expansion_ref.1, bf16[1,128,2048]{2,1,0:T(8,128)(2,1)} %contraction_ref.1), custom_call_target="tpu_custom_call" | custom-call | flops 2000000000 | bytes 1000000 | tf_op jit(solution)/shard_map/pallas_call | solution.py:325
  2.6 4.0 %collective-permute-start = (bf16[6144,128]{1,0:T(8,128)(2,1)}, bf16[6144,128]{1,0:T(8,128)(2,1)}, u32[]{:S(2)}, u32[]{:S(2)}) collective-permute-start(bf16[6144,128]{1,0:T(8,128)(2,1)} %shard_map.156.w0), channel_id=1, source_target_pairs={{2,0},{4,2},{6,4},{8,6},{10,8},{12,10},{14,12},{0,14},{15,1},{1,3}... | collective-permute-start | bytes 4718600 | tf_op jit(solution)/shard_map/ppermute | solution.py:385
  6.6 9.2 %shard_map.154 = (bf16[4,128,128]{2,1,0:T(8,128)(2,1)}, f32[256,128]{1,0:T(8,128)}, f32[256,128]{1,0:T(8,128)}) custom-call(bf16[256,128]{1,0:T(8,128)(2,1)} %refs_0_.1, bf16[256,128]{1,0:T(8,128)(2,1)} %refs_1_.1, bf16[256,128]{1,0:T(8,128)(2,1)} %refs_2_.1, bf16[256,128]{1,0:T(8,128)(2,1)} %refs_3_.1, f32[256,128]{1,0:T(8,128)} %refs_4_.1, f32[2,256]{1,0:T(2,128)} %bitcast.26), custom_call_target="tpu_custom_call" | custom-call | flops 2000000000 | bytes 1000000 | tf_op jit(solution)/shard_map/pallas_call | solution.py:325
  15.8 4.0 %all-to-all-start = ((bf16[4,128,128]{2,1,0:T(8,128)(2,1)}), bf16[4,128,128]{2,1,0:T(8,128)(2,1)S(1)}, u32[]{:S(2)}, u32[]{:S(2)}) async-start(bf16[4,128,128]{2,1,0:T(8,128)(2,1)} %get-tuple-element.24), calls=%async_computation | async-start | bytes 262144 | tf_op jit(solution)/shard_map/all_to_all | solution.py:341
  19.8 0.8 constant_dynamic-slice_fusion.skip_ref
  20.7 0.1 pad_add_fusion.pos_ref
  20.7 3.9 %all-to-all-done.got_ref = bf16[4,128,128]{2,1,0:T(8,128)(2,1)S(1)} async-done(((bf16[4,128,128]{2,1,0:T(8,128)(2,1)}), bf16[4,128,128]{2,1,0:T(8,128)(2,1)S(1)}, u32[]{:S(2)}, u32[]{:S(2)}) %all-to-all-start) | async-done | bytes 131104 | tf_op jit(solution)/shard_map/all_to_all | solution.py:341
  24.6 1.4 shard_map.155
  26.0 0.6 collective-permute-done.w1
  26.6 2.6 %collective-permute-start.2 = (bf16[6144,128]{1,0:T(8,128)(2,1)}, bf16[6144,128]{1,0:T(8,128)(2,1)S(1)}, u32[]{:S(2)}, u32[]{:S(2)}) collective-permute-start(bf16[6144,128]{1,0:T(8,128)(2,1)} %collective-permute-done.w1), channel_id=1, source_target_pairs={{2,0},{4,2},{6,4},{8,6},{10,8},{12,10},{14,12},{0,14},{15,1},{1,3}... | collective-permute-start | bytes 4718600 | tf_op jit(solution)/shard_map/ppermute | solution.py:411
  29.2 19.4 %all_to_all.30.got_ref = bf16[8,128,128]{2,1,0:T(8,128)(2,1)S(1)} all-to-all(bf16[8,128,128]{2,1,0:T(8,128)(2,1)S(1)} %get-tuple-element.27), channel_id=1, replica_groups=mesh['z'=8,'x'=4,'y'=8,'c'=2] {'z'}, dimensions={0} | all-to-all | bytes 524288 | tf_op jit(solution)/shard_map/all_to_all | solution.py:341
  48.7 3.4 %shard_map.157 = (bf16[8,256,128]{2,1,0:T(8,128)(2,1)S(1)}, bf16[8,256,128]{2,1,0:T(8,128)(2,1)S(1)}) custom-call(s32[4]{0:T(128)S(1)} %pad_add_fusion.pos_ref, bf16[8,128,128]{2,1,0:T(8,128)(2,1)S(1)} %all_to_all.30.got_ref, f32[256,128]{1,0:T(8,128)S(1)} %get-tuple-element.28.prefix_ref, f32[256,128]{1,0:T(8,128)S(1)} %copy-done.7, ...), custom_call_target="tpu_custom_call" | custom-call | flops 2000000000 | bytes 1000000 | tf_op jit(solution)/shard_map/pallas_call | solution.py:325
  52.1 7.4 %collective-permute-start.1 = (bf16[8,256,128]{2,1,0:T(8,128)(2,1)S(1)}, bf16[8,256,128]{2,1,0:T(8,128)(2,1)S(1)}, u32[]{:S(2)}, u32[]{:S(2)}) collective-permute-start(bf16[8,256,128]{2,1,0:T(8,128)(2,1)S(1)} %get-tuple-element.32), channel_id=1, source_target_pairs={{0,1},{1,0},{2,3},{3,2},{4,5},{5,4},{6,7},{7,6},{8,9},{9,8},{10,11... | collective-permute-start | bytes 1572872 | tf_op jit(solution)/shard_map/ppermute | solution.py:345
  59.5 1.5 collective-permute-done.1
  61.0 0.1 add_convert_fusion.1
  61.2 20.1 %all_to_all.31.parts_ref = bf16[8,256,128]{2,1,0:T(8,128)(2,1)S(1)} all-to-all(bf16[8,256,128]{2,1,0:T(8,128)(2,1)S(1)} %add_convert_fusion.1), channel_id=1, replica_groups=mesh['z'=8,'x'=4,'y'=8,'c'=2] {'y'}, dimensions={0} | all-to-all | bytes 1048576 | tf_op jit(solution)/shard_map/all_to_all | solution.py:341
  81.3 1.9 collective-permute-start.4
  83.3 1.6 shard_map.158
  84.9 32.5 %all_to_all.32 = bf16[256,8,128]{2,1,0:T(8,128)(2,1)S(1)} all-to-all(bf16[256,8,128]{2,1,0:T(8,128)(2,1)S(1)} %bitcast.16), channel_id=1, replica_groups=mesh['z'=8,'x'=4,'y'=8,'c'=2] {'z','x','y'}, dimensions={0} | all-to-all | bytes 1048576 | tf_op jit(solution)/shard_map/all_to_all | solution.py:341
  117.4 3.4 %collective-permute-start.3 = (bf16[32,8,8,128]{3,2,1,0:T(8,128)(2,1)S(1)}, bf16[32,8,8,128]{3,2,1,0:T(8,128)(2,1)S(1)}, u32[]{:S(2)}, u32[]{:S(2)}) collective-permute-start(bf16[32,8,8,128]{3,2,1,0:T(8,128)(2,1)S(1)} %bitcast.14), channel_id=1, source_target_pairs={{0,1},{1,0},{2,3},{3,2},{4,5},{5,4},{6,7},{7,6},{8,9},{9,8},{10,11... | collective-permute-start | bytes 1572872 | tf_op jit(solution)/shard_map/ppermute | solution.py:345
  120.8 1.5 collective-permute-done.3.other_ref
  122.3 3.4 %shard_map.159 = (bf16[32,8,8,128]{3,2,1,0:T(8,128)(2,1)S(1)}, bf16[32,8,8,128]{3,2,1,0:T(8,128)(2,1)S(1)}) custom-call(s32[4]{0:T(128)S(1)} %pad_add_fusion.pos_ref, bf16[32,8,8,128]{3,2,1,0:T(8,128)(2,1)S(1)} %bitcast.15, bf16[32,8,8,128]{3,2,1,0:T(8,128)(2,1)S(1)} %collective-permute-done.3.other_ref, f32[1,2048]{1,0:T(1,128)S(1)} %bitcast.19, ...), custom_call_target="tpu_custom_call" | custom-call | flops 2000000000 | bytes 1000000 | tf_op jit(solution)/shard_map/pallas_call | solution.py:325
  125.7 0.0 copy-start.5
  125.7 2.3 %collective-permute-start.5 = (bf16[32,8,8,128]{3,2,1,0:T(8,128)(2,1)S(1)}, bf16[32,8,8,128]{3,2,1,0:T(8,128)(2,1)S(1)}, u32[]{:S(2)}, u32[]{:S(2)}) collective-permute-start(bf16[32,8,8,128]{3,2,1,0:T(8,128)(2,1)S(1)} %get-tuple-element.41), channel_id=1, source_target_pairs={{0,1},{1,0},{2,3},{3,2},{4,5},{5,4},{6,7},{7,6},{8,9},{9,8},{10,11... | collective-permute-start | bytes 1572872 | tf_op jit(solution)/shard_map/ppermute | solution.py:345
  128.0 1.5 collective-permute-done.5
  129.5 0.2 add_convert_fusion
  129.7 34.7 %all_to_all.33 = bf16[256,8,128]{2,1,0:T(8,128)(2,1)S(1)} all-to-all(bf16[256,8,128]{2,1,0:T(8,128)(2,1)S(1)} %bitcast.25), channel_id=1, replica_groups=mesh['z'=8,'x'=4,'y'=8,'c'=2] {'z','x','y'}, dimensions={0} | all-to-all | bytes 1048576 | tf_op jit(solution)/shard_map/all_to_all | solution.py:341
  164.4 1.2 shard_map.160
  165.6 19.0 %all_to_all.34.own_ref = bf16[8,256,128]{2,1,0:T(8,128)(2,1)S(1)} all-to-all(bf16[8,256,128]{2,1,0:T(8,128)(2,1)S(1)} %shard_map.160), channel_id=1, replica_groups=mesh['z'=8,'x'=4,'y'=8,'c'=2] {'y'}, dimensions={0} | all-to-all | bytes 1048576 | tf_op jit(solution)/shard_map/all_to_all | solution.py:341
  184.7 4.6 %collective-permute-start.6 = (bf16[8,256,128]{2,1,0:T(8,128)(2,1)S(1)}, bf16[8,256,128]{2,1,0:T(8,128)(2,1)S(1)}, u32[]{:S(2)}, u32[]{:S(2)}) collective-permute-start(bf16[8,256,128]{2,1,0:T(8,128)(2,1)S(1)} %all_to_all.34.own_ref), channel_id=1, source_target_pairs={{0,1},{1,0},{2,3},{3,2},{4,5},{5,4},{6,7},{7,6},{8,9},{9,8},{10,11... | collective-permute-start | bytes 1572872 | tf_op jit(solution)/shard_map/ppermute | solution.py:345
  189.2 1.5 collective-permute-done.6.other_ref
  190.8 1.7 shard_map.161
  (19 shorter events, 0.0 us)
Async XLA Ops:
  2.6 24.0 %collective-permute-start = (bf16[6144,128]{1,0:T(8,128)(2,1)}, bf16[6144,128]{1,0:T(8,128)(2,1)}, u32[]{:S(2)}, u32[]{:S(2)}) collective-permute-start(bf16[6144,128]{1,0:T(8,128)(2,1)} %shard_map.156.w0), channel_id=1, source_target_pairs={{2,0},{4,2},{6,4},{8,6},{10,8},{12,10},{14,12},{0,14},{15,1},{1,3}... | collective-permute-start | bytes 4718600 | tf_op jit(solution)/shard_map/ppermute | solution.py:385
  15.8 8.8 %all-to-all-start = ((bf16[4,128,128]{2,1,0:T(8,128)(2,1)}), bf16[4,128,128]{2,1,0:T(8,128)(2,1)S(1)}, u32[]{:S(2)}, u32[]{:S(2)}) async-start(bf16[4,128,128]{2,1,0:T(8,128)(2,1)} %get-tuple-element.24), calls=%async_computation | async-start | bytes 262144 | tf_op jit(solution)/shard_map/all_to_all | solution.py:341
  20.7 28.0 %copy-start.1 = (bf16[128,2048]{1,0:T(8,128)(2,1)S(1)}, bf16[128,2048]{1,0:T(8,128)(2,1)}, u32[]{:S(2)}) copy-start(bf16[128,2048]{1,0:T(8,128)(2,1)} %w_ref.1) | copy-start | bytes 1572868
  20.7 28.0 %copy-start.6 = (f32[128]{0:T(128)S(1)}, f32[128]{0:T(128)}, u32[]{:S(2)}) copy-start(f32[128]{0:T(128)} %param.22) | copy-start | bytes 1540
  20.7 28.0 %copy-start.7 = (f32[256,128]{1,0:T(8,128)S(1)}, f32[256,128]{1,0:T(8,128)}, u32[]{:S(2)}) copy-start(f32[256,128]{1,0:T(8,128)} %get-tuple-element.29.map_ref) | copy-start | bytes 393220
  20.7 28.0 %copy-start.8 = (f32[256,128]{1,0:T(8,128)S(1)}, f32[256,128]{1,0:T(8,128)}, u32[]{:S(2)}) copy-start(f32[256,128]{1,0:T(8,128)} %get-tuple-element.30.loc_ref) | copy-start | bytes 393220
  26.6 34.6 %collective-permute-start.2 = (bf16[6144,128]{1,0:T(8,128)(2,1)}, bf16[6144,128]{1,0:T(8,128)(2,1)S(1)}, u32[]{:S(2)}, u32[]{:S(2)}) collective-permute-start(bf16[6144,128]{1,0:T(8,128)(2,1)} %collective-permute-done.w1), channel_id=1, source_target_pairs={{2,0},{4,2},{6,4},{8,6},{10,8},{12,10},{14,12},{0,14},{15,1},{1,3}... | collective-permute-start | bytes 4718600 | tf_op jit(solution)/shard_map/ppermute | solution.py:411
  52.1 31.1 %copy-start.2 = (f32[2048]{0:T(1024)S(1)}, f32[2048]{0:T(1024)}, u32[]{:S(2)}) copy-start(f32[2048]{0:T(1024)} %param.25) | copy-start | bytes 24580
  52.1 31.1 %copy-start.3 = (s32[256,2]{0,1:T(2,128)S(1)}, s32[256,2]{0,1:T(2,128)}, u32[]{:S(2)}) copy-start(s32[256,2]{0,1:T(2,128)} %param.28) | copy-start | bytes 6148
  52.1 8.9 %collective-permute-start.1 = (bf16[8,256,128]{2,1,0:T(8,128)(2,1)S(1)}, bf16[8,256,128]{2,1,0:T(8,128)(2,1)S(1)}, u32[]{:S(2)}, u32[]{:S(2)}) collective-permute-start(bf16[8,256,128]{2,1,0:T(8,128)(2,1)S(1)} %get-tuple-element.32), channel_id=1, source_target_pairs={{0,1},{1,0},{2,3},{3,2},{4,5},{5,4},{6,7},{7,6},{8,9},{9,8},{10,11... | collective-permute-start | bytes 1572872 | tf_op jit(solution)/shard_map/ppermute | solution.py:345
  81.3 41.0 %collective-permute-start.4 = (bf16[6144,128]{1,0:T(8,128)(2,1)S(1)}, bf16[6144,128]{1,0:T(8,128)(2,1)S(1)}, u32[]{:S(2)}, u32[]{:S(2)}) collective-permute-start(bf16[6144,128]{1,0:T(8,128)(2,1)S(1)} %collective-permute-done.2.w2), channel_id=1, source_target_pairs={{2,0},{4,2},{6,4},{8,6},{10,8},{12,10},{14,12},{0,14},{15,1},{1,3}... | collective-permute-start | bytes 4718600 | tf_op jit(solution)/shard_map/ppermute | solution.py:429
  83.2 39.0 %copy-start = (bf16[6144,128]{1,0:T(8,128)(2,1)S(1)}, bf16[6144,128]{1,0:T(8,128)(2,1)}, u32[]{:S(2)}) copy-start(bf16[6144,128]{1,0:T(8,128)(2,1)} %shard_map.156.w0) | copy-start | bytes 4718596
  117.4 4.9 %collective-permute-start.3 = (bf16[32,8,8,128]{3,2,1,0:T(8,128)(2,1)S(1)}, bf16[32,8,8,128]{3,2,1,0:T(8,128)(2,1)S(1)}, u32[]{:S(2)}, u32[]{:S(2)}) collective-permute-start(bf16[32,8,8,128]{3,2,1,0:T(8,128)(2,1)S(1)} %bitcast.14), channel_id=1, source_target_pairs={{0,1},{1,0},{2,3},{3,2},{4,5},{5,4},{6,7},{7,6},{8,9},{9,8},{10,11... | collective-permute-start | bytes 1572872 | tf_op jit(solution)/shard_map/ppermute | solution.py:345
  125.7 38.7 %copy-start.4 = (f32[256,2]{0,1:T(2,128)S(1)}, f32[256,2]{0,1:T(2,128)}, u32[]{:S(2)}) copy-start(f32[256,2]{0,1:T(2,128)} %param.27) | copy-start | bytes 6148
  125.7 38.7 %copy-start.5 = (f32[256]{0:T(256)S(1)}, f32[256]{0:T(256)}, u32[]{:S(2)}) copy-start(f32[256]{0:T(256)} %param.26) | copy-start | bytes 3076
  125.7 3.8 %collective-permute-start.5 = (bf16[32,8,8,128]{3,2,1,0:T(8,128)(2,1)S(1)}, bf16[32,8,8,128]{3,2,1,0:T(8,128)(2,1)S(1)}, u32[]{:S(2)}, u32[]{:S(2)}) collective-permute-start(bf16[32,8,8,128]{3,2,1,0:T(8,128)(2,1)S(1)} %get-tuple-element.41), channel_id=1, source_target_pairs={{0,1},{1,0},{2,3},{3,2},{4,5},{5,4},{6,7},{7,6},{8,9},{9,8},{10,11... | collective-permute-start | bytes 1572872 | tf_op jit(solution)/shard_map/ppermute | solution.py:345
  184.7 6.1 %collective-permute-start.6 = (bf16[8,256,128]{2,1,0:T(8,128)(2,1)S(1)}, bf16[8,256,128]{2,1,0:T(8,128)(2,1)S(1)}, u32[]{:S(2)}, u32[]{:S(2)}) collective-permute-start(bf16[8,256,128]{2,1,0:T(8,128)(2,1)S(1)} %all_to_all.34.own_ref), channel_id=1, source_target_pairs={{0,1},{1,0},{2,3},{3,2},{4,5},{5,4},{6,7},{7,6},{8,9},{9,8},{10,11... | collective-permute-start | bytes 1572872 | tf_op jit(solution)/shard_map/ppermute | solution.py:345

commit v3 on v2

--- a/solution.py
+++ b/solution.py
@@ -17,10 +17,25 @@
 INTERPRET = False
 
 
-def mm(a, b, contract=((1,), (0,)), precision=lax.Precision.HIGHEST):
-    return lax.dot_general(
-        a, b, (contract, ((), ())), precision=precision, preferred_element_type=F32
-    )
+def dot(a, b, contract=((1,), (0,))):
+    return lax.dot_general(a, b, (contract, ((), ())), preferred_element_type=F32)
+
+
+def halves(a):
+    high = a.astype(BF16)
+    return high, (a - high.astype(F32)).astype(BF16)
+
+
+def mm(a, b, contract=((1,), (0,))):
+    (a_high, a_low), (b_high, b_low) = halves(a), halves(b)
+    return dot(a_high, b_high, contract) + (
+        dot(a_high, b_low, contract) + dot(a_low, b_high, contract)
+    )
+
+
+def mm_exact(a, b, contract=((1,), (0,))):
+    high, low = halves(a)
+    return dot(high, b, contract) + dot(low, b, contract)
 
 
 def iota(shape, dim):
@@ -43,7 +58,7 @@
 
 
 def same_head_ones():
-    return (iota((W, W), 0) // SEG == iota((W, W), 1) // SEG).astype(F32)
+    return (iota((W, W), 0) // SEG == iota((W, W), 1) // SEG).astype(F32).astype(BF16)
 
 
 def pack_kernel(switch_ref, expansion_ref, contraction_ref, out_ref, sems):
@@ -91,11 +106,13 @@
     rate = 1.0 / (1.0 + jnp.exp(-s_ref[...].astype(F32)))
     bias = jnp.where(iota((rows, W), 1) < SEG, bias_columns[:, 0:1], bias_columns[:, 1:2])
     decay = bias - DECAY / (1.0 + jnp.exp(-f_ref[...]))
-    removal = key * lax.rsqrt(mm(key * key, same_head_ones()) + 1e-06)
+    removal = key * lax.rsqrt(mm_exact(key * key, same_head_ones()) + 1e-06)
     beta = removal * rate
     row, col = iota((rows, rows), 0), iota((rows, rows), 1)
-    below = ((row // SEG == col // SEG) & (row >= col)).astype(F32)
-    total = mm(below, decay)
+    below = ((row // SEG == col // SEG) & (row >= col)).astype(F32).astype(BF16)
+    high, low = halves(decay)
+    rest = (decay - high.astype(F32) - low.astype(F32)).astype(BF16)
+    total = dot(below, high) + (dot(below, low) + dot(below, rest))
 
     row, col = iota((W, W), 0), iota((W, W), 1)
     same = row // SEG == col // SEG
@@ -183,6 +200,10 @@
     return stack_heads(pair[:SEG]), stack_heads(pair[SEG:])
 
 
+def times(state, change):
+    return state + mm_exact(state, change.astype(BF16))
+
+
 def compose_kernel(pos_ref, got_ref, pair_ref, prefix_ref):
     mine = pos_ref[0]
     eye = eye128()
@@ -191,7 +212,7 @@
     prefix = jnp.where(mine > 0, run, jnp.concatenate([eye, jnp.zeros((W, W), F32)], axis=0))
     for n in range(1, got_ref.shape[0]):
         change, add = unpack(got_ref[n])
-        run = run + mm(run, change)
+        run = times(run, change)
         run = jnp.concatenate([run[:W], run[W:] + add], axis=0)
         prefix = jnp.where(n < mine, run, prefix)
     pair = jnp.concatenate([flat_heads(run[:W] - eye), flat_heads(run[W:])], axis=0).astype(BF16)
@@ -205,12 +226,12 @@
     state = jnp.where(mine > 0, unpack(got_ref[0])[1], 0.0)
     for n in range(1, got_ref.shape[0] - 1):
         change, add = unpack(got_ref[n])
-        state = jnp.where(n < mine, state + mm(state, change) + add, state)
+        state = jnp.where(n < mine, times(state, change) + add, state)
     state = mm(state, prefix_ref[:W]) + prefix_ref[W:]
     out = loc_ref[...] + mm(map_ref[...], state, ((1,), (1,)))
     ones = same_head_ones()
-    centered = out - mm(out, ones) * (1.0 / SEG)
-    spread = mm(centered * centered, ones) * (1.0 / SEG)
+    centered = out - mm_exact(out, ones) * (1.0 / SEG)
+    spread = mm_exact(centered * centered, ones) * (1.0 / SEG)
     mixed = (centered * lax.rsqrt(spread + 0.00064) * gain_ref[...]).astype(BF16)
     for n in range(keep_ref.shape[0]):
         part = jnp.dot(mixed, w_ref[:, n * 2 * W : (n + 1) * 2 * W], preferred_element_type=F32)
@@ -219,33 +240,37 @@
         send_ref[n] = jnp.where(core == 0, second, first).astype(BF16)
 
 
-def slots_of(ids_ref, experts, capacity):
-    tokens = ids_ref.shape[1]
-    named = columns_of(ids_ref[...].astype(F32)).astype(jnp.int32)
-    names = [named[:, k : k + 1] for k in range(2)]
-    hot = [(iota((tokens, experts), 1) == name).astype(F32) for name in names]
-    earlier = (iota((tokens, tokens), 0) > iota((tokens, tokens), 1)).astype(BF16)
-    ahead = jnp.dot(earlier, (hot[0] + hot[1]).astype(BF16), preferred_element_type=F32)
+def route_kernel(table_ref, hot_ref, high_ref, low_ref):
+    experts, capacity = 32, 32
+    tokens, places = table_ref.shape[1], hot_ref.shape[0]
+    names = [table_ref[k : k + 1, :] for k in range(2)]
+    hot = [(iota((experts, tokens), 0).astype(F32) == name).astype(F32) for name in names]
+    earlier = (iota((tokens, tokens), 0) < iota((tokens, tokens), 1)).astype(F32).astype(BF16)
+    ahead = dot((hot[0] + hot[1]).astype(BF16), earlier)
     ranks = [
-        jnp.sum(hot[0] * ahead, axis=1, keepdims=True),
-        jnp.sum(hot[1] * (ahead + hot[0]), axis=1, keepdims=True),
+        jnp.sum(hot[0] * ahead, axis=0, keepdims=True),
+        jnp.sum(hot[1] * (ahead + hot[0]), axis=0, keepdims=True),
     ]
-    return [name * capacity + rank.astype(jnp.int32) for name, rank in zip(names, ranks)]
-
-
-def dispatch_kernel(pos_ref, parts_ref, skip_ref, gain_ref, ids_ref, hid_ref, out_ref):
+    slots = [name * capacity + rank for name, rank in zip(names, ranks)]
+    place = iota((places, tokens), 0).astype(F32)
+    hot_ref[...] = ((place == slots[0]) | (place == slots[1])).astype(F32).astype(BF16)
+    shares = columns_of(table_ref[2:4, :])
+    found = columns_of(jnp.concatenate(slots, axis=0))
+    place = iota((tokens, places), 1).astype(F32)
+    weight = jnp.zeros((tokens, places), F32)
+    for k in range(2):
+        weight = weight + jnp.where(place == found[:, k : k + 1], shares[:, k : k + 1], 0.0)
+    high_ref[...], low_ref[...] = halves(weight)
+
+
+def dispatch_kernel(pos_ref, parts_ref, skip_ref, gain_ref, hot_ref, hid_ref, out_ref):
     hidden = skip_ref[...].astype(F32)
     for n in range(parts_ref.shape[0]):
         hidden = hidden + parts_ref[n].astype(F32)
     hid_ref[...] = hidden
     column = pl.multiple_of((pos_ref[2] * 2 + pos_ref[3]) * W, W)
     scaled = (hidden * gain_ref[:, pl.ds(column, W)]).astype(BF16)
-    tokens, places = ids_ref.shape[1], out_ref.shape[0] * out_ref.shape[1] // 2
-    first, second = slots_of(ids_ref, 32, 32)
-    lane = iota((tokens, places), 1)
-    hot = ((lane == first) | (lane == second)).astype(F32).astype(BF16)
-    rows = lax.dot_general(hot, scaled, (((0,), (0,)), ((), ())), preferred_element_type=F32)
-    rows = rows.astype(BF16).reshape(32, 32, W)
+    rows = dot(hot_ref[...], scaled).astype(BF16).reshape(32, 32, W)
     out_ref[:, :32, :] = rows
     out_ref[:, 32:, :] = rows
 
@@ -287,31 +312,52 @@
         send_ref[:, n] = send.astype(BF16)
 
 
-def combine_kernel(ret_ref, hid_ref, ids_ref, chance_ref, within_ref, out_ref):
+def combine_kernel(ret_ref, hid_ref, high_ref, low_ref, out_ref):
     half = ret_ref.shape[1] // 2
     rows = ret_ref[:, :half].astype(F32) + ret_ref[:, half:].astype(F32)
     rows = rows.reshape(-1, W).astype(BF16)
-    tokens, places = ids_ref.shape[1], rows.shape[0]
-    slots = slots_of(ids_ref, 32, 32)
-    lane = iota((tokens, places), 1)
-    within = within_ref[...]
-    shares = columns_of(chance_ref[...] * within / jnp.sum(within, axis=0, keepdims=True))
-    result = hid_ref[...]
-    for k in range(2):
-        hot = (lane == slots[k]).astype(F32).astype(BF16)
-        picked = jnp.dot(hot, rows, preferred_element_type=F32)
-        result = result + picked * shares[:, k : k + 1]
+    result = hid_ref[...] + (dot(high_ref[...], rows) + dot(low_ref[...], rows))
     result = result.astype(BF16)
     for n in range(out_ref.shape[0]):
         out_ref[n] = result
 
 
-def assemble_kernel(pos_ref, own_ref, other_ref, out_ref):
-    core = pos_ref[3]
-    for n in range(own_ref.shape[0]):
-        own, other = own_ref[n], other_ref[n]
-        out_ref[:, 2 * n * W : (2 * n + 1) * W] = jnp.where(core == 0, own, other)
-        out_ref[:, (2 * n + 1) * W : (2 * n + 2) * W] = jnp.where(core == 0, other, own)
+def columns_out(first, blocks_ref, out_ref, sems):
+    copies = []
+    for n in range(blocks_ref.shape[0]):
+        column = pl.multiple_of((2 * n + first) * W, W)
+        copies.append(
+            pltpu.make_async_copy(blocks_ref.at[n], out_ref.at[:, pl.ds(column, W)], sems.at[n])
+        )
+    for copy in copies:
+        copy.start()
+    for copy in copies:
+        copy.wait()
+
+
+def own_out_kernel(pos_ref, own_ref, out_ref, sems):
+    columns_out(pos_ref[3], own_ref, out_ref, sems)
+
+
+def other_out_kernel(pos_ref, other_ref, half_ref, out_ref, sems):
+    columns_out(1 - pos_ref[3], other_ref, out_ref, sems)
+
+
+def output_call(kernel, shape, pos, blocks, *half):
+    near = [pl.BlockSpec(memory_space=pltpu.SMEM), pl.BlockSpec(memory_space=pltpu.VMEM)]
+    return pl.pallas_call(
+        kernel,
+        out_shape=jax.ShapeDtypeStruct(shape, BF16),
+        in_specs=near + [pl.BlockSpec(memory_space=pl.ANY)] * len(half),
+        out_specs=pl.BlockSpec(memory_space=pl.ANY),
+        scratch_shapes=[pltpu.SemaphoreType.DMA((blocks.shape[0],))],
+        input_output_aliases={2: 0} if half else {},
+        compiler_params=pltpu.CompilerParams(vmem_limit_bytes=8 << 20),
+        cost_estimate=pl.CostEstimate(
+            flops=1_000_000_000, bytes_accessed=1_000_000, transcendentals=0
+        ),
+        interpret=INTERPRET,
+    )(pos, blocks, *half)
 
 
 def call(kernel, outs, *args, scalars=0, flops=2_000_000_000, far=(), scratch=(), grant=40 << 20):
@@ -403,7 +449,16 @@
     )
     own_skip = lax.dynamic_slice_in_dim(skip, (here[2] * 2 + here[3]) * W, W, 1)
     gathered = exchange(pairs, "x")
-    gathered, own_skip = lax.optimization_barrier((gathered, own_skip))
+    shares = within_chance.T
+    shares = cluster_chance[None] * shares / jnp.sum(shares, axis=0, keepdims=True)
+    hot, high, low = call(
+        route_kernel,
+        [((4 * tokens, tokens), BF16)] + [((tokens, 4 * tokens), BF16)] * 2,
+        jnp.concatenate([ids.T.astype(F32), shares], axis=0),
+    )
+    gathered, own_skip, hot, high, low = lax.optimization_barrier(
+        (gathered, own_skip, hot, high, low)
+    )
     pairs, prefix = call(
         compose_kernel, [((n_z, W, W), BF16), ((2 * W, W), F32)], pos, gathered, scalars=1
     )
@@ -434,7 +489,7 @@
         parts,
         own_skip,
         norm_gain[None],
-        ids.T,
+        hot,
         scalars=1,
     )
     own = exchange(outgoing.reshape(n_z * n_x * n_y, 8, W), ("z", "x", "y"))
@@ -452,17 +507,11 @@
     summed = (keep.astype(F32) + swap_cores(send).astype(F32)).astype(BF16)
     returned = exchange(summed.reshape(n_z * n_x * n_y, 8, W), ("z", "x", "y"))
     returned = returned.reshape(n_z * n_x, n_y, 8, W)
-    copies = call(
-        combine_kernel,
-        [((n_y, tokens, W), BF16)],
-        returned,
-        hidden,
-        ids.T,
-        cluster_chance[None],
-        within_chance.T,
-    )
+    copies = call(combine_kernel, [((n_y, tokens, W), BF16)], returned, hidden, high, low)
     own = exchange(copies, "y")
-    return call(assemble_kernel, [((tokens, width), BF16)], pos, own, swap_cores(own), scalars=1)
+    other = swap_cores(own)
+    half = output_call(own_out_kernel, (tokens, width), pos, own)
+    return output_call(other_out_kernel, (tokens, width), pos, other, half)
 
 
 def solution(mesh):

time: 193 us -> 191 us (0.990)
  Pallas kernels: 24.5 us -> 20.8 us
  other arithmetic: 0.4 us -> 2.49 us
    pallas_call x8, Pallas kernels: 24.5 us -> 18 us  [call(): pl.pallas_call(kernel, out_shape=shapes if len(shapes) > 1 else shapes[0]...]
    ppermute x3, waiting for transfers between devices: 0.6 us -> 3.72 us  [body(): weights.append(lax.ppermute(weights[-1], TP, ring))]
    all_to_all x1, waiting for transfers between devices: 3.89 us -> 0.94 us  [exchange(): return lax.all_to_all(parts, axes, split_axis=0, concat_axis=0, tiled=True)]
    pallas_call x0 -> x2, Pallas kernels: none -> 2.78 us  [output_call(): pl.pallas_call(kernel, out_shape=jax.ShapeDtypeStruct(shape, BF16), in_sp...]
  transfers between devices with their start and end apart: 8 -> 8, of which waited for: 6 -> 6; matrix products, arithmetic and copies ran while one was open for 1% -> 2% of each run, Pallas kernels for 8% -> 7%
where the time goes in v3:
time: 191 us
  blocking collectives  126 us (66%)
  starting transfers between devices  30.8 us (16%)
  Pallas kernels  20.8 us (11%)
  waiting for transfers between devices  9.14 us (5%)
  other arithmetic  2.49 us (1%)
    all_to_all x5, blocking collectives, exchange(): return lax.all_to_all(parts, axes, split_axis=0, concat_axis=0, tiled=True)  126 us
    ppermute x4, starting transfers between devices, swap_cores(): return lax.ppermute(data, 'c', [(0, 1), (1, 0)])  18.9 us
    pallas_call x8, Pallas kernels, call(): pl.pallas_call(kernel, out_shape=shapes if len(shapes) > 1 else shapes[0]...  18 us
    ppermute x3, starting transfers between devices, body(): weights.append(lax.ppermute(weights[-1], TP, ring))  7.84 us
    ppermute x4, waiting for transfers between devices, swap_cores(): return lax.ppermute(data, 'c', [(0, 1), (1, 0)])  4.48 us
    all_to_all x1, starting transfers between devices, exchange(): return lax.all_to_all(parts, axes, split_axis=0, concat_axis=0, tiled=True)  4.02 us
  transfers between devices with their start and end apart: 8, of which 6 were waited for; matrix products, arithmetic and copies ran while one was open for 2% of the time, Pallas kernels for 7%

profile of v3, /device:TPU:1, one launch (start us, length us, event | category | flops | bytes accessed | tf_op | source)
XLA Modules:
  0.0 190.6 jit_solution(12293236570879567937)
XLA Ops:
  0.0 2.6 %shard_map.157.w0 = bf16[6144,128]{1,0:T(8,128)(2,1)} custom-call(bf16[1,2048,128]{2,1,0:T(8,128)(2,1)} %switch_ref.1, bf16[1,2048,128]{2,1,0:T(8,128)(2,1)} %expansion_ref.1, bf16[1,128,2048]{2,1,0:T(8,128)(2,1)} %contraction_ref.1), custom_call_target="tpu_custom_call" | custom-call | flops 2000000000 | bytes 1000000 | tf_op jit(solution)/shard_map/pallas_call | solution.py:371
  2.6 4.0 %collective-permute-start = (bf16[6144,128]{1,0:T(8,128)(2,1)}, bf16[6144,128]{1,0:T(8,128)(2,1)}, u32[]{:S(2)}, u32[]{:S(2)}) collective-permute-start(bf16[6144,128]{1,0:T(8,128)(2,1)} %shard_map.157.w0), channel_id=1, source_target_pairs={{2,0},{4,2},{6,4},{8,6},{10,8},{12,10},{14,12},{0,14},{15,1},{1,3}... | collective-permute-start | bytes 4718600 | tf_op jit(solution)/shard_map/ppermute | solution.py:431
  6.6 6.4 %shard_map.154 = (bf16[4,128,128]{2,1,0:T(8,128)(2,1)}, f32[256,128]{1,0:T(8,128)}, f32[256,128]{1,0:T(8,128)}) custom-call(bf16[256,128]{1,0:T(8,128)(2,1)} %refs_0_.1, bf16[256,128]{1,0:T(8,128)(2,1)} %refs_1_.1, bf16[256,128]{1,0:T(8,128)(2,1)} %refs_2_.1, bf16[256,128]{1,0:T(8,128)(2,1)} %refs_3_.1, f32[256,128]{1,0:T(8,128)} %refs_4_.1, f32[2,256]{1,0:T(2,128)} %bitcast.23), custom_call_target="tpu_custom_call" | custom-call | flops 2000000000 | bytes 1000000 | tf_op jit(solution)/shard_map/pallas_call | solution.py:371
  13.0 4.0 %all-to-all-start = ((bf16[4,128,128]{2,1,0:T(8,128)(2,1)}), bf16[4,128,128]{2,1,0:T(8,128)(2,1)S(1)}, u32[]{:S(2)}, u32[]{:S(2)}) async-start(bf16[4,128,128]{2,1,0:T(8,128)(2,1)} %get-tuple-element.30), calls=%async_computation | async-start | bytes 262144 | tf_op jit(solution)/shard_map/all_to_all | solution.py:387
  17.1 0.7 reduce_sum.9
  17.7 0.7 convert_bitcast_fusion
  18.4 0.7 divide_bitcast_fusion
  19.1 0.9 constant_dynamic-slice_fusion.skip_ref
  20.0 0.9 shard_map.155
  20.9 0.9 all-to-all-done.got_ref
  21.9 1.0 shard_map.156
  22.9 3.7 %collective-permute-done.w1 = bf16[6144,128]{1,0:T(8,128)(2,1)} collective-permute-done((bf16[6144,128]{1,0:T(8,128)(2,1)}, bf16[6144,128]{1,0:T(8,128)(2,1)}, u32[]{:S(2)}, u32[]{:S(2)}) %collective-permute-start) | collective-permute-done | bytes 1572896 | tf_op jit(solution)/shard_map/ppermute | solution.py:431
  26.7 1.9 %collective-permute-start.2 = (bf16[6144,128]{1,0:T(8,128)(2,1)}, bf16[6144,128]{1,0:T(8,128)(2,1)S(1)}, u32[]{:S(2)}, u32[]{:S(2)}) collective-permute-start(bf16[6144,128]{1,0:T(8,128)(2,1)} %collective-permute-done.w1), channel_id=1, source_target_pairs={{2,0},{4,2},{6,4},{8,6},{10,8},{12,10},{14,12},{0,14},{15,1},{1,3}... | collective-permute-start | bytes 4718600 | tf_op jit(solution)/shard_map/ppermute | solution.py:466
  28.6 19.1 %all_to_all.30.got_ref = bf16[8,128,128]{2,1,0:T(8,128)(2,1)S(1)} all-to-all(bf16[8,128,128]{2,1,0:T(8,128)(2,1)S(1)} %get-tuple-element.36), channel_id=1, replica_groups=mesh['z'=8,'x'=4,'y'=8,'c'=2] {'z'}, dimensions={0} | all-to-all | bytes 524288 | tf_op jit(solution)/shard_map/all_to_all | solution.py:387
  47.7 2.5 %shard_map.158 = (bf16[8,256,128]{2,1,0:T(8,128)(2,1)S(1)}, bf16[8,256,128]{2,1,0:T(8,128)(2,1)S(1)}) custom-call(s32[4]{0:T(128)S(1)} %pad_add_fusion.pos_ref, bf16[8,128,128]{2,1,0:T(8,128)(2,1)S(1)} %all_to_all.30.got_ref, f32[256,128]{1,0:T(8,128)S(1)} %get-tuple-element.37.prefix_ref, f32[256,128]{1,0:T(8,128)S(1)} %copy-done.4, ...), custom_call_target="tpu_custom_call" | custom-call | flops 2000000000 | bytes 1000000 | tf_op jit(solution)/shard_map/pallas_call | solution.py:371
  50.2 8.1 %collective-permute-start.1 = (bf16[8,256,128]{2,1,0:T(8,128)(2,1)S(1)}, bf16[8,256,128]{2,1,0:T(8,128)(2,1)S(1)}, u32[]{:S(2)}, u32[]{:S(2)}) collective-permute-start(bf16[8,256,128]{2,1,0:T(8,128)(2,1)S(1)} %get-tuple-element.41), channel_id=1, source_target_pairs={{0,1},{1,0},{2,3},{3,2},{4,5},{5,4},{6,7},{7,6},{8,9},{9,8},{10,11... | collective-permute-start | bytes 1572872 | tf_op jit(solution)/shard_map/ppermute | solution.py:391
  58.3 1.5 collective-permute-done.1
  60.0 20.4 %all_to_all.31.parts_ref = bf16[8,256,128]{2,1,0:T(8,128)(2,1)S(1)} all-to-all(bf16[8,256,128]{2,1,0:T(8,128)(2,1)S(1)} %add_convert_fusion.1), channel_id=1, replica_groups=mesh['z'=8,'x'=4,'y'=8,'c'=2] {'y'}, dimensions={0} | all-to-all | bytes 1048576 | tf_op jit(solution)/shard_map/all_to_all | solution.py:387
  80.4 1.9 %collective-permute-start.4 = (bf16[6144,128]{1,0:T(8,128)(2,1)S(1)}, bf16[6144,128]{1,0:T(8,128)(2,1)S(1)}, u32[]{:S(2)}, u32[]{:S(2)}) collective-permute-start(bf16[6144,128]{1,0:T(8,128)(2,1)S(1)} %collective-permute-done.2.w2), channel_id=1, source_target_pairs={{2,0},{4,2},{6,4},{8,6},{10,8},{12,10},{14,12},{0,14},{15,1},{1,3}... | collective-permute-start | bytes 4718600 | tf_op jit(solution)/shard_map/ppermute | solution.py:484
  82.4 0.9 shard_map.159
  83.3 32.9 %all_to_all.32 = bf16[256,8,128]{2,1,0:T(8,128)(2,1)S(1)} all-to-all(bf16[256,8,128]{2,1,0:T(8,128)(2,1)S(1)} %bitcast.17), channel_id=1, replica_groups=mesh['z'=8,'x'=4,'y'=8,'c'=2] {'z','x','y'}, dimensions={0} | all-to-all | bytes 1048576 | tf_op jit(solution)/shard_map/all_to_all | solution.py:387
  116.1 4.0 %collective-permute-start.3 = (bf16[32,8,8,128]{3,2,1,0:T(8,128)(2,1)S(1)}, bf16[32,8,8,128]{3,2,1,0:T(8,128)(2,1)S(1)}, u32[]{:S(2)}, u32[]{:S(2)}) collective-permute-start(bf16[32,8,8,128]{3,2,1,0:T(8,128)(2,1)S(1)} %bitcast.15), channel_id=1, source_target_pairs={{0,1},{1,0},{2,3},{3,2},{4,5},{5,4},{6,7},{7,6},{8,9},{9,8},{10,11... | collective-permute-start | bytes 1572872 | tf_op jit(solution)/shard_map/ppermute | solution.py:391
  120.1 1.3 collective-permute-done.3.other_ref
  121.5 3.3 %shard_map.160 = (bf16[32,8,8,128]{3,2,1,0:T(8,128)(2,1)S(1)}, bf16[32,8,8,128]{3,2,1,0:T(8,128)(2,1)S(1)}) custom-call(s32[4]{0:T(128)S(1)} %pad_add_fusion.pos_ref, bf16[32,8,8,128]{3,2,1,0:T(8,128)(2,1)S(1)} %bitcast.16, bf16[32,8,8,128]{3,2,1,0:T(8,128)(2,1)S(1)} %collective-permute-done.3.other_ref, f32[1,2048]{1,0:T(1,128)S(1)} %bitcast.20, ...), custom_call_target="tpu_custom_call" | custom-call | flops 2000000000 | bytes 1000000 | tf_op jit(solution)/shard_map/pallas_call | solution.py:371
  124.8 2.3 %collective-permute-start.5 = (bf16[32,8,8,128]{3,2,1,0:T(8,128)(2,1)S(1)}, bf16[32,8,8,128]{3,2,1,0:T(8,128)(2,1)S(1)}, u32[]{:S(2)}, u32[]{:S(2)}) collective-permute-start(bf16[32,8,8,128]{3,2,1,0:T(8,128)(2,1)S(1)} %get-tuple-element.51), channel_id=1, source_target_pairs={{0,1},{1,0},{2,3},{3,2},{4,5},{5,4},{6,7},{7,6},{8,9},{9,8},{10,11... | collective-permute-start | bytes 1572872 | tf_op jit(solution)/shard_map/ppermute | solution.py:391
  127.1 1.5 collective-permute-done.5
  128.8 34.6 %all_to_all.33 = bf16[256,8,128]{2,1,0:T(8,128)(2,1)S(1)} all-to-all(bf16[256,8,128]{2,1,0:T(8,128)(2,1)S(1)} %bitcast.22), channel_id=1, replica_groups=mesh['z'=8,'x'=4,'y'=8,'c'=2] {'z','x','y'}, dimensions={0} | all-to-all | bytes 1048576 | tf_op jit(solution)/shard_map/all_to_all | solution.py:387
  163.5 0.4 shard_map.161
  163.9 19.0 %all_to_all.34.own_ref = bf16[8,256,128]{2,1,0:T(8,128)(2,1)S(1)} all-to-all(bf16[8,256,128]{2,1,0:T(8,128)(2,1)S(1)} %shard_map.161), channel_id=1, replica_groups=mesh['z'=8,'x'=4,'y'=8,'c'=2] {'y'}, dimensions={0} | all-to-all | bytes 1048576 | tf_op jit(solution)/shard_map/all_to_all | solution.py:387
  182.9 4.6 %collective-permute-start.6 = (bf16[8,256,128]{2,1,0:T(8,128)(2,1)S(1)}, bf16[8,256,128]{2,1,0:T(8,128)(2,1)S(1)}, u32[]{:S(2)}, u32[]{:S(2)}) collective-permute-start(bf16[8,256,128]{2,1,0:T(8,128)(2,1)S(1)} %all_to_all.34.own_ref), channel_id=1, source_target_pairs={{0,1},{1,0},{2,3},{3,2},{4,5},{5,4},{6,7},{7,6},{8,9},{9,8},{10,11... | collective-permute-start | bytes 1572872 | tf_op jit(solution)/shard_map/ppermute | solution.py:391
  187.5 1.4 shard_map.162.half_ref
  189.0 1.4 shard_map.163
  (19 shorter events, 0.6 us)
Async XLA Ops:
  2.6 24.1 %collective-permute-start = (bf16[6144,128]{1,0:T(8,128)(2,1)}, bf16[6144,128]{1,0:T(8,128)(2,1)}, u32[]{:S(2)}, u32[]{:S(2)}) collective-permute-start(bf16[6144,128]{1,0:T(8,128)(2,1)} %shard_map.157.w0), channel_id=1, source_target_pairs={{2,0},{4,2},{6,4},{8,6},{10,8},{12,10},{14,12},{0,14},{15,1},{1,3}... | collective-permute-start | bytes 4718600 | tf_op jit(solution)/shard_map/ppermute | solution.py:431
  13.0 8.8 %all-to-all-start = ((bf16[4,128,128]{2,1,0:T(8,128)(2,1)}), bf16[4,128,128]{2,1,0:T(8,128)(2,1)S(1)}, u32[]{:S(2)}, u32[]{:S(2)}) async-start(bf16[4,128,128]{2,1,0:T(8,128)(2,1)} %get-tuple-element.30), calls=%async_computation | async-start | bytes 262144 | tf_op jit(solution)/shard_map/all_to_all | solution.py:387
  21.9 25.8 %copy-start.1 = (bf16[128,2048]{1,0:T(8,128)(2,1)S(1)}, bf16[128,2048]{1,0:T(8,128)(2,1)}, u32[]{:S(2)}) copy-start(bf16[128,2048]{1,0:T(8,128)(2,1)} %w_ref.1) | copy-start | bytes 1572868
  21.9 25.8 %copy-start.3 = (f32[128]{0:T(128)S(1)}, f32[128]{0:T(128)}, u32[]{:S(2)}) copy-start(f32[128]{0:T(128)} %param.22) | copy-start | bytes 1540
  21.9 25.8 %copy-start.4 = (f32[256,128]{1,0:T(8,128)S(1)}, f32[256,128]{1,0:T(8,128)}, u32[]{:S(2)}) copy-start(f32[256,128]{1,0:T(8,128)} %get-tuple-element.38.map_ref) | copy-start | bytes 393220
  21.9 25.8 %copy-start.5 = (f32[256,128]{1,0:T(8,128)S(1)}, f32[256,128]{1,0:T(8,128)}, u32[]{:S(2)}) copy-start(f32[256,128]{1,0:T(8,128)} %get-tuple-element.39.loc_ref) | copy-start | bytes 393220
  26.7 33.4 %collective-permute-start.2 = (bf16[6144,128]{1,0:T(8,128)(2,1)}, bf16[6144,128]{1,0:T(8,128)(2,1)S(1)}, u32[]{:S(2)}, u32[]{:S(2)}) collective-permute-start(bf16[6144,128]{1,0:T(8,128)(2,1)} %collective-permute-done.w1), channel_id=1, source_target_pairs={{2,0},{4,2},{6,4},{8,6},{10,8},{12,10},{14,12},{0,14},{15,1},{1,3}... | collective-permute-start | bytes 4718600 | tf_op jit(solution)/shard_map/ppermute | solution.py:466
  50.2 32.1 %copy-start.2 = (f32[2048]{0:T(1024)S(1)}, f32[2048]{0:T(1024)}, u32[]{:S(2)}) copy-start(f32[2048]{0:T(1024)} %param.25) | copy-start | bytes 24580
  50.2 9.6 %collective-permute-start.1 = (bf16[8,256,128]{2,1,0:T(8,128)(2,1)S(1)}, bf16[8,256,128]{2,1,0:T(8,128)(2,1)S(1)}, u32[]{:S(2)}, u32[]{:S(2)}) collective-permute-start(bf16[8,256,128]{2,1,0:T(8,128)(2,1)S(1)} %get-tuple-element.41), channel_id=1, source_target_pairs={{0,1},{1,0},{2,3},{3,2},{4,5},{5,4},{6,7},{7,6},{8,9},{9,8},{10,11... | collective-permute-start | bytes 1572872 | tf_op jit(solution)/shard_map/ppermute | solution.py:391
  80.4 41.0 %collective-permute-start.4 = (bf16[6144,128]{1,0:T(8,128)(2,1)S(1)}, bf16[6144,128]{1,0:T(8,128)(2,1)S(1)}, u32[]{:S(2)}, u32[]{:S(2)}) collective-permute-start(bf16[6144,128]{1,0:T(8,128)(2,1)S(1)} %collective-permute-done.2.w2), channel_id=1, source_target_pairs={{2,0},{4,2},{6,4},{8,6},{10,8},{12,10},{14,12},{0,14},{15,1},{1,3}... | collective-permute-start | bytes 4718600 | tf_op jit(solution)/shard_map/ppermute | solution.py:484
  82.4 39.1 %copy-start = (bf16[6144,128]{1,0:T(8,128)(2,1)S(1)}, bf16[6144,128]{1,0:T(8,128)(2,1)}, u32[]{:S(2)}) copy-start(bf16[6144,128]{1,0:T(8,128)(2,1)} %shard_map.157.w0) | copy-start | bytes 4718596
  116.1 5.3 %collective-permute-start.3 = (bf16[32,8,8,128]{3,2,1,0:T(8,128)(2,1)S(1)}, bf16[32,8,8,128]{3,2,1,0:T(8,128)(2,1)S(1)}, u32[]{:S(2)}, u32[]{:S(2)}) collective-permute-start(bf16[32,8,8,128]{3,2,1,0:T(8,128)(2,1)S(1)} %bitcast.15), channel_id=1, source_target_pairs={{0,1},{1,0},{2,3},{3,2},{4,5},{5,4},{6,7},{7,6},{8,9},{9,8},{10,11... | collective-permute-start | bytes 1572872 | tf_op jit(solution)/shard_map/ppermute | solution.py:391
  124.8 3.8 %collective-permute-start.5 = (bf16[32,8,8,128]{3,2,1,0:T(8,128)(2,1)S(1)}, bf16[32,8,8,128]{3,2,1,0:T(8,128)(2,1)S(1)}, u32[]{:S(2)}, u32[]{:S(2)}) collective-permute-start(bf16[32,8,8,128]{3,2,1,0:T(8,128)(2,1)S(1)} %get-tuple-element.51), channel_id=1, source_target_pairs={{0,1},{1,0},{2,3},{3,2},{4,5},{5,4},{6,7},{7,6},{8,9},{9,8},{10,11... | collective-permute-start | bytes 1572872 | tf_op jit(solution)/shard_map/ppermute | solution.py:391
  182.9 6.1 %collective-permute-start.6 = (bf16[8,256,128]{2,1,0:T(8,128)(2,1)S(1)}, bf16[8,256,128]{2,1,0:T(8,128)(2,1)S(1)}, u32[]{:S(2)}, u32[]{:S(2)}) collective-permute-start(bf16[8,256,128]{2,1,0:T(8,128)(2,1)S(1)} %all_to_all.34.own_ref), channel_id=1, source_target_pairs={{0,1},{1,0},{2,3},{3,2},{4,5},{5,4},{6,7},{7,6},{8,9},{9,8},{10,11... | collective-permute-start | bytes 1572872 | tf_op jit(solution)/shard_map/ppermute | solution.py:391

commit v4 on v3

--- a/solution.py
+++ b/solution.py
@@ -240,22 +240,28 @@
         send_ref[n] = jnp.where(core == 0, second, first).astype(BF16)
 
 
-def route_kernel(table_ref, hot_ref, high_ref, low_ref):
+def route_kernel(names_ref, hot_ref, slots_ref):
     experts, capacity = 32, 32
-    tokens, places = table_ref.shape[1], hot_ref.shape[0]
-    names = [table_ref[k : k + 1, :] for k in range(2)]
-    hot = [(iota((experts, tokens), 0).astype(F32) == name).astype(F32) for name in names]
+    tokens, places = names_ref.shape[1], hot_ref.shape[0]
+    names = [names_ref[k : k + 1, :] for k in range(2)]
+    hot = [(iota((experts, tokens), 0) == name).astype(F32) for name in names]
     earlier = (iota((tokens, tokens), 0) < iota((tokens, tokens), 1)).astype(F32).astype(BF16)
     ahead = dot((hot[0] + hot[1]).astype(BF16), earlier)
     ranks = [
         jnp.sum(hot[0] * ahead, axis=0, keepdims=True),
         jnp.sum(hot[1] * (ahead + hot[0]), axis=0, keepdims=True),
     ]
-    slots = [name * capacity + rank for name, rank in zip(names, ranks)]
+    slots = [(name * capacity).astype(F32) + rank for name, rank in zip(names, ranks)]
     place = iota((places, tokens), 0).astype(F32)
     hot_ref[...] = ((place == slots[0]) | (place == slots[1])).astype(F32).astype(BF16)
-    shares = columns_of(table_ref[2:4, :])
-    found = columns_of(jnp.concatenate(slots, axis=0))
+    slots_ref[...] = jnp.concatenate(slots, axis=0)
+
+
+def weigh_kernel(slots_ref, chance_ref, within_ref, high_ref, low_ref):
+    tokens, places = high_ref.shape
+    within = within_ref[...]
+    shares = columns_of(chance_ref[...] * within / jnp.sum(within, axis=0, keepdims=True))
+    found = columns_of(slots_ref[...])
     place = iota((tokens, places), 1).astype(F32)
     weight = jnp.zeros((tokens, places), F32)
     for k in range(2):
@@ -264,11 +270,11 @@
 
 
 def dispatch_kernel(pos_ref, parts_ref, skip_ref, gain_ref, hot_ref, hid_ref, out_ref):
+    column = pl.multiple_of((pos_ref[2] * 2 + pos_ref[3]) * W, W)
     hidden = skip_ref[...].astype(F32)
     for n in range(parts_ref.shape[0]):
         hidden = hidden + parts_ref[n].astype(F32)
     hid_ref[...] = hidden
-    column = pl.multiple_of((pos_ref[2] * 2 + pos_ref[3]) * W, W)
     scaled = (hidden * gain_ref[:, pl.ds(column, W)]).astype(BF16)
     rows = dot(hot_ref[...], scaled).astype(BF16).reshape(32, 32, W)
     out_ref[:, :32, :] = rows
@@ -416,6 +422,7 @@
 
     ring = [(((y + 1) % n_y) * 2, y * 2) for y in range(n_y)]
     ring += [(((y - 1) % n_y) * 2 + 1, y * 2 + 1) for y in range(n_y)]
+    back = [(target, source) for source, target in ring]
     weights = [
         call(
             pack_kernel,
@@ -447,23 +454,13 @@
         ],
         grant=67043328,
     )
-    own_skip = lax.dynamic_slice_in_dim(skip, (here[2] * 2 + here[3]) * W, W, 1)
     gathered = exchange(pairs, "x")
-    shares = within_chance.T
-    shares = cluster_chance[None] * shares / jnp.sum(shares, axis=0, keepdims=True)
-    hot, high, low = call(
-        route_kernel,
-        [((4 * tokens, tokens), BF16)] + [((tokens, 4 * tokens), BF16)] * 2,
-        jnp.concatenate([ids.T.astype(F32), shares], axis=0),
-    )
-    gathered, own_skip, hot, high, low = lax.optimization_barrier(
-        (gathered, own_skip, hot, high, low)
-    )
+    weights.append(lax.ppermute(weights[0], TP, back))
+    hot, slots = call(route_kernel, [((4 * tokens, tokens), BF16), ((2, tokens), F32)], ids.T)
+    gathered, hot = lax.optimization_barrier((gathered, hot))
     pairs, prefix = call(
         compose_kernel, [((n_z, W, W), BF16), ((2 * W, W), F32)], pos, gathered, scalars=1
     )
-    pairs, weights[1] = lax.optimization_barrier((pairs, weights[1]))
-    weights.append(lax.ppermute(weights[-1], TP, ring))
     gathered = exchange(pairs, "z")
     keep, send = call(
         readout_kernel,
@@ -477,11 +474,13 @@
         blender,
         scalars=1,
     )
-    branch = (keep.astype(F32) + swap_cores(send).astype(F32)).astype(BF16)
-    branch, weights[2] = lax.optimization_barrier((branch, weights[2]))
+    own_skip = lax.dynamic_slice_in_dim(skip, (here[2] * 2 + here[3]) * W, W, 1)
+    send, own_skip = lax.optimization_barrier((swap_cores(send), own_skip))
+    branch = (keep.astype(F32) + send.astype(F32)).astype(BF16)
+    branch, weights[1], weights[2] = lax.optimization_barrier((branch, weights[1], weights[2]))
     parts = exchange(branch, "y")
-    parts, weights[2] = lax.optimization_barrier((parts, weights[2]))
-    weights.append(lax.ppermute(weights[-1], TP, ring))
+    parts, weights[1] = lax.optimization_barrier((parts, weights[1]))
+    weights.append(lax.ppermute(weights[1], TP, ring))
     hidden, outgoing = call(
         dispatch_kernel,
         [((tokens, W), F32), ((n_z * n_x, 64, W), BF16)],
@@ -504,7 +503,15 @@
         *weights,
         scalars=1,
     )
-    summed = (keep.astype(F32) + swap_cores(send).astype(F32)).astype(BF16)
+    high, low = call(
+        weigh_kernel,
+        [((tokens, 4 * tokens), BF16)] * 2,
+        slots,
+        cluster_chance[None],
+        within_chance.T,
+    )
+    send, high, low = lax.optimization_barrier((swap_cores(send), high, low))
+    summed = (keep.astype(F32) + send.astype(F32)).astype(BF16)
     returned = exchange(summed.reshape(n_z * n_x * n_y, 8, W), ("z", "x", "y"))
     returned = returned.reshape(n_z * n_x, n_y, 8, W)
     copies = call(combine_kernel, [((n_y, tokens, W), BF16)], returned, hidden, high, low)

time: 191 us -> 189 us (0.990)
  waiting for transfers between devices: 9.14 us -> 6.73 us
  other arithmetic: 2.49 us -> 0.4 us
  blocking collectives: 126 us -> 128 us
    ppermute x0 -> x2, starting transfers between devices: none -> 5.72 us  [the longest x1 3.81 us: body(): weights.append(lax.ppermute(weights[0], TP, back))]
    ppermute x3 -> x1, starting transfers between devices: 7.84 us -> 4.02 us  [body(): weights.append(lax.ppermute(weights[-1], TP, ring))]
    ppermute x3 -> x1, waiting for transfers between devices: 3.72 us -> 0.01 us  [body(): weights.append(lax.ppermute(weights[-1], TP, ring))]
    ppermute x4, starting transfers between devices: 18.9 us -> 16.1 us  [swap_cores(): return lax.ppermute(data, 'c', [(0, 1), (1, 0)])]
    all_to_all x1, waiting for transfers between devices: 0.94 us -> 3.68 us  [exchange(): return lax.all_to_all(parts, axes, split_axis=0, concat_axis=0, tiled=True)]
    all_to_all x5, blocking collectives: 126 us -> 128 us  [exchange(): return lax.all_to_all(parts, axes, split_axis=0, concat_axis=0, tiled=True)]
    pallas_call x8 -> x9, Pallas kernels: 18 us -> 18.6 us  [call(): pl.pallas_call(kernel, out_shape=shapes if len(shapes) > 1 else shapes[0]...]
  transfers between devices with their start and end apart: 8 -> 8, of which waited for: 6 -> 5; matrix products, arithmetic and copies ran while one was open for 2% -> 1% of each run, Pallas kernels for 7% -> 7%
where the time goes in v4:
time: 189 us; the launch traced here: 188 us
  blocking collectives  128 us (68%)
  starting transfers between devices  29.8 us (16%)
  Pallas kernels  21.4 us (11%)
  waiting for transfers between devices  6.73 us (4%)
    all_to_all x5, blocking collectives, exchange(): return lax.all_to_all(parts, axes, split_axis=0, concat_axis=0, tiled=True)  128 us
    pallas_call x9, Pallas kernels, call(): pl.pallas_call(kernel, out_shape=shapes if len(shapes) > 1 else shapes[0]...  18.6 us
    ppermute x4, starting transfers between devices, swap_cores(): return lax.ppermute(data, 'c', [(0, 1), (1, 0)])  16.1 us
    all_to_all x1, starting transfers between devices, exchange(): return lax.all_to_all(parts, axes, split_axis=0, concat_axis=0, tiled=True)  4.03 us
    ppermute x1, starting transfers between devices, body(): weights.append(lax.ppermute(weights[-1], TP, ring))  4.02 us
    ppermute x1, starting transfers between devices, body(): weights.append(lax.ppermute(weights[0], TP, back))  3.81 us
  transfers between devices with their start and end apart: 8, of which 5 were waited for; matrix products, arithmetic and copies ran while one was open for 1% of the time, Pallas kernels for 7%

profile of v4, /device:TPU:1, one launch (start us, length us, event | category | flops | bytes accessed | tf_op | source)
XLA Modules:
  0.0 188.5 jit_solution(17566172818976959412)
XLA Ops:
  0.0 2.6 %shard_map.158.w0 = bf16[6144,128]{1,0:T(8,128)(2,1)} custom-call(bf16[1,2048,128]{2,1,0:T(8,128)(2,1)} %switch_ref.1, bf16[1,2048,128]{2,1,0:T(8,128)(2,1)} %expansion_ref.1, bf16[1,128,2048]{2,1,0:T(8,128)(2,1)} %contraction_ref.1), custom_call_target="tpu_custom_call" | custom-call | flops 2000000000 | bytes 1000000 | tf_op jit(solution)/shard_map/pallas_call | solution.py:377
  2.6 4.0 %collective-permute-start.1 = (bf16[6144,128]{1,0:T(8,128)(2,1)}, bf16[6144,128]{1,0:T(8,128)(2,1)}, u32[]{:S(2)}, u32[]{:S(2)}) collective-permute-start(bf16[6144,128]{1,0:T(8,128)(2,1)} %shard_map.158.w0), channel_id=1, source_target_pairs={{2,0},{4,2},{6,4},{8,6},{10,8},{12,10},{14,12},{0,14},{15,1},{1,3}... | collective-permute-start | bytes 4718600 | tf_op jit(solution)/shard_map/ppermute | solution.py:438
  6.6 3.8 %collective-permute-start.2 = (bf16[6144,128]{1,0:T(8,128)(2,1)}, bf16[6144,128]{1,0:T(8,128)(2,1)}, u32[]{:S(2)}, u32[]{:S(2)}) collective-permute-start(bf16[6144,128]{1,0:T(8,128)(2,1)} %shard_map.158.w0), channel_id=1, source_target_pairs={{0,2},{2,4},{4,6},{6,8},{8,10},{10,12},{12,14},{14,0},{1,15},{3,1}... | collective-permute-start | bytes 4718600 | tf_op jit(solution)/shard_map/ppermute | solution.py:458
  10.4 6.4 %shard_map.154 = (bf16[4,128,128]{2,1,0:T(8,128)(2,1)}, f32[256,128]{1,0:T(8,128)}, f32[256,128]{1,0:T(8,128)}) custom-call(bf16[256,128]{1,0:T(8,128)(2,1)} %refs_0_.1, bf16[256,128]{1,0:T(8,128)(2,1)} %refs_1_.1, bf16[256,128]{1,0:T(8,128)(2,1)} %refs_2_.1, bf16[256,128]{1,0:T(8,128)(2,1)} %refs_3_.1, f32[256,128]{1,0:T(8,128)} %refs_4_.1, f32[2,256]{1,0:T(2,128)} %bitcast.25), custom_call_target="tpu_custom_call" | custom-call | flops 2000000000 | bytes 1000000 | tf_op jit(solution)/shard_map/pallas_call | solution.py:377
  16.8 4.0 %all-to-all-start = ((bf16[4,128,128]{2,1,0:T(8,128)(2,1)}), bf16[4,128,128]{2,1,0:T(8,128)(2,1)S(1)}, u32[]{:S(2)}, u32[]{:S(2)}) async-start(bf16[4,128,128]{2,1,0:T(8,128)(2,1)} %get-tuple-element.32), calls=%async_computation | async-start | bytes 262144 | tf_op jit(solution)/shard_map/all_to_all | solution.py:393
  20.9 0.7 copy-done.3
  21.5 0.4 shard_map.155
  22.0 3.7 %all-to-all-done.got_ref = bf16[4,128,128]{2,1,0:T(8,128)(2,1)S(1)} async-done(((bf16[4,128,128]{2,1,0:T(8,128)(2,1)}), bf16[4,128,128]{2,1,0:T(8,128)(2,1)S(1)}, u32[]{:S(2)}, u32[]{:S(2)}) %all-to-all-start) | async-done | bytes 131104 | tf_op jit(solution)/shard_map/all_to_all | solution.py:393
  25.7 1.0 shard_map.156
  26.8 19.2 %all_to_all.30.got_ref = bf16[8,128,128]{2,1,0:T(8,128)(2,1)S(1)} all-to-all(bf16[8,128,128]{2,1,0:T(8,128)(2,1)S(1)} %get-tuple-element.35), channel_id=1, replica_groups=mesh['z'=8,'x'=4,'y'=8,'c'=2] {'z'}, dimensions={0} | all-to-all | bytes 524288 | tf_op jit(solution)/shard_map/all_to_all | solution.py:393
  46.0 2.5 %shard_map.157 = (bf16[8,256,128]{2,1,0:T(8,128)(2,1)S(1)}, bf16[8,256,128]{2,1,0:T(8,128)(2,1)S(1)}) custom-call(s32[4]{0:T(128)S(1)} %pad_add_fusion.pos_ref, bf16[8,128,128]{2,1,0:T(8,128)(2,1)S(1)} %all_to_all.30.got_ref, f32[256,128]{1,0:T(8,128)S(1)} %get-tuple-element.36.prefix_ref, f32[256,128]{1,0:T(8,128)S(1)} %copy-done.7, ...), custom_call_target="tpu_custom_call" | custom-call | flops 2000000000 | bytes 1000000 | tf_op jit(solution)/shard_map/pallas_call | solution.py:377
  48.5 5.6 %collective-permute-start = (bf16[8,256,128]{2,1,0:T(8,128)(2,1)S(1)}, bf16[8,256,128]{2,1,0:T(8,128)(2,1)S(1)}, u32[]{:S(2)}, u32[]{:S(2)}) collective-permute-start(bf16[8,256,128]{2,1,0:T(8,128)(2,1)S(1)} %get-tuple-element.40), channel_id=1, source_target_pairs={{0,1},{1,0},{2,3},{3,2},{4,5},{5,4},{6,7},{7,6},{8,9},{9,8},{10,11... | collective-permute-start | bytes 1572872 | tf_op jit(solution)/shard_map/ppermute | solution.py:397
  54.2 0.8 constant_dynamic-slice_fusion.skip_ref
  55.0 0.7 collective-permute-done
  55.7 0.1 add_convert_fusion.1
  55.8 22.5 %all_to_all.31.parts_ref = bf16[8,256,128]{2,1,0:T(8,128)(2,1)S(1)} all-to-all(bf16[8,256,128]{2,1,0:T(8,128)(2,1)S(1)} %add_convert_fusion.1), channel_id=1, replica_groups=mesh['z'=8,'x'=4,'y'=8,'c'=2] {'y'}, dimensions={0} | all-to-all | bytes 1048576 | tf_op jit(solution)/shard_map/all_to_all | solution.py:393
  78.4 1.9 %collective-permute-start.4 = (bf16[6144,128]{1,0:T(8,128)(2,1)}, bf16[6144,128]{1,0:T(8,128)(2,1)S(1)}, u32[]{:S(2)}, u32[]{:S(2)}) collective-permute-start(bf16[6144,128]{1,0:T(8,128)(2,1)} %collective-permute-done.1.w1), channel_id=1, source_target_pairs={{2,0},{4,2},{6,4},{8,6},{10,8},{12,10},{14,12},{0,14},{15,1},{1,3}... | collective-permute-start | bytes 4718600 | tf_op jit(solution)/shard_map/ppermute | solution.py:483
  80.3 0.9 shard_map.159
  81.2 31.5 %all_to_all.32 = bf16[256,8,128]{2,1,0:T(8,128)(2,1)S(1)} all-to-all(bf16[256,8,128]{2,1,0:T(8,128)(2,1)S(1)} %bitcast.16), channel_id=1, replica_groups=mesh['z'=8,'x'=4,'y'=8,'c'=2] {'z','x','y'}, dimensions={0} | all-to-all | bytes 1048576 | tf_op jit(solution)/shard_map/all_to_all | solution.py:393
  112.8 3.6 %collective-permute-start.3 = (bf16[32,8,8,128]{3,2,1,0:T(8,128)(2,1)S(1)}, bf16[32,8,8,128]{3,2,1,0:T(8,128)(2,1)S(1)}, u32[]{:S(2)}, u32[]{:S(2)}) collective-permute-start(bf16[32,8,8,128]{3,2,1,0:T(8,128)(2,1)S(1)} %bitcast.14), channel_id=1, source_target_pairs={{0,1},{1,0},{2,3},{3,2},{4,5},{5,4},{6,7},{7,6},{8,9},{9,8},{10,11... | collective-permute-start | bytes 1572872 | tf_op jit(solution)/shard_map/ppermute | solution.py:397
  116.3 1.3 collective-permute-done.3.other_ref
  117.7 3.8 %shard_map.160 = (bf16[32,8,8,128]{3,2,1,0:T(8,128)(2,1)S(1)}, bf16[32,8,8,128]{3,2,1,0:T(8,128)(2,1)S(1)}) custom-call(s32[4]{0:T(128)S(1)} %pad_add_fusion.pos_ref, bf16[32,8,8,128]{3,2,1,0:T(8,128)(2,1)S(1)} %bitcast.15, bf16[32,8,8,128]{3,2,1,0:T(8,128)(2,1)S(1)} %collective-permute-done.3.other_ref, f32[1,2048]{1,0:T(1,128)S(1)} %bitcast.19, ...), custom_call_target="tpu_custom_call" | custom-call | flops 2000000000 | bytes 1000000 | tf_op jit(solution)/shard_map/pallas_call | solution.py:377
  121.5 2.3 %collective-permute-start.5 = (bf16[32,8,8,128]{3,2,1,0:T(8,128)(2,1)S(1)}, bf16[32,8,8,128]{3,2,1,0:T(8,128)(2,1)S(1)}, u32[]{:S(2)}, u32[]{:S(2)}) collective-permute-start(bf16[32,8,8,128]{3,2,1,0:T(8,128)(2,1)S(1)} %get-tuple-element.51), channel_id=1, source_target_pairs={{0,1},{1,0},{2,3},{3,2},{4,5},{5,4},{6,7},{7,6},{8,9},{9,8},{10,11... | collective-permute-start | bytes 1572872 | tf_op jit(solution)/shard_map/ppermute | solution.py:397
  123.8 0.6 shard_map.161
  124.4 0.9 collective-permute-done.5
  125.3 0.2 add_convert_fusion
  125.5 35.8 %all_to_all.33 = bf16[256,8,128]{2,1,0:T(8,128)(2,1)S(1)} all-to-all(bf16[256,8,128]{2,1,0:T(8,128)(2,1)S(1)} %bitcast.24), channel_id=1, replica_groups=mesh['z'=8,'x'=4,'y'=8,'c'=2] {'z','x','y'}, dimensions={0} | all-to-all | bytes 1048576 | tf_op jit(solution)/shard_map/all_to_all | solution.py:393
  161.3 0.4 shard_map.162
  161.8 19.0 %all_to_all.34.own_ref = bf16[8,256,128]{2,1,0:T(8,128)(2,1)S(1)} all-to-all(bf16[8,256,128]{2,1,0:T(8,128)(2,1)S(1)} %shard_map.162), channel_id=1, replica_groups=mesh['z'=8,'x'=4,'y'=8,'c'=2] {'y'}, dimensions={0} | all-to-all | bytes 1048576 | tf_op jit(solution)/shard_map/all_to_all | solution.py:393
  180.8 4.6 %collective-permute-start.6 = (bf16[8,256,128]{2,1,0:T(8,128)(2,1)S(1)}, bf16[8,256,128]{2,1,0:T(8,128)(2,1)S(1)}, u32[]{:S(2)}, u32[]{:S(2)}) collective-permute-start(bf16[8,256,128]{2,1,0:T(8,128)(2,1)S(1)} %all_to_all.34.own_ref), channel_id=1, source_target_pairs={{0,1},{1,0},{2,3},{3,2},{4,5},{5,4},{6,7},{7,6},{8,9},{9,8},{10,11... | collective-permute-start | bytes 1572872 | tf_op jit(solution)/shard_map/ppermute | solution.py:397
  185.4 1.4 shard_map.163.half_ref
  186.9 1.4 shard_map.164
  (22 shorter events, 0.2 us)
Async XLA Ops:
  2.6 53.2 %collective-permute-start.1 = (bf16[6144,128]{1,0:T(8,128)(2,1)}, bf16[6144,128]{1,0:T(8,128)(2,1)}, u32[]{:S(2)}, u32[]{:S(2)}) collective-permute-start(bf16[6144,128]{1,0:T(8,128)(2,1)} %shard_map.158.w0), channel_id=1, source_target_pairs={{2,0},{4,2},{6,4},{8,6},{10,8},{12,10},{14,12},{0,14},{15,1},{1,3}... | collective-permute-start | bytes 4718600 | tf_op jit(solution)/shard_map/ppermute | solution.py:438
  6.6 49.2 %collective-permute-start.2 = (bf16[6144,128]{1,0:T(8,128)(2,1)}, bf16[6144,128]{1,0:T(8,128)(2,1)}, u32[]{:S(2)}, u32[]{:S(2)}) collective-permute-start(bf16[6144,128]{1,0:T(8,128)(2,1)} %shard_map.158.w0), channel_id=1, source_target_pairs={{0,2},{2,4},{4,6},{6,8},{8,10},{10,12},{12,14},{14,0},{1,15},{3,1}... | collective-permute-start | bytes 4718600 | tf_op jit(solution)/shard_map/ppermute | solution.py:458
  16.8 8.9 %all-to-all-start = ((bf16[4,128,128]{2,1,0:T(8,128)(2,1)}), bf16[4,128,128]{2,1,0:T(8,128)(2,1)S(1)}, u32[]{:S(2)}, u32[]{:S(2)}) async-start(bf16[4,128,128]{2,1,0:T(8,128)(2,1)} %get-tuple-element.32), calls=%async_computation | async-start | bytes 262144 | tf_op jit(solution)/shard_map/all_to_all | solution.py:393
  20.9 0.7 copy-start.3
  25.7 20.3 %copy-start.1 = (bf16[128,2048]{1,0:T(8,128)(2,1)S(1)}, bf16[128,2048]{1,0:T(8,128)(2,1)}, u32[]{:S(2)}) copy-start(bf16[128,2048]{1,0:T(8,128)(2,1)} %w_ref.1) | copy-start | bytes 1572868
  25.7 20.3 %copy-start.6 = (f32[128]{0:T(128)S(1)}, f32[128]{0:T(128)}, u32[]{:S(2)}) copy-start(f32[128]{0:T(128)} %param.22) | copy-start | bytes 1540
  25.7 20.3 %copy-start.7 = (f32[256,128]{1,0:T(8,128)S(1)}, f32[256,128]{1,0:T(8,128)}, u32[]{:S(2)}) copy-start(f32[256,128]{1,0:T(8,128)} %get-tuple-element.37.map_ref) | copy-start | bytes 393220
  25.7 20.3 %copy-start.8 = (f32[256,128]{1,0:T(8,128)S(1)}, f32[256,128]{1,0:T(8,128)}, u32[]{:S(2)}) copy-start(f32[256,128]{1,0:T(8,128)} %get-tuple-element.38.loc_ref) | copy-start | bytes 393220
  48.5 31.8 %copy-start.2 = (f32[2048]{0:T(1024)S(1)}, f32[2048]{0:T(1024)}, u32[]{:S(2)}) copy-start(f32[2048]{0:T(1024)} %param.25) | copy-start | bytes 24580
  48.5 7.2 %collective-permute-start = (bf16[8,256,128]{2,1,0:T(8,128)(2,1)S(1)}, bf16[8,256,128]{2,1,0:T(8,128)(2,1)S(1)}, u32[]{:S(2)}, u32[]{:S(2)}) collective-permute-start(bf16[8,256,128]{2,1,0:T(8,128)(2,1)S(1)} %get-tuple-element.40), channel_id=1, source_target_pairs={{0,1},{1,0},{2,3},{3,2},{4,5},{5,4},{6,7},{7,6},{8,9},{9,8},{10,11... | collective-permute-start | bytes 1572872 | tf_op jit(solution)/shard_map/ppermute | solution.py:397
  78.4 39.3 %collective-permute-start.4 = (bf16[6144,128]{1,0:T(8,128)(2,1)}, bf16[6144,128]{1,0:T(8,128)(2,1)S(1)}, u32[]{:S(2)}, u32[]{:S(2)}) collective-permute-start(bf16[6144,128]{1,0:T(8,128)(2,1)} %collective-permute-done.1.w1), channel_id=1, source_target_pairs={{2,0},{4,2},{6,4},{8,6},{10,8},{12,10},{14,12},{0,14},{15,1},{1,3}... | collective-permute-start | bytes 4718600 | tf_op jit(solution)/shard_map/ppermute | solution.py:483
  80.3 37.4 %copy-start = (bf16[6144,128]{1,0:T(8,128)(2,1)S(1)}, bf16[6144,128]{1,0:T(8,128)(2,1)}, u32[]{:S(2)}) copy-start(bf16[6144,128]{1,0:T(8,128)(2,1)} %shard_map.158.w0) | copy-start | bytes 4718596
  112.8 11.0 %copy-start.4 = (f32[256,2]{0,1:T(2,128)S(1)}, f32[256,2]{0,1:T(2,128)}, u32[]{:S(2)}) copy-start(f32[256,2]{0,1:T(2,128)} %param.27) | copy-start | bytes 6148
  112.8 11.0 %copy-start.5 = (f32[256]{0:T(256)S(1)}, f32[256]{0:T(256)}, u32[]{:S(2)}) copy-start(f32[256]{0:T(256)} %param.26) | copy-start | bytes 3076
  112.8 4.9 %collective-permute-start.3 = (bf16[32,8,8,128]{3,2,1,0:T(8,128)(2,1)S(1)}, bf16[32,8,8,128]{3,2,1,0:T(8,128)(2,1)S(1)}, u32[]{:S(2)}, u32[]{:S(2)}) collective-permute-start(bf16[32,8,8,128]{3,2,1,0:T(8,128)(2,1)S(1)} %bitcast.14), channel_id=1, source_target_pairs={{0,1},{1,0},{2,3},{3,2},{4,5},{5,4},{6,7},{7,6},{8,9},{9,8},{10,11... | collective-permute-start | bytes 1572872 | tf_op jit(solution)/shard_map/ppermute | solution.py:397
  121.5 3.8 %collective-permute-start.5 = (bf16[32,8,8,128]{3,2,1,0:T(8,128)(2,1)S(1)}, bf16[32,8,8,128]{3,2,1,0:T(8,128)(2,1)S(1)}, u32[]{:S(2)}, u32[]{:S(2)}) collective-permute-start(bf16[32,8,8,128]{3,2,1,0:T(8,128)(2,1)S(1)} %get-tuple-element.51), channel_id=1, source_target_pairs={{0,1},{1,0},{2,3},{3,2},{4,5},{5,4},{6,7},{7,6},{8,9},{9,8},{10,11... | collective-permute-start | bytes 1572872 | tf_op jit(solution)/shard_map/ppermute | solution.py:397
  180.8 6.1 %collective-permute-start.6 = (bf16[8,256,128]{2,1,0:T(8,128)(2,1)S(1)}, bf16[8,256,128]{2,1,0:T(8,128)(2,1)S(1)}, u32[]{:S(2)}, u32[]{:S(2)}) collective-permute-start(bf16[8,256,128]{2,1,0:T(8,128)(2,1)S(1)} %all_to_all.34.own_ref), channel_id=1, source_target_pairs={{0,1},{1,0},{2,3},{3,2},{4,5},{5,4},{6,7},{7,6},{8,9},{9,8},{10,11... | collective-permute-start | bytes 1572872 | tf_op jit(solution)/shard_map/ppermute | solution.py:397

commit v5 on v4

--- a/solution.py
+++ b/solution.py
@@ -221,7 +221,7 @@
     prefix_ref[...] = prefix
 
 
-def readout_kernel(pos_ref, got_ref, prefix_ref, map_ref, loc_ref, gain_ref, w_ref, keep_ref, send_ref):
+def readout_kernel(pos_ref, got_ref, prefix_ref, map_ref, loc_ref, gain_ref, w_ref, send_ref, mixed_ref):
     mine, core = pos_ref[1], pos_ref[3]
     state = jnp.where(mine > 0, unpack(got_ref[0])[1], 0.0)
     for n in range(1, got_ref.shape[0] - 1):
@@ -233,15 +233,24 @@
     centered = out - mm_exact(out, ones) * (1.0 / SEG)
     spread = mm_exact(centered * centered, ones) * (1.0 / SEG)
     mixed = (centered * lax.rsqrt(spread + 0.00064) * gain_ref[...]).astype(BF16)
-    for n in range(keep_ref.shape[0]):
-        part = jnp.dot(mixed, w_ref[:, n * 2 * W : (n + 1) * 2 * W], preferred_element_type=F32)
-        first, second = part[:, :W], part[:, W:]
-        keep_ref[n] = jnp.where(core == 0, first, second).astype(BF16)
-        send_ref[n] = jnp.where(core == 0, second, first).astype(BF16)
+    mixed_ref[...] = mixed
+    branch_columns(1 - core, mixed, w_ref, send_ref)
+
+
+def branch_columns(core, mixed, w_ref, out_ref):
+    for n in range(0, out_ref.shape[0], 2):
+        sides = [w_ref[:, pl.ds(pl.multiple_of((2 * m + core) * W, W), W)] for m in (n, n + 1)]
+        part = dot(mixed, jnp.concatenate(sides, axis=1)).astype(BF16)
+        out_ref[n] = part[:, :W]
+        out_ref[n + 1] = part[:, W:]
+
+
+def branch_keep_kernel(pos_ref, mixed_ref, w_ref, keep_ref):
+    branch_columns(pos_ref[3], mixed_ref[...], w_ref, keep_ref)
 
 
 def route_kernel(names_ref, hot_ref, slots_ref):
-    experts, capacity = 32, 32
+    experts = 32
     tokens, places = names_ref.shape[1], hot_ref.shape[0]
     names = [names_ref[k : k + 1, :] for k in range(2)]
     hot = [(iota((experts, tokens), 0) == name).astype(F32) for name in names]
@@ -251,7 +260,12 @@
         jnp.sum(hot[0] * ahead, axis=0, keepdims=True),
         jnp.sum(hot[1] * (ahead + hot[0]), axis=0, keepdims=True),
     ]
-    slots = [(name * capacity).astype(F32) + rank for name, rank in zip(names, ranks)]
+    ranks = [rank.astype(jnp.int32) for rank in ranks]
+    slots = [
+        ((name >> 2) << 7) + ((rank >> 3) << 5) + ((name & 3) << 3) + (rank & 7)
+        for name, rank in zip(names, ranks)
+    ]
+    slots = [slot.astype(F32) for slot in slots]
     place = iota((places, tokens), 0).astype(F32)
     hot_ref[...] = ((place == slots[0]) | (place == slots[1])).astype(F32).astype(BF16)
     slots_ref[...] = jnp.concatenate(slots, axis=0)
@@ -276,46 +290,77 @@
         hidden = hidden + parts_ref[n].astype(F32)
     hid_ref[...] = hidden
     scaled = (hidden * gain_ref[:, pl.ds(column, W)]).astype(BF16)
-    rows = dot(hot_ref[...], scaled).astype(BF16).reshape(32, 32, W)
-    out_ref[:, :32, :] = rows
-    out_ref[:, 32:, :] = rows
-
-
-def expert_kernel(pos_ref, own_ref, other_ref, gain_ref, w0, w1, w2, w3, keep_ref, send_ref):
-    core = pos_ref[3]
-    sources, ways, lines, _ = own_ref.shape
-    rows, width = sources * lines, gain_ref.shape[1]
-    blocks = []
-    for n in range(ways):
-        own = own_ref[:, n].astype(F32).reshape(rows, W)
-        other = other_ref[:, n].astype(F32).reshape(rows, W)
-        blocks.append(jnp.where(core == 0, own, other))
-        blocks.append(jnp.where(core == 0, other, own))
+    groups = out_ref.shape[1] // 2
+    rows = dot(hot_ref[...], scaled)
+    rows = rows.reshape(out_ref.shape[0], groups, *out_ref.shape[2:]).astype(BF16)
+    out_ref[:, :groups] = rows
+    out_ref[:, groups:] = rows
+
+
+def block_at(n, core):
+    return pl.multiple_of((2 * n + core) * W, W)
+
+
+def columns_product(core, data_ref, gain_ref, weight_refs):
+    ways, width = data_ref.shape[1], gain_ref.shape[1]
+    blocks = [data_ref[:, n].astype(F32).reshape(-1, W) for n in range(ways)]
+    squares = jnp.zeros(blocks[0].shape, F32)
+    for n, block in enumerate(blocks):
+        plain = block * (1.0 / gain_ref[:, pl.ds(block_at(n, core), W)])
+        squares = squares + plain * plain
     data = jnp.concatenate([block.astype(BF16) for block in blocks], axis=1)
-    squares = jnp.zeros((rows, W), F32)
-    for n, block in enumerate(blocks):
-        plain = block * (1.0 / gain_ref[:, n * W : (n + 1) * W])
-        squares = squares + plain * plain
-    scale = lax.rsqrt(jnp.sum(squares, axis=1, keepdims=True) * (1.0 / width) + 1e-06)
+    acts = []
+    for w_ref in weight_refs:
+        sides = [
+            jnp.concatenate(
+                [w_ref[pl.ds(at + block_at(n, core), W), :] for n in range(ways)], axis=0
+            )
+            for at in (0, width)
+        ]
+        acts.append(dot(data, jnp.concatenate(sides, axis=1)))
+    return squares, acts
+
+
+def down_columns(core, hidden, width, weight_refs, out_ref):
+    for n in range(0, out_ref.shape[1], 2):
+        sides = [
+            jnp.concatenate(
+                [w_ref[pl.ds(2 * width + block_at(m, core), W), :] for w_ref in weight_refs], axis=0
+            )
+            for m in (n, n + 1)
+        ]
+        part = dot(hidden, jnp.concatenate(sides, axis=1))
+        shape = (out_ref.shape[0], *out_ref.shape[2:])
+        out_ref[:, n] = part[:, :W].reshape(shape).astype(BF16)
+        out_ref[:, n + 1] = part[:, W:].reshape(shape).astype(BF16)
+
+
+def expert_own_kernel(pos_ref, own_ref, gain_ref, w0, w1, w2, w3, act_ref, square_ref):
+    square_ref[...], acts = columns_product(pos_ref[3], own_ref, gain_ref, (w0, w1, w2, w3))
+    for n, act in enumerate(acts):
+        act_ref[n] = act
+
+
+def expert_kernel(
+    pos_ref, other_ref, gain_ref, act_ref, square_ref, w0, w1, w2, w3, send_ref, hidden_ref
+):
+    core, width = pos_ref[3], gain_ref.shape[1]
+    squares, acts = columns_product(1 - core, other_ref, gain_ref, (w0, w1, w2, w3))
+    total = jnp.sum(squares + square_ref[...], axis=1, keepdims=True)
+    scale = lax.rsqrt(total * (1.0 / width) + 1e-06)
     hidden = []
-    for w_ref in (w0, w1, w2, w3):
-        both = jnp.concatenate([w_ref[:width], w_ref[width : 2 * width]], axis=1)
-        act = jnp.dot(data, both, preferred_element_type=F32) * scale
+    for n, act in enumerate(acts):
+        act = (act + act_ref[n]) * scale
         gate, up = act[:, :W], act[:, W:]
         hidden.append((gate / (1.0 + jnp.exp(-gate)) * up).astype(BF16))
     hidden = jnp.concatenate(hidden, axis=1)
-    for n in range(ways):
-        at = 2 * width + 2 * n * W
-        pieces = [
-            jnp.concatenate([w_ref[at : at + W], w_ref[at + W : at + 2 * W]], axis=1)
-            for w_ref in (w0, w1, w2, w3)
-        ]
-        part = jnp.dot(hidden, jnp.concatenate(pieces, axis=0), preferred_element_type=F32)
-        first, second = part[:, :W], part[:, W:]
-        keep = jnp.where(core == 0, first, second).reshape(sources, lines, W)
-        send = jnp.where(core == 0, second, first).reshape(sources, lines, W)
-        keep_ref[:, n] = keep.astype(BF16)
-        send_ref[:, n] = send.astype(BF16)
+    hidden_ref[...] = hidden
+    down_columns(1 - core, hidden, width, (w0, w1, w2, w3), send_ref)
+
+
+def expert_keep_kernel(pos_ref, hidden_ref, w0, w1, w2, w3, keep_ref):
+    width = w0.shape[0] // 3
+    down_columns(pos_ref[3], hidden_ref[...], width, (w0, w1, w2, w3), keep_ref)
 
 
 def combine_kernel(ret_ref, hid_ref, high_ref, low_ref, out_ref):
@@ -462,9 +507,9 @@
         compose_kernel, [((n_z, W, W), BF16), ((2 * W, W), F32)], pos, gathered, scalars=1
     )
     gathered = exchange(pairs, "z")
-    keep, send = call(
+    send, mixed = call(
         readout_kernel,
-        [((n_y, tokens, W), BF16), ((n_y, tokens, W), BF16)],
+        [((n_y, tokens, W), BF16), ((tokens, W), BF16)],
         pos,
         gathered,
         prefix,
@@ -475,7 +520,8 @@
         scalars=1,
     )
     own_skip = lax.dynamic_slice_in_dim(skip, (here[2] * 2 + here[3]) * W, W, 1)
-    send, own_skip = lax.optimization_barrier((swap_cores(send), own_skip))
+    keep = call(branch_keep_kernel, [((n_y, tokens, W), BF16)], pos, mixed, blender, scalars=1)
+    send, own_skip, keep = lax.optimization_barrier((swap_cores(send), own_skip, keep))
     branch = (keep.astype(F32) + send.astype(F32)).astype(BF16)
     branch, weights[1], weights[2] = lax.optimization_barrier((branch, weights[1], weights[2]))
     parts = exchange(branch, "y")
@@ -483,7 +529,7 @@
     weights.append(lax.ppermute(weights[1], TP, ring))
     hidden, outgoing = call(
         dispatch_kernel,
-        [((tokens, W), F32), ((n_z * n_x, 64, W), BF16)],
+        [((tokens, W), F32), ((n_z, n_y, n_x, 8, W), BF16)],
         pos,
         parts,
         own_skip,
@@ -491,15 +537,15 @@
         hot,
         scalars=1,
     )
-    own = exchange(outgoing.reshape(n_z * n_x * n_y, 8, W), ("z", "x", "y"))
-    own = own.reshape(n_z * n_x, n_y, 8, W)
-    keep, send = call(
-        expert_kernel,
-        [((n_z * n_x, n_y, 8, W), BF16), ((n_z * n_x, n_y, 8, W), BF16)],
+    own = exchange(outgoing.reshape(n_z * n_x * n_y, 8, W), ("z", "y", "x"))
+    own = own.reshape(n_z, n_y, n_x, 8, W)
+    gains = norm_gain[None]
+    acts, squares = call(
+        expert_own_kernel,
+        [((4, tokens, 2 * W), F32), ((tokens, W), F32)],
         pos,
         own,
-        swap_cores(own),
-        norm_gain[None],
+        gains,
         *weights,
         scalars=1,
     )
@@ -510,10 +556,25 @@
         cluster_chance[None],
         within_chance.T,
     )
-    send, high, low = lax.optimization_barrier((swap_cores(send), high, low))
+    other, acts = lax.optimization_barrier((swap_cores(own), acts))
+    send, units = call(
+        expert_kernel,
+        [((n_z, n_y, n_x, 8, W), BF16), ((tokens, 4 * W), BF16)],
+        pos,
+        other,
+        gains,
+        acts,
+        squares,
+        *weights,
+        scalars=1,
+    )
+    keep = call(
+        expert_keep_kernel, [((n_z, n_y, n_x, 8, W), BF16)], pos, units, *weights, scalars=1
+    )
+    send, keep, high, low = lax.optimization_barrier((swap_cores(send), keep, high, low))
     summed = (keep.astype(F32) + send.astype(F32)).astype(BF16)
-    returned = exchange(summed.reshape(n_z * n_x * n_y, 8, W), ("z", "x", "y"))
-    returned = returned.reshape(n_z * n_x, n_y, 8, W)
+    returned = exchange(summed.reshape(n_z * n_x * n_y, 8, W), ("z", "y", "x"))
+    returned = returned.reshape(n_z, n_y, n_x, 8, W)
     copies = call(combine_kernel, [((n_y, tokens, W), BF16)], returned, hidden, high, low)
     own = exchange(copies, "y")
     other = swap_cores(own)

time: 189 us -> 189 us (level)
  Pallas kernels: 21.4 us -> 26.2 us
  waiting for transfers between devices: 6.73 us -> 3.8 us
  blocking collectives: 128 us -> 126 us
    pallas_call x9 -> x12, Pallas kernels: 18.6 us -> 23.4 us  [call(): pl.pallas_call(kernel, out_shape=shapes if len(shapes) > 1 else shapes[0]...]
    ppermute x4, waiting for transfers between devices: 3.04 us -> 0.12 us  [swap_cores(): return lax.ppermute(data, 'c', [(0, 1), (1, 0)])]
  transfers between devices with their start and end apart: 8 -> 8, of which waited for: 5 -> 2; matrix products, arithmetic and copies ran while one was open for 1% -> 1% of each run, Pallas kernels for 7% -> 10%
where the time goes in v5:
time: 189 us
  blocking collectives  126 us (67%)
  starting transfers between devices  29.8 us (16%)
  Pallas kernels  26.2 us (14%)
  waiting for transfers between devices  3.8 us (2%)
    all_to_all x5, blocking collectives, exchange(): return lax.all_to_all(parts, axes, split_axis=0, concat_axis=0, tiled=True)  126 us
    pallas_call x12, Pallas kernels, call(): pl.pallas_call(kernel, out_shape=shapes if len(shapes) > 1 else shapes[0]...  23.4 us
    ppermute x4, starting transfers between devices, swap_cores(): return lax.ppermute(data, 'c', [(0, 1), (1, 0)])  16 us
    ppermute x1, starting transfers between devices, body(): weights.append(lax.ppermute(weights[-1], TP, ring))  4.02 us
    all_to_all x1, starting transfers between devices, exchange(): return lax.all_to_all(parts, axes, split_axis=0, concat_axis=0, tiled=True)  4.02 us
    ppermute x1, starting transfers between devices, body(): weights.append(lax.ppermute(weights[0], TP, back))  3.81 us
  transfers between devices with their start and end apart: 8, of which 2 were waited for; matrix products, arithmetic and copies ran while one was open for 1% of the time, Pallas kernels for 10%

profile of v5, /device:TPU:1, one launch (start us, length us, event | category | flops | bytes accessed | tf_op | source)
XLA Modules:
  0.0 188.5 jit_solution(5676248212974769108)
XLA Ops:
  0.0 2.6 %shard_map.159.w0 = bf16[6144,128]{1,0:T(8,128)(2,1)} custom-call(bf16[1,2048,128]{2,1,0:T(8,128)(2,1)} %switch_ref.1, bf16[1,2048,128]{2,1,0:T(8,128)(2,1)} %expansion_ref.1, bf16[1,128,2048]{2,1,0:T(8,128)(2,1)} %contraction_ref.1), custom_call_target="tpu_custom_call" | custom-call | flops 2000000000 | bytes 1000000 | tf_op jit(solution)/shard_map/pallas_call | solution.py:422
  2.6 4.0 %collective-permute-start.1 = (bf16[6144,128]{1,0:T(8,128)(2,1)}, bf16[6144,128]{1,0:T(8,128)(2,1)}, u32[]{:S(2)}, u32[]{:S(2)}) collective-permute-start(bf16[6144,128]{1,0:T(8,128)(2,1)} %shard_map.159.w0), channel_id=1, source_target_pairs={{2,0},{4,2},{6,4},{8,6},{10,8},{12,10},{14,12},{0,14},{15,1},{1,3}... | collective-permute-start | bytes 4718600 | tf_op jit(solution)/shard_map/ppermute | solution.py:483
  6.6 3.8 %collective-permute-start.2 = (bf16[6144,128]{1,0:T(8,128)(2,1)}, bf16[6144,128]{1,0:T(8,128)(2,1)}, u32[]{:S(2)}, u32[]{:S(2)}) collective-permute-start(bf16[6144,128]{1,0:T(8,128)(2,1)} %shard_map.159.w0), channel_id=1, source_target_pairs={{0,2},{2,4},{4,6},{6,8},{8,10},{10,12},{12,14},{14,0},{1,15},{3,1}... | collective-permute-start | bytes 4718600 | tf_op jit(solution)/shard_map/ppermute | solution.py:503
  10.5 6.4 %shard_map.154 = (bf16[4,128,128]{2,1,0:T(8,128)(2,1)}, f32[256,128]{1,0:T(8,128)}, f32[256,128]{1,0:T(8,128)}) custom-call(bf16[256,128]{1,0:T(8,128)(2,1)} %refs_0_.1, bf16[256,128]{1,0:T(8,128)(2,1)} %refs_1_.1, bf16[256,128]{1,0:T(8,128)(2,1)} %refs_2_.1, bf16[256,128]{1,0:T(8,128)(2,1)} %refs_3_.1, f32[256,128]{1,0:T(8,128)} %refs_4_.1, f32[2,256]{1,0:T(2,128)} %bitcast.26), custom_call_target="tpu_custom_call" | custom-call | flops 2000000000 | bytes 1000000 | tf_op jit(solution)/shard_map/pallas_call | solution.py:422
  16.8 4.0 %all-to-all-start = ((bf16[4,128,128]{2,1,0:T(8,128)(2,1)}), bf16[4,128,128]{2,1,0:T(8,128)(2,1)S(1)}, u32[]{:S(2)}, u32[]{:S(2)}) async-start(bf16[4,128,128]{2,1,0:T(8,128)(2,1)} %get-tuple-element.38), calls=%async_computation | async-start | bytes 262144 | tf_op jit(solution)/shard_map/all_to_all | solution.py:438
  20.9 0.7 copy-done.3
  21.5 0.4 shard_map.155
  22.0 3.7 %all-to-all-done.got_ref = bf16[4,128,128]{2,1,0:T(8,128)(2,1)S(1)} async-done(((bf16[4,128,128]{2,1,0:T(8,128)(2,1)}), bf16[4,128,128]{2,1,0:T(8,128)(2,1)S(1)}, u32[]{:S(2)}, u32[]{:S(2)}) %all-to-all-start) | async-done | bytes 131104 | tf_op jit(solution)/shard_map/all_to_all | solution.py:438
  25.7 1.0 shard_map.156
  26.8 19.2 %all_to_all.30.got_ref = bf16[8,128,128]{2,1,0:T(8,128)(2,1)S(1)} all-to-all(bf16[8,128,128]{2,1,0:T(8,128)(2,1)S(1)} %get-tuple-element.41), channel_id=1, replica_groups=mesh['z'=8,'x'=4,'y'=8,'c'=2] {'z'}, dimensions={0} | all-to-all | bytes 524288 | tf_op jit(solution)/shard_map/all_to_all | solution.py:438
  46.0 2.4 %shard_map.157 = (bf16[8,256,128]{2,1,0:T(8,128)(2,1)S(1)}, bf16[256,128]{1,0:T(8,128)(2,1)S(1)}) custom-call(s32[4]{0:T(128)S(1)} %pad_add_fusion.pos_ref, bf16[8,128,128]{2,1,0:T(8,128)(2,1)S(1)} %all_to_all.30.got_ref, f32[256,128]{1,0:T(8,128)S(1)} %get-tuple-element.42.prefix_ref, f32[256,128]{1,0:T(8,128)S(1)} %copy-done.7, f32[256,128]{1,0:T(8,128)S(1)} %copy-done.8, ...), custom_call_target="tpu_custom_call" | custom-call | flops 2000000000 | bytes 1000000 | tf_op jit(solution)/shard_map/pallas_call | solution.py:422
  48.4 5.7 %collective-permute-start = (bf16[8,256,128]{2,1,0:T(8,128)(2,1)S(1)}, bf16[8,256,128]{2,1,0:T(8,128)(2,1)S(1)}, u32[]{:S(2)}, u32[]{:S(2)}) collective-permute-start(bf16[8,256,128]{2,1,0:T(8,128)(2,1)S(1)} %get-tuple-element.45), channel_id=1, source_target_pairs={{0,1},{1,0},{2,3},{3,2},{4,5},{5,4},{6,7},{7,6},{8,9},{9,8},{10,11... | collective-permute-start | bytes 1572872 | tf_op jit(solution)/shard_map/ppermute | solution.py:442
  54.1 0.8 constant_dynamic-slice_fusion.skip_ref
  54.9 0.9 shard_map.158
  55.8 0.1 add_convert_fusion.1
  56.0 23.7 %all_to_all.31.parts_ref = bf16[8,256,128]{2,1,0:T(8,128)(2,1)S(1)} all-to-all(bf16[8,256,128]{2,1,0:T(8,128)(2,1)S(1)} %add_convert_fusion.1), channel_id=1, replica_groups=mesh['z'=8,'x'=4,'y'=8,'c'=2] {'y'}, dimensions={0} | all-to-all | bytes 1048576 | tf_op jit(solution)/shard_map/all_to_all | solution.py:438
  79.6 1.9 %collective-permute-start.4 = (bf16[6144,128]{1,0:T(8,128)(2,1)}, bf16[6144,128]{1,0:T(8,128)(2,1)S(1)}, u32[]{:S(2)}, u32[]{:S(2)}) collective-permute-start(bf16[6144,128]{1,0:T(8,128)(2,1)} %collective-permute-done.1.w1), channel_id=1, source_target_pairs={{2,0},{4,2},{6,4},{8,6},{10,8},{12,10},{14,12},{0,14},{15,1},{1,3}... | collective-permute-start | bytes 4718600 | tf_op jit(solution)/shard_map/ppermute | solution.py:529
  81.6 0.9 shard_map.160
  82.5 31.6 %all_to_all.32 = bf16[256,8,128]{2,1,0:T(8,128)(2,1)S(1)} all-to-all(bf16[256,8,128]{2,1,0:T(8,128)(2,1)S(1)} %bitcast.16), channel_id=1, replica_groups=mesh['z'=8,'x'=4,'y'=8,'c'=2] {'z','y','x'}, dimensions={0} | all-to-all | bytes 1048576 | tf_op jit(solution)/shard_map/all_to_all | solution.py:438
  114.0 2.5 %collective-permute-start.3 = (bf16[8,8,4,8,128]{4,3,2,1,0:T(8,128)(2,1)S(1)}, bf16[8,8,4,8,128]{4,3,2,1,0:T(8,128)(2,1)S(1)}, u32[]{:S(2)}, u32[]{:S(2)}) collective-permute-start(bf16[8,8,4,8,128]{4,3,2,1,0:T(8,128)(2,1)S(1)} %bitcast.14), channel_id=1, source_target_pairs={{0,1},{1,0},{2,3},{3,2},{4,5},{5,4},{6,7},{7,6},{8,9},{9,8},{10,11... | collective-permute-start | bytes 1572872 | tf_op jit(solution)/shard_map/ppermute | solution.py:442
  116.6 2.6 %shard_map.161 = (f32[4,256,256]{2,1,0:T(8,128)S(1)}, f32[256,128]{1,0:T(8,128)S(1)}) custom-call(s32[4]{0:T(128)S(1)} %pad_add_fusion.pos_ref, bf16[8,8,4,8,128]{4,3,2,1,0:T(8,128)(2,1)S(1)} %bitcast.15, f32[1,2048]{1,0:T(1,128)S(1)} %bitcast.19, bf16[6144,128]{1,0:T(8,128)(2,1)S(1)} %copy-done, bf16[6144,128]{1,0:T(8,128)(2,1)} %collective-permute-done.1.w1, ...), custom_call_target="tpu_custom_call" | custom-call | flops 2000000000 | bytes 1000000 | tf_op jit(solution)/shard_map/pallas_call | solution.py:422
  119.3 2.9 %shard_map.162 = (bf16[8,8,4,8,128]{4,3,2,1,0:T(8,128)(2,1)S(1)}, bf16[256,512]{1,0:T(8,128)(2,1)S(1)}) custom-call(s32[4]{0:T(128)S(1)} %pad_add_fusion.pos_ref, bf16[8,8,4,8,128]{4,3,2,1,0:T(8,128)(2,1)S(1)} %collective-permute-done.3.other_ref, f32[1,2048]{1,0:T(1,128)S(1)} %bitcast.20, f32[4,256,256]{2,1,0:T(8,128)S(1)} %get-tuple-element.59.act_ref, ...), custom_call_target="tpu_custom_call" | custom-call | flops 2000000000 | bytes 1000000 | tf_op jit(solution)/shard_map/pallas_call | solution.py:422
  122.2 2.0 %collective-permute-start.5 = (bf16[8,8,4,8,128]{4,3,2,1,0:T(8,128)(2,1)S(1)}, bf16[8,8,4,8,128]{4,3,2,1,0:T(8,128)(2,1)S(1)}, u32[]{:S(2)}, u32[]{:S(2)}) collective-permute-start(bf16[8,8,4,8,128]{4,3,2,1,0:T(8,128)(2,1)S(1)} %get-tuple-element.61), channel_id=1, source_target_pairs={{0,1},{1,0},{2,3},{3,2},{4,5},{5,4},{6,7},{7,6},{8,9},{9,8},{10,11... | collective-permute-start | bytes 1572872 | tf_op jit(solution)/shard_map/ppermute | solution.py:442
  124.2 0.6 shard_map.164
  124.8 2.3 %shard_map.163 = bf16[8,8,4,8,128]{4,3,2,1,0:T(8,128)(2,1)S(1)} custom-call(s32[4]{0:T(128)S(1)} %pad_add_fusion.pos_ref, bf16[256,512]{1,0:T(8,128)(2,1)S(1)} %get-tuple-element.62.hidden_ref, bf16[6144,128]{1,0:T(8,128)(2,1)S(1)} %copy-done, bf16[6144,128]{1,0:T(8,128)(2,1)} %collective-permute-done.1.w1, bf16[6144,128]{1,0:T(8,128)(2,1)} %collective-permute-done.2.w2, ...), custom_call_target="tpu_custom_call" | custom-call | flops 2000000000 | bytes 1000000 | tf_op jit(solution)/shard_map/pallas_call | solution.py:422
  127.1 0.1 add_convert_fusion
  127.3 33.7 %all_to_all.33 = bf16[256,8,128]{2,1,0:T(8,128)(2,1)S(1)} all-to-all(bf16[256,8,128]{2,1,0:T(8,128)(2,1)S(1)} %bitcast.25), channel_id=1, replica_groups=mesh['z'=8,'x'=4,'y'=8,'c'=2] {'z','y','x'}, dimensions={0} | all-to-all | bytes 1048576 | tf_op jit(solution)/shard_map/all_to_all | solution.py:438
  161.0 0.4 shard_map.165
  161.4 18.2 %all_to_all.34.own_ref = bf16[8,256,128]{2,1,0:T(8,128)(2,1)S(1)} all-to-all(bf16[8,256,128]{2,1,0:T(8,128)(2,1)S(1)} %shard_map.165), channel_id=1, replica_groups=mesh['z'=8,'x'=4,'y'=8,'c'=2] {'y'}, dimensions={0} | all-to-all | bytes 1048576 | tf_op jit(solution)/shard_map/all_to_all | solution.py:438
  179.6 5.8 %collective-permute-start.6 = (bf16[8,256,128]{2,1,0:T(8,128)(2,1)S(1)}, bf16[8,256,128]{2,1,0:T(8,128)(2,1)S(1)}, u32[]{:S(2)}, u32[]{:S(2)}) collective-permute-start(bf16[8,256,128]{2,1,0:T(8,128)(2,1)S(1)} %all_to_all.34.own_ref), channel_id=1, source_target_pairs={{0,1},{1,0},{2,3},{3,2},{4,5},{5,4},{6,7},{7,6},{8,9},{9,8},{10,11... | collective-permute-start | bytes 1572872 | tf_op jit(solution)/shard_map/ppermute | solution.py:442
  185.4 1.4 shard_map.166.half_ref
  187.0 1.4 shard_map.167
  (25 shorter events, 0.2 us)
Async XLA Ops:
  2.6 53.4 %collective-permute-start.1 = (bf16[6144,128]{1,0:T(8,128)(2,1)}, bf16[6144,128]{1,0:T(8,128)(2,1)}, u32[]{:S(2)}, u32[]{:S(2)}) collective-permute-start(bf16[6144,128]{1,0:T(8,128)(2,1)} %shard_map.159.w0), channel_id=1, source_target_pairs={{2,0},{4,2},{6,4},{8,6},{10,8},{12,10},{14,12},{0,14},{15,1},{1,3}... | collective-permute-start | bytes 4718600 | tf_op jit(solution)/shard_map/ppermute | solution.py:483
  6.6 49.3 %collective-permute-start.2 = (bf16[6144,128]{1,0:T(8,128)(2,1)}, bf16[6144,128]{1,0:T(8,128)(2,1)}, u32[]{:S(2)}, u32[]{:S(2)}) collective-permute-start(bf16[6144,128]{1,0:T(8,128)(2,1)} %shard_map.159.w0), channel_id=1, source_target_pairs={{0,2},{2,4},{4,6},{6,8},{8,10},{10,12},{12,14},{14,0},{1,15},{3,1}... | collective-permute-start | bytes 4718600 | tf_op jit(solution)/shard_map/ppermute | solution.py:503
  16.8 8.8 %all-to-all-start = ((bf16[4,128,128]{2,1,0:T(8,128)(2,1)}), bf16[4,128,128]{2,1,0:T(8,128)(2,1)S(1)}, u32[]{:S(2)}, u32[]{:S(2)}) async-start(bf16[4,128,128]{2,1,0:T(8,128)(2,1)} %get-tuple-element.38), calls=%async_computation | async-start | bytes 262144 | tf_op jit(solution)/shard_map/all_to_all | solution.py:438
  20.9 0.7 copy-start.3
  25.7 20.3 %copy-start.2 = (bf16[128,2048]{1,0:T(8,128)(2,1)S(1)}, bf16[128,2048]{1,0:T(8,128)(2,1)}, u32[]{:S(2)}) copy-start(bf16[128,2048]{1,0:T(8,128)(2,1)} %w_ref.3) | copy-start | bytes 1572868
  25.7 20.3 %copy-start.6 = (f32[128]{0:T(128)S(1)}, f32[128]{0:T(128)}, u32[]{:S(2)}) copy-start(f32[128]{0:T(128)} %param.22) | copy-start | bytes 1540
  25.7 20.3 %copy-start.7 = (f32[256,128]{1,0:T(8,128)S(1)}, f32[256,128]{1,0:T(8,128)}, u32[]{:S(2)}) copy-start(f32[256,128]{1,0:T(8,128)} %get-tuple-element.43.map_ref) | copy-start | bytes 393220
  25.7 20.3 %copy-start.8 = (f32[256,128]{1,0:T(8,128)S(1)}, f32[256,128]{1,0:T(8,128)}, u32[]{:S(2)}) copy-start(f32[256,128]{1,0:T(8,128)} %get-tuple-element.44.loc_ref) | copy-start | bytes 393220
  48.4 7.4 %collective-permute-start = (bf16[8,256,128]{2,1,0:T(8,128)(2,1)S(1)}, bf16[8,256,128]{2,1,0:T(8,128)(2,1)S(1)}, u32[]{:S(2)}, u32[]{:S(2)}) collective-permute-start(bf16[8,256,128]{2,1,0:T(8,128)(2,1)S(1)} %get-tuple-element.45), channel_id=1, source_target_pairs={{0,1},{1,0},{2,3},{3,2},{4,5},{5,4},{6,7},{7,6},{8,9},{9,8},{10,11... | collective-permute-start | bytes 1572872 | tf_op jit(solution)/shard_map/ppermute | solution.py:442
  55.8 25.8 %copy-start.1 = (f32[2048]{0:T(1024)S(1)}, f32[2048]{0:T(1024)}, u32[]{:S(2)}) copy-start(f32[2048]{0:T(1024)} %param.25) | copy-start | bytes 24580
  79.6 36.9 %collective-permute-start.4 = (bf16[6144,128]{1,0:T(8,128)(2,1)}, bf16[6144,128]{1,0:T(8,128)(2,1)S(1)}, u32[]{:S(2)}, u32[]{:S(2)}) collective-permute-start(bf16[6144,128]{1,0:T(8,128)(2,1)} %collective-permute-done.1.w1), channel_id=1, source_target_pairs={{2,0},{4,2},{6,4},{8,6},{10,8},{12,10},{14,12},{0,14},{15,1},{1,3}... | collective-permute-start | bytes 4718600 | tf_op jit(solution)/shard_map/ppermute | solution.py:529
  81.6 35.0 %copy-start = (bf16[6144,128]{1,0:T(8,128)(2,1)S(1)}, bf16[6144,128]{1,0:T(8,128)(2,1)}, u32[]{:S(2)}) copy-start(bf16[6144,128]{1,0:T(8,128)(2,1)} %shard_map.159.w0) | copy-start | bytes 4718596
  114.0 5.2 %collective-permute-start.3 = (bf16[8,8,4,8,128]{4,3,2,1,0:T(8,128)(2,1)S(1)}, bf16[8,8,4,8,128]{4,3,2,1,0:T(8,128)(2,1)S(1)}, u32[]{:S(2)}, u32[]{:S(2)}) collective-permute-start(bf16[8,8,4,8,128]{4,3,2,1,0:T(8,128)(2,1)S(1)} %bitcast.14), channel_id=1, source_target_pairs={{0,1},{1,0},{2,3},{3,2},{4,5},{5,4},{6,7},{7,6},{8,9},{9,8},{10,11... | collective-permute-start | bytes 1572872 | tf_op jit(solution)/shard_map/ppermute | solution.py:442
  119.2 5.0 %copy-start.4 = (f32[256,2]{0,1:T(2,128)S(1)}, f32[256,2]{0,1:T(2,128)}, u32[]{:S(2)}) copy-start(f32[256,2]{0,1:T(2,128)} %param.27) | copy-start | bytes 6148
  119.2 5.0 %copy-start.5 = (f32[256]{0:T(256)S(1)}, f32[256]{0:T(256)}, u32[]{:S(2)}) copy-start(f32[256]{0:T(256)} %param.26) | copy-start | bytes 3076
  122.2 4.9 %collective-permute-start.5 = (bf16[8,8,4,8,128]{4,3,2,1,0:T(8,128)(2,1)S(1)}, bf16[8,8,4,8,128]{4,3,2,1,0:T(8,128)(2,1)S(1)}, u32[]{:S(2)}, u32[]{:S(2)}) collective-permute-start(bf16[8,8,4,8,128]{4,3,2,1,0:T(8,128)(2,1)S(1)} %get-tuple-element.61), channel_id=1, source_target_pairs={{0,1},{1,0},{2,3},{3,2},{4,5},{5,4},{6,7},{7,6},{8,9},{9,8},{10,11... | collective-permute-start | bytes 1572872 | tf_op jit(solution)/shard_map/ppermute | solution.py:442
  179.6 7.4 %collective-permute-start.6 = (bf16[8,256,128]{2,1,0:T(8,128)(2,1)S(1)}, bf16[8,256,128]{2,1,0:T(8,128)(2,1)S(1)}, u32[]{:S(2)}, u32[]{:S(2)}) collective-permute-start(bf16[8,256,128]{2,1,0:T(8,128)(2,1)S(1)} %all_to_all.34.own_ref), channel_id=1, source_target_pairs={{0,1},{1,0},{2,3},{3,2},{4,5},{5,4},{6,7},{7,6},{8,9},{9,8},{10,11... | collective-permute-start | bytes 1572872 | tf_op jit(solution)/shard_map/ppermute | solution.py:442

commit v6 on v5

--- a/solution.py
+++ b/solution.py
@@ -61,24 +61,60 @@
     return (iota((W, W), 0) // SEG == iota((W, W), 1) // SEG).astype(F32).astype(BF16)
 
 
-def pack_kernel(switch_ref, expansion_ref, contraction_ref, out_ref, sems):
+def pack_kernel(switch_ref, expansion_ref, contraction_ref, out_ref, held, sems):
     depth = switch_ref.shape[1]
     copies = [
-        pltpu.make_async_copy(switch_ref.at[0], out_ref.at[pl.ds(0, depth)], sems.at[0]),
-        pltpu.make_async_copy(expansion_ref.at[0], out_ref.at[pl.ds(depth, depth)], sems.at[1]),
+        pltpu.make_async_copy(switch_ref.at[0], held.at[pl.ds(0, depth)], sems.at[0]),
+        pltpu.make_async_copy(expansion_ref.at[0], held.at[pl.ds(depth, depth)], sems.at[1]),
     ]
     for n in range(depth // W):
         copies.append(
             pltpu.make_async_copy(
                 contraction_ref.at[0, :, pl.ds(n * W, W)],
-                out_ref.at[pl.ds(2 * depth + n * W, W)],
+                held.at[pl.ds(2 * depth + n * W, W)],
                 sems.at[2 + n],
             )
         )
+    onward = [
+        pltpu.make_async_copy(
+            held.at[pl.ds(n * depth, depth)],
+            out_ref.at[pl.ds(n * depth, depth)],
+            sems.at[len(copies) + n],
+        )
+        for n in range(3)
+    ]
     for copy in copies:
         copy.start()
-    for copy in copies:
+    for n in range(2):
+        copies[n].wait()
+        onward[n].start()
+    for copy in copies[2:]:
         copy.wait()
+    onward[2].start()
+    for copy in onward:
+        copy.wait()
+
+
+def hold_kernel(far_ref, near_ref, sem):
+    copy = pltpu.make_async_copy(far_ref, near_ref, sem)
+    copy.start()
+    copy.wait()
+
+
+def hold(data):
+    return pl.pallas_call(
+        hold_kernel,
+        name="hold",
+        out_shape=jax.ShapeDtypeStruct(data.shape, data.dtype),
+        in_specs=[pl.BlockSpec(memory_space=pl.ANY)],
+        out_specs=pl.BlockSpec(memory_space=pltpu.VMEM),
+        scratch_shapes=[pltpu.SemaphoreType.DMA(())],
+        compiler_params=pltpu.CompilerParams(vmem_limit_bytes=8 << 20),
+        cost_estimate=pl.CostEstimate(
+            flops=1_000_000_000, bytes_accessed=1_000_000, transcendentals=0
+        ),
+        interpret=INTERPRET,
+    )(data)
 
 
 def columns_of(rows):
@@ -285,7 +321,7 @@
 
 def dispatch_kernel(pos_ref, parts_ref, skip_ref, gain_ref, hot_ref, hid_ref, out_ref):
     column = pl.multiple_of((pos_ref[2] * 2 + pos_ref[3]) * W, W)
-    hidden = skip_ref[...].astype(F32)
+    hidden = skip_ref[:, pl.ds(column, W)].astype(F32)
     for n in range(parts_ref.shape[0]):
         hidden = hidden + parts_ref[n].astype(F32)
     hid_ref[...] = hidden
@@ -468,18 +504,20 @@
     ring = [(((y + 1) % n_y) * 2, y * 2) for y in range(n_y)]
     ring += [(((y - 1) % n_y) * 2 + 1, y * 2 + 1) for y in range(n_y)]
     back = [(target, source) for source, target in ring]
-    weights = [
-        call(
-            pack_kernel,
-            [((3 * width, W), BF16)],
-            switch,
-            expansion,
-            contraction,
-            far=(0, 1, 2),
-            scratch=[pltpu.SemaphoreType.DMA((2 + width // W,))],
-            grant=67043328,
-        )
-    ]
+    packed = pl.pallas_call(
+        pack_kernel,
+        name="pack",
+        out_shape=jax.ShapeDtypeStruct((3 * width, W), BF16),
+        in_specs=[pl.BlockSpec(memory_space=pltpu.HBM)] * 3,
+        out_specs=pl.BlockSpec(memory_space=pltpu.HBM),
+        scratch_shapes=[
+            pltpu.VMEM((3 * width, W), BF16),
+            pltpu.SemaphoreType.DMA((5 + width // W,)),
+        ],
+        compiler_params=pltpu.CompilerParams(vmem_limit_bytes=67043328),
+        interpret=INTERPRET,
+    )(switch, expansion, contraction)
+    weights = [packed]
     weights.append(lax.ppermute(weights[-1], TP, ring))
     pairs, state_map, local = call(
         mixer_kernel,
@@ -507,6 +545,8 @@
         compose_kernel, [((n_z, W, W), BF16), ((2 * W, W), F32)], pos, gathered, scalars=1
     )
     gathered = exchange(pairs, "z")
+    gathered, weights[1] = lax.optimization_barrier((gathered, weights[1]))
+    weights.append(lax.ppermute(weights[1], TP, ring))
     send, mixed = call(
         readout_kernel,
         [((n_y, tokens, W), BF16), ((tokens, W), BF16)],
@@ -519,20 +559,17 @@
         blender,
         scalars=1,
     )
-    own_skip = lax.dynamic_slice_in_dim(skip, (here[2] * 2 + here[3]) * W, W, 1)
     keep = call(branch_keep_kernel, [((n_y, tokens, W), BF16)], pos, mixed, blender, scalars=1)
-    send, own_skip, keep = lax.optimization_barrier((swap_cores(send), own_skip, keep))
+    near = hold(weights[1])
+    send, keep, near = lax.optimization_barrier((swap_cores(send), keep, near))
     branch = (keep.astype(F32) + send.astype(F32)).astype(BF16)
-    branch, weights[1], weights[2] = lax.optimization_barrier((branch, weights[1], weights[2]))
     parts = exchange(branch, "y")
-    parts, weights[1] = lax.optimization_barrier((parts, weights[1]))
-    weights.append(lax.ppermute(weights[1], TP, ring))
     hidden, outgoing = call(
         dispatch_kernel,
         [((tokens, W), F32), ((n_z, n_y, n_x, 8, W), BF16)],
         pos,
         parts,
-        own_skip,
+        skip,
         norm_gain[None],
         hot,
         scalars=1,
@@ -540,6 +577,7 @@
     own = exchange(outgoing.reshape(n_z * n_x * n_y, 8, W), ("z", "y", "x"))
     own = own.reshape(n_z, n_y, n_x, 8, W)
     gains = norm_gain[None]
+    weights[1] = near
     acts, squares = call(
         expert_own_kernel,
         [((4, tokens, 2 * W), F32), ((tokens, W), F32)],

time: 189 us -> 195 us (1.032)
  blocking collectives: 126 us -> 110 us
  waiting for transfers between devices: 3.8 us -> 14.6 us
  starting transfers between devices: 29.8 us -> 36.6 us
  local copies, waits for them, and re-layouts: 1.57 us -> 3.8 us
    all_to_all x5 -> x4, blocking collectives: 126 us -> 110 us  [exchange(): return lax.all_to_all(parts, axes, split_axis=0, concat_axis=0, tiled=True)]
    all_to_all x1 -> x2, waiting for transfers between devices: 3.67 us -> 14.5 us  [exchange(): return lax.all_to_all(parts, axes, split_axis=0, concat_axis=0, tiled=True)]
    all_to_all x1 -> x2, starting transfers between devices: 4.02 us -> 8.18 us  [exchange(): return lax.all_to_all(parts, axes, split_axis=0, concat_axis=0, tiled=True)]
    pallas_call x0 -> x2, Pallas kernels: none -> 3.78 us  [the longest x1 2.36 us: body(): pl.pallas_call(pack_kernel, name='pack', out_shape=jax.ShapeDtypeStruct((...]
    unnamed x18 -> x24, local copies, waits for them, and re-layouts: 0.72 us -> 3.8 us
    pallas_call x12 -> x11, Pallas kernels: 23.4 us -> 21.3 us  [call(): pl.pallas_call(kernel, out_shape=shapes if len(shapes) > 1 else shapes[0]...]
    ppermute x4, starting transfers between devices: 16 us -> 18 us  [swap_cores(): return lax.ppermute(data, 'c', [(0, 1), (1, 0)])]
  transfers between devices with their start and end apart: 8 -> 9, of which waited for: 2 -> 3; matrix products, arithmetic and copies ran while one was open for 1% -> 0% of each run, Pallas kernels for 10% -> 9%
where the time goes in v6:
time: 195 us; the launch traced here: 194 us
  blocking collectives  110 us (56%)
  starting transfers between devices  36.6 us (19%)
  Pallas kernels  27.9 us (14%)
  waiting for transfers between devices  14.6 us (7%)
  local copies, waits for them, and re-layouts  3.8 us (2%)
    all_to_all x4, blocking collectives, exchange(): return lax.all_to_all(parts, axes, split_axis=0, concat_axis=0, tiled=True)  110 us
    pallas_call x11, Pallas kernels, call(): pl.pallas_call(kernel, out_shape=shapes if len(shapes) > 1 else shapes[0]...  21.3 us
    ppermute x4, starting transfers between devices, swap_cores(): return lax.ppermute(data, 'c', [(0, 1), (1, 0)])  18 us
    all_to_all x2, waiting for transfers between devices, exchange(): return lax.all_to_all(parts, axes, split_axis=0, concat_axis=0, tiled=True)  14.5 us
    all_to_all x2, starting transfers between devices, exchange(): return lax.all_to_all(parts, axes, split_axis=0, concat_axis=0, tiled=True)  8.18 us
    ppermute x1, starting transfers between devices, body(): weights.append(lax.ppermute(weights[0], TP, back))  4.47 us
    ppermute x1, starting transfers between devices, body(): weights.append(lax.ppermute(weights[-1], TP, ring))  4.02 us
  transfers between devices with their start and end apart: 9, of which 3 were waited for; matrix products, arithmetic and copies ran while one was open for 0% of the time, Pallas kernels for 9%

profile of v6, /device:TPU:1, one launch (start us, length us, event | category | flops | bytes accessed | tf_op | source)
XLA Modules:
  0.0 194.1 jit_solution(16422710704049292122)
XLA Ops:
  0.0 2.4 %pack.1.w0 = bf16[6144,128]{1,0:T(8,128)(2,1)} custom-call(bf16[1,2048,128]{2,1,0:T(8,128)(2,1)} %switch_ref.1, bf16[1,2048,128]{2,1,0:T(8,128)(2,1)} %expansion_ref.1, bf16[1,128,2048]{2,1,0:T(8,128)(2,1)} %contraction_ref.1), custom_call_target="tpu_custom_call" | custom-call | tf_op jit(solution)/shard_map/pack/pallas_call | solution.py:507
  2.4 4.0 %collective-permute-start = (bf16[6144,128]{1,0:T(8,128)(2,1)}, bf16[6144,128]{1,0:T(8,128)(2,1)}, u32[]{:S(2)}, u32[]{:S(2)}) collective-permute-start(bf16[6144,128]{1,0:T(8,128)(2,1)} %pack.1.w0), channel_id=1, source_target_pairs={{2,0},{4,2},{6,4},{8,6},{10,8},{12,10},{14,12},{0,14},{15,1},{1,3}... | collective-permute-start | bytes 4718600 | tf_op jit(solution)/shard_map/ppermute | solution.py:521
  6.4 6.4 %shard_map.154 = (bf16[4,128,128]{2,1,0:T(8,128)(2,1)}, f32[256,128]{1,0:T(8,128)}, f32[256,128]{1,0:T(8,128)}) custom-call(bf16[256,128]{1,0:T(8,128)(2,1)} %refs_0_.1, bf16[256,128]{1,0:T(8,128)(2,1)} %refs_1_.1, bf16[256,128]{1,0:T(8,128)(2,1)} %refs_2_.1, bf16[256,128]{1,0:T(8,128)(2,1)} %refs_3_.1, f32[256,128]{1,0:T(8,128)} %refs_4_.1, f32[2,256]{1,0:T(2,128)} %bitcast.26), custom_call_target="tpu_custom_call" | custom-call | flops 2000000000 | bytes 1000000 | tf_op jit(solution)/shard_map/pallas_call | solution.py:458
  12.8 4.0 %all-to-all-start = ((bf16[4,128,128]{2,1,0:T(8,128)(2,1)}), bf16[4,128,128]{2,1,0:T(8,128)(2,1)S(1)}, u32[]{:S(2)}, u32[]{:S(2)}) async-start(bf16[4,128,128]{2,1,0:T(8,128)(2,1)} %get-tuple-element.35), calls=%async_computation | async-start | bytes 262144 | tf_op jit(solution)/shard_map/all_to_all | solution.py:474
  16.8 0.7 copy-done.4
  17.9 0.8 copy-done.8
  18.8 2.9 %all-to-all-done.got_ref = bf16[4,128,128]{2,1,0:T(8,128)(2,1)S(1)} async-done(((bf16[4,128,128]{2,1,0:T(8,128)(2,1)}), bf16[4,128,128]{2,1,0:T(8,128)(2,1)S(1)}, u32[]{:S(2)}, u32[]{:S(2)}) %all-to-all-start) | async-done | bytes 131104 | tf_op jit(solution)/shard_map/all_to_all | solution.py:474
  21.7 1.0 shard_map.156
  22.7 19.3 %all_to_all.30.got_ref = bf16[8,128,128]{2,1,0:T(8,128)(2,1)S(1)} all-to-all(bf16[8,128,128]{2,1,0:T(8,128)(2,1)S(1)} %get-tuple-element.38), channel_id=1, replica_groups=mesh['z'=8,'x'=4,'y'=8,'c'=2] {'z'}, dimensions={0} | all-to-all | bytes 524288 | tf_op jit(solution)/shard_map/all_to_all | solution.py:474
  42.0 2.4 %shard_map.157 = (bf16[8,256,128]{2,1,0:T(8,128)(2,1)S(1)}, bf16[256,128]{1,0:T(8,128)(2,1)S(1)}) custom-call(s32[4]{0:T(128)S(1)} %pad_add_fusion.pos_ref, bf16[8,128,128]{2,1,0:T(8,128)(2,1)S(1)} %all_to_all.30.got_ref, f32[256,128]{1,0:T(8,128)S(1)} %get-tuple-element.40.prefix_ref, f32[256,128]{1,0:T(8,128)S(1)} %copy-done.10, ...), custom_call_target="tpu_custom_call" | custom-call | flops 2000000000 | bytes 1000000 | tf_op jit(solution)/shard_map/pallas_call | solution.py:458
  44.4 7.5 %collective-permute-start.1 = (bf16[8,256,128]{2,1,0:T(8,128)(2,1)S(1)}, bf16[8,256,128]{2,1,0:T(8,128)(2,1)S(1)}, u32[]{:S(2)}, u32[]{:S(2)}) collective-permute-start(bf16[8,256,128]{2,1,0:T(8,128)(2,1)S(1)} %get-tuple-element.43), channel_id=1, source_target_pairs={{0,1},{1,0},{2,3},{3,2},{4,5},{5,4},{6,7},{7,6},{8,9},{9,8},{10,11... | collective-permute-start | bytes 1572872 | tf_op jit(solution)/shard_map/ppermute | solution.py:478
  51.9 1.4 hold.1.w1
  53.3 0.9 shard_map.158
  54.2 0.9 add_convert_fusion.1
  55.2 4.2 %all-to-all-start.2 = ((bf16[8,256,128]{2,1,0:T(8,128)(2,1)}), bf16[8,256,128]{2,1,0:T(8,128)(2,1)}, u32[]{:S(2)}, u32[]{:S(2)}) async-start(bf16[8,256,128]{2,1,0:T(8,128)(2,1)} %add_convert_fusion.1), calls=%async_computation.2 | async-start | bytes 1048576 | tf_op jit(solution)/shard_map/all_to_all | solution.py:474
  59.3 4.5 %collective-permute-start.3 = (bf16[6144,128]{1,0:T(8,128)(2,1)S(1)}, bf16[6144,128]{1,0:T(8,128)(2,1)}, u32[]{:S(2)}, u32[]{:S(2)}) collective-permute-start(bf16[6144,128]{1,0:T(8,128)(2,1)S(1)} %copy-done), channel_id=1, source_target_pairs={{0,2},{2,4},{4,6},{6,8},{8,10},{10,12},{12,14},{14,0},{1,15},{3,1}... | collective-permute-start | bytes 4718600 | tf_op jit(solution)/shard_map/ppermute | solution.py:541
  63.8 1.9 collective-permute-start.4
  65.8 11.6 %all-to-all-done.2.parts_ref = bf16[8,256,128]{2,1,0:T(8,128)(2,1)} async-done(((bf16[8,256,128]{2,1,0:T(8,128)(2,1)}), bf16[8,256,128]{2,1,0:T(8,128)(2,1)}, u32[]{:S(2)}, u32[]{:S(2)}) %all-to-all-start.2) | async-done | bytes 524320 | tf_op jit(solution)/shard_map/all_to_all | solution.py:474
  77.4 1.2 copy-done.2
  78.6 1.0 copy-done.9
  79.6 1.4 shard_map.159
  81.0 40.7 %all_to_all.31 = bf16[256,8,128]{2,1,0:T(8,128)(2,1)S(1)} all-to-all(bf16[256,8,128]{2,1,0:T(8,128)(2,1)S(1)} %bitcast.17), channel_id=1, replica_groups=mesh['z'=8,'x'=4,'y'=8,'c'=2] {'z','y','x'}, dimensions={0} | all-to-all | bytes 1048576 | tf_op jit(solution)/shard_map/all_to_all | solution.py:474
  121.7 2.8 %collective-permute-start.2 = (bf16[8,8,4,8,128]{4,3,2,1,0:T(8,128)(2,1)S(1)}, bf16[8,8,4,8,128]{4,3,2,1,0:T(8,128)(2,1)S(1)}, u32[]{:S(2)}, u32[]{:S(2)}) collective-permute-start(bf16[8,8,4,8,128]{4,3,2,1,0:T(8,128)(2,1)S(1)} %bitcast.14), channel_id=1, source_target_pairs={{0,1},{1,0},{2,3},{3,2},{4,5},{5,4},{6,7},{7,6},{8,9},{9,8},{10,11... | collective-permute-start | bytes 1572872 | tf_op jit(solution)/shard_map/ppermute | solution.py:478
  124.5 2.6 %shard_map.160 = (f32[4,256,256]{2,1,0:T(8,128)S(1)}, f32[256,128]{1,0:T(8,128)S(1)}) custom-call(s32[4]{0:T(128)S(1)} %pad_add_fusion.pos_ref, bf16[8,8,4,8,128]{4,3,2,1,0:T(8,128)(2,1)S(1)} %bitcast.15, f32[1,2048]{1,0:T(1,128)S(1)} %bitcast.19, bf16[6144,128]{1,0:T(8,128)(2,1)S(1)} %copy-done, bf16[6144,128]{1,0:T(8,128)(2,1)S(1)} %hold.1.w1, ...), custom_call_target="tpu_custom_call" | custom-call | flops 2000000000 | bytes 1000000 | tf_op jit(solution)/shard_map/pallas_call | solution.py:458
  127.2 2.9 %shard_map.161 = (bf16[8,8,4,8,128]{4,3,2,1,0:T(8,128)(2,1)S(1)}, bf16[256,512]{1,0:T(8,128)(2,1)S(1)}) custom-call(s32[4]{0:T(128)S(1)} %pad_add_fusion.pos_ref, bf16[8,8,4,8,128]{4,3,2,1,0:T(8,128)(2,1)S(1)} %collective-permute-done.2.other_ref, f32[1,2048]{1,0:T(1,128)S(1)} %bitcast.20, f32[4,256,256]{2,1,0:T(8,128)S(1)} %get-tuple-element.53.act_ref, ...), custom_call_target="tpu_custom_call" | custom-call | flops 2000000000 | bytes 1000000 | tf_op jit(solution)/shard_map/pallas_call | solution.py:458
  130.1 1.9 collective-permute-start.5
  132.6 2.3 %shard_map.162 = bf16[8,8,4,8,128]{4,3,2,1,0:T(8,128)(2,1)S(1)} custom-call(s32[4]{0:T(128)S(1)} %pad_add_fusion.pos_ref, bf16[256,512]{1,0:T(8,128)(2,1)S(1)} %get-tuple-element.56.hidden_ref, bf16[6144,128]{1,0:T(8,128)(2,1)S(1)} %copy-done, bf16[6144,128]{1,0:T(8,128)(2,1)S(1)} %hold.1.w1, bf16[6144,128]{1,0:T(8,128)(2,1)} %collective-permute-done.3.w2, ...), custom_call_target="tpu_custom_call" | custom-call | flops 2000000000 | bytes 1000000 | tf_op jit(solution)/shard_map/pallas_call | solution.py:458
  135.2 31.4 %all_to_all.32 = bf16[256,8,128]{2,1,0:T(8,128)(2,1)S(1)} all-to-all(bf16[256,8,128]{2,1,0:T(8,128)(2,1)S(1)} %bitcast.25), channel_id=1, replica_groups=mesh['z'=8,'x'=4,'y'=8,'c'=2] {'z','y','x'}, dimensions={0} | all-to-all | bytes 1048576 | tf_op jit(solution)/shard_map/all_to_all | solution.py:474
  167.0 18.2 %all_to_all.33.own_ref = bf16[8,256,128]{2,1,0:T(8,128)(2,1)S(1)} all-to-all(bf16[8,256,128]{2,1,0:T(8,128)(2,1)S(1)} %shard_map.164), channel_id=1, replica_groups=mesh['z'=8,'x'=4,'y'=8,'c'=2] {'y'}, dimensions={0} | all-to-all | bytes 1048576 | tf_op jit(solution)/shard_map/all_to_all | solution.py:474
  185.2 5.8 %collective-permute-start.6 = (bf16[8,256,128]{2,1,0:T(8,128)(2,1)S(1)}, bf16[8,256,128]{2,1,0:T(8,128)(2,1)S(1)}, u32[]{:S(2)}, u32[]{:S(2)}) collective-permute-start(bf16[8,256,128]{2,1,0:T(8,128)(2,1)S(1)} %all_to_all.33.own_ref), channel_id=1, source_target_pairs={{0,1},{1,0},{2,3},{3,2},{4,5},{5,4},{6,7},{7,6},{8,9},{9,8},{10,11... | collective-permute-start | bytes 1572872 | tf_op jit(solution)/shard_map/ppermute | solution.py:478
  191.0 1.4 shard_map.165.half_ref
  192.5 1.4 shard_map.166
  (32 shorter events, 1.8 us)
Async XLA Ops:
  2.4 39.6 %collective-permute-start = (bf16[6144,128]{1,0:T(8,128)(2,1)}, bf16[6144,128]{1,0:T(8,128)(2,1)}, u32[]{:S(2)}, u32[]{:S(2)}) collective-permute-start(bf16[6144,128]{1,0:T(8,128)(2,1)} %pack.1.w0), channel_id=1, source_target_pairs={{2,0},{4,2},{6,4},{8,6},{10,8},{12,10},{14,12},{0,14},{15,1},{1,3}... | collective-permute-start | bytes 4718600 | tf_op jit(solution)/shard_map/ppermute | solution.py:521
  12.8 8.8 %all-to-all-start = ((bf16[4,128,128]{2,1,0:T(8,128)(2,1)}), bf16[4,128,128]{2,1,0:T(8,128)(2,1)S(1)}, u32[]{:S(2)}, u32[]{:S(2)}) async-start(bf16[4,128,128]{2,1,0:T(8,128)(2,1)} %get-tuple-element.35), calls=%async_computation | async-start | bytes 262144 | tf_op jit(solution)/shard_map/all_to_all | solution.py:474
  16.8 0.7 copy-start.4
  17.9 0.8 copy-start.8
  21.6 20.3 %copy-start.3 = (bf16[128,2048]{1,0:T(8,128)(2,1)S(1)}, bf16[128,2048]{1,0:T(8,128)(2,1)}, u32[]{:S(2)}) copy-start(bf16[128,2048]{1,0:T(8,128)(2,1)} %w_ref.3) | copy-start | bytes 1572868
  21.7 20.3 %copy-start.7 = (f32[128]{0:T(128)S(1)}, f32[128]{0:T(128)}, u32[]{:S(2)}) copy-start(f32[128]{0:T(128)} %param.22) | copy-start | bytes 1540
  21.7 20.3 %copy-start.10 = (f32[256,128]{1,0:T(8,128)S(1)}, f32[256,128]{1,0:T(8,128)}, u32[]{:S(2)}) copy-start(f32[256,128]{1,0:T(8,128)} %get-tuple-element.41.map_ref) | copy-start | bytes 393220
  21.7 20.4 %copy-start.11 = (f32[256,128]{1,0:T(8,128)S(1)}, f32[256,128]{1,0:T(8,128)}, u32[]{:S(2)}) copy-start(f32[256,128]{1,0:T(8,128)} %get-tuple-element.42.loc_ref) | copy-start | bytes 393220
  44.4 9.9 %collective-permute-start.1 = (bf16[8,256,128]{2,1,0:T(8,128)(2,1)S(1)}, bf16[8,256,128]{2,1,0:T(8,128)(2,1)S(1)}, u32[]{:S(2)}, u32[]{:S(2)}) collective-permute-start(bf16[8,256,128]{2,1,0:T(8,128)(2,1)S(1)} %get-tuple-element.43), channel_id=1, source_target_pairs={{0,1},{1,0},{2,3},{3,2},{4,5},{5,4},{6,7},{7,6},{8,9},{9,8},{10,11... | collective-permute-start | bytes 1572872 | tf_op jit(solution)/shard_map/ppermute | solution.py:478
  54.2 5.1 %copy-start = (bf16[6144,128]{1,0:T(8,128)(2,1)S(1)}, bf16[6144,128]{1,0:T(8,128)(2,1)}, u32[]{:S(2)}) copy-start(bf16[6144,128]{1,0:T(8,128)(2,1)} %pack.1.w0) | copy-start | bytes 4718596
  54.2 23.2 %copy-start.1 = (f32[2048]{0:T(1024)S(1)}, f32[2048]{0:T(1024)}, u32[]{:S(2)}) copy-start(f32[2048]{0:T(1024)} %param.25) | copy-start | bytes 24580
  55.2 22.2 %all-to-all-start.2 = ((bf16[8,256,128]{2,1,0:T(8,128)(2,1)}), bf16[8,256,128]{2,1,0:T(8,128)(2,1)}, u32[]{:S(2)}, u32[]{:S(2)}) async-start(bf16[8,256,128]{2,1,0:T(8,128)(2,1)} %add_convert_fusion.1), calls=%async_computation.2 | async-start | bytes 1048576 | tf_op jit(solution)/shard_map/all_to_all | solution.py:474
  59.3 65.1 %collective-permute-start.3 = (bf16[6144,128]{1,0:T(8,128)(2,1)S(1)}, bf16[6144,128]{1,0:T(8,128)(2,1)}, u32[]{:S(2)}, u32[]{:S(2)}) collective-permute-start(bf16[6144,128]{1,0:T(8,128)(2,1)S(1)} %copy-done), channel_id=1, source_target_pairs={{0,2},{2,4},{4,6},{6,8},{8,10},{10,12},{12,14},{14,0},{1,15},{3,1}... | collective-permute-start | bytes 4718600 | tf_op jit(solution)/shard_map/ppermute | solution.py:541
  63.8 60.7 %collective-permute-start.4 = (bf16[6144,128]{1,0:T(8,128)(2,1)}, bf16[6144,128]{1,0:T(8,128)(2,1)}, u32[]{:S(2)}, u32[]{:S(2)}) collective-permute-start(bf16[6144,128]{1,0:T(8,128)(2,1)} %collective-permute-done.far_ref), channel_id=1, source_target_pairs={{2,0},{4,2},{6,4},{8,6},{10,8},{12,10},{14,12},{0,14},{15,1},{1,3}... | collective-permute-start | bytes 4718600 | tf_op jit(solution)/shard_map/ppermute | solution.py:549
  77.4 1.2 copy-start.2
  78.6 1.0 copy-start.9
  121.7 5.4 %collective-permute-start.2 = (bf16[8,8,4,8,128]{4,3,2,1,0:T(8,128)(2,1)S(1)}, bf16[8,8,4,8,128]{4,3,2,1,0:T(8,128)(2,1)S(1)}, u32[]{:S(2)}, u32[]{:S(2)}) collective-permute-start(bf16[8,8,4,8,128]{4,3,2,1,0:T(8,128)(2,1)S(1)} %bitcast.14), channel_id=1, source_target_pairs={{0,1},{1,0},{2,3},{3,2},{4,5},{5,4},{6,7},{7,6},{8,9},{9,8},{10,11... | collective-permute-start | bytes 1572872 | tf_op jit(solution)/shard_map/ppermute | solution.py:478
  127.1 4.9 %copy-start.5 = (f32[256,2]{0,1:T(2,128)S(1)}, f32[256,2]{0,1:T(2,128)}, u32[]{:S(2)}) copy-start(f32[256,2]{0,1:T(2,128)} %param.27) | copy-start | bytes 6148
  127.2 4.9 %copy-start.6 = (f32[256]{0:T(256)S(1)}, f32[256]{0:T(256)}, u32[]{:S(2)}) copy-start(f32[256]{0:T(256)} %param.26) | copy-start | bytes 3076
  130.1 4.9 %collective-permute-start.5 = (bf16[8,8,4,8,128]{4,3,2,1,0:T(8,128)(2,1)S(1)}, bf16[8,8,4,8,128]{4,3,2,1,0:T(8,128)(2,1)S(1)}, u32[]{:S(2)}, u32[]{:S(2)}) collective-permute-start(bf16[8,8,4,8,128]{4,3,2,1,0:T(8,128)(2,1)S(1)} %get-tuple-element.55), channel_id=1, source_target_pairs={{0,1},{1,0},{2,3},{3,2},{4,5},{5,4},{6,7},{7,6},{8,9},{9,8},{10,11... | collective-permute-start | bytes 1572872 | tf_op jit(solution)/shard_map/ppermute | solution.py:478
  185.2 7.4 %collective-permute-start.6 = (bf16[8,256,128]{2,1,0:T(8,128)(2,1)S(1)}, bf16[8,256,128]{2,1,0:T(8,128)(2,1)S(1)}, u32[]{:S(2)}, u32[]{:S(2)}) collective-permute-start(bf16[8,256,128]{2,1,0:T(8,128)(2,1)S(1)} %all_to_all.33.own_ref), channel_id=1, source_target_pairs={{0,1},{1,0},{2,3},{3,2},{4,5},{5,4},{6,7},{7,6},{8,9},{9,8},{10,11... | collective-permute-start | bytes 1572872 | tf_op jit(solution)/shard_map/ppermute | solution.py:478

commit v7 on v6

--- a/solution.py
+++ b/solution.py
@@ -257,8 +257,9 @@
     prefix_ref[...] = prefix
 
 
-def readout_kernel(pos_ref, got_ref, prefix_ref, map_ref, loc_ref, gain_ref, w_ref, send_ref, mixed_ref):
+def readout_kernel(pos_ref, got_ref, prefix_ref, map_ref, loc_ref, gain_ref, w_ref, names_ref, send_ref, mixed_ref, hot_ref, slots_ref):
     mine, core = pos_ref[1], pos_ref[3]
+    route_kernel(names_ref, hot_ref, slots_ref)
     state = jnp.where(mine > 0, unpack(got_ref[0])[1], 0.0)
     for n in range(1, got_ref.shape[0] - 1):
         change, add = unpack(got_ref[n])
@@ -539,17 +540,20 @@
     )
     gathered = exchange(pairs, "x")
     weights.append(lax.ppermute(weights[0], TP, back))
-    hot, slots = call(route_kernel, [((4 * tokens, tokens), BF16), ((2, tokens), F32)], ids.T)
-    gathered, hot = lax.optimization_barrier((gathered, hot))
     pairs, prefix = call(
         compose_kernel, [((n_z, W, W), BF16), ((2 * W, W), F32)], pos, gathered, scalars=1
     )
     gathered = exchange(pairs, "z")
     gathered, weights[1] = lax.optimization_barrier((gathered, weights[1]))
     weights.append(lax.ppermute(weights[1], TP, ring))
-    send, mixed = call(
+    send, mixed, hot, slots = call(
         readout_kernel,
-        [((n_y, tokens, W), BF16), ((tokens, W), BF16)],
+        [
+            ((n_y, tokens, W), BF16),
+            ((tokens, W), BF16),
+            ((4 * tokens, tokens), BF16),
+            ((2, tokens), F32),
+        ],
         pos,
         gathered,
         prefix,
@@ -557,6 +561,7 @@
         local,
         head_gain[None],
         blender,
+        ids.T,
         scalars=1,
     )
     keep = call(branch_keep_kernel, [((n_y, tokens, W), BF16)], pos, mixed, blender, scalars=1)

time: 195 us -> 195 us (level)
    pallas_call x11 -> x10, Pallas kernels: 21.3 us -> 21.2 us  [call(): pl.pallas_call(kernel, out_shape=shapes if len(shapes) > 1 else shapes[0]...]
where the time goes in v7:
time: 195 us; the launch traced here: 194 us
  blocking collectives  110 us (56%)
  starting transfers between devices  36.6 us (19%)
  Pallas kernels  27.8 us (14%)
  waiting for transfers between devices  16.5 us (8%)
  local copies, waits for them, and re-layouts  2.31 us (1%)
    all_to_all x4, blocking collectives, exchange(): return lax.all_to_all(parts, axes, split_axis=0, concat_axis=0, tiled=True)  110 us
    pallas_call x10, Pallas kernels, call(): pl.pallas_call(kernel, out_shape=shapes if len(shapes) > 1 else shapes[0]...  21.2 us
    ppermute x4, starting transfers between devices, swap_cores(): return lax.ppermute(data, 'c', [(0, 1), (1, 0)])  18 us
    all_to_all x2, waiting for transfers between devices, exchange(): return lax.all_to_all(parts, axes, split_axis=0, concat_axis=0, tiled=True)  16.3 us
    all_to_all x2, starting transfers between devices, exchange(): return lax.all_to_all(parts, axes, split_axis=0, concat_axis=0, tiled=True)  8.17 us
    ppermute x1, starting transfers between devices, body(): weights.append(lax.ppermute(weights[0], TP, back))  4.47 us
    ppermute x1, starting transfers between devices, body(): weights.append(lax.ppermute(weights[-1], TP, ring))  4.02 us
  transfers between devices with their start and end apart: 9, of which 3 were waited for; matrix products, arithmetic and copies ran while one was open for 0% of the time, Pallas kernels for 9%

profile of v7, /device:TPU:1, one launch (start us, length us, event | category | flops | bytes accessed | tf_op | source)
XLA Modules:
  0.0 194.3 jit_solution(16948968078464058859)
XLA Ops:
  0.0 2.4 %pack.1.w0 = bf16[6144,128]{1,0:T(8,128)(2,1)} custom-call(bf16[1,2048,128]{2,1,0:T(8,128)(2,1)} %switch_ref.1, bf16[1,2048,128]{2,1,0:T(8,128)(2,1)} %expansion_ref.1, bf16[1,128,2048]{2,1,0:T(8,128)(2,1)} %contraction_ref.1), custom_call_target="tpu_custom_call" | custom-call | tf_op jit(solution)/shard_map/pack/pallas_call | solution.py:508
  2.4 4.0 %collective-permute-start = (bf16[6144,128]{1,0:T(8,128)(2,1)}, bf16[6144,128]{1,0:T(8,128)(2,1)}, u32[]{:S(2)}, u32[]{:S(2)}) collective-permute-start(bf16[6144,128]{1,0:T(8,128)(2,1)} %pack.1.w0), channel_id=1, source_target_pairs={{2,0},{4,2},{6,4},{8,6},{10,8},{12,10},{14,12},{0,14},{15,1},{1,3}... | collective-permute-start | bytes 4718600 | tf_op jit(solution)/shard_map/ppermute | solution.py:522
  6.4 6.4 %shard_map.154 = (bf16[4,128,128]{2,1,0:T(8,128)(2,1)}, f32[256,128]{1,0:T(8,128)}, f32[256,128]{1,0:T(8,128)}) custom-call(bf16[256,128]{1,0:T(8,128)(2,1)} %refs_0_.1, bf16[256,128]{1,0:T(8,128)(2,1)} %refs_1_.1, bf16[256,128]{1,0:T(8,128)(2,1)} %refs_2_.1, bf16[256,128]{1,0:T(8,128)(2,1)} %refs_3_.1, f32[256,128]{1,0:T(8,128)} %refs_4_.1, f32[2,256]{1,0:T(2,128)} %bitcast.26), custom_call_target="tpu_custom_call" | custom-call | flops 2000000000 | bytes 1000000 | tf_op jit(solution)/shard_map/pallas_call | solution.py:459
  12.8 4.0 %all-to-all-start = ((bf16[4,128,128]{2,1,0:T(8,128)(2,1)}), bf16[4,128,128]{2,1,0:T(8,128)(2,1)S(1)}, u32[]{:S(2)}, u32[]{:S(2)}) async-start(bf16[4,128,128]{2,1,0:T(8,128)(2,1)} %get-tuple-element.33), calls=%async_computation | async-start | bytes 262144 | tf_op jit(solution)/shard_map/all_to_all | solution.py:475
  16.9 4.7 %all-to-all-done.got_ref = bf16[4,128,128]{2,1,0:T(8,128)(2,1)S(1)} async-done(((bf16[4,128,128]{2,1,0:T(8,128)(2,1)}), bf16[4,128,128]{2,1,0:T(8,128)(2,1)S(1)}, u32[]{:S(2)}, u32[]{:S(2)}) %all-to-all-start) | async-done | bytes 131104 | tf_op jit(solution)/shard_map/all_to_all | solution.py:475
  21.7 1.0 shard_map.155
  22.7 19.3 %all_to_all.30.got_ref = bf16[8,128,128]{2,1,0:T(8,128)(2,1)S(1)} all-to-all(bf16[8,128,128]{2,1,0:T(8,128)(2,1)S(1)} %get-tuple-element.34), channel_id=1, replica_groups=mesh['z'=8,'x'=4,'y'=8,'c'=2] {'z'}, dimensions={0} | all-to-all | bytes 524288 | tf_op jit(solution)/shard_map/all_to_all | solution.py:475
  42.0 2.6 %shard_map.156 = (bf16[8,256,128]{2,1,0:T(8,128)(2,1)S(1)}, bf16[256,128]{1,0:T(8,128)(2,1)S(1)}, bf16[1024,256]{1,0:T(8,128)(2,1)S(1)}, f32[2,256]{1,0:T(2,128)S(1)}) custom-call(s32[4]{0:T(128)S(1)} %pad_add_fusion.pos_ref, bf16[8,128,128]{2,1,0:T(8,128)(2,1)S(1)} %all_to_all.30.got_ref, f32[256,128]{1,0:T(8,128)S(1)} %get-tuple-element.36.prefix_ref, ...), custom_call_target="tpu_custom_call" | custom-call | flops 2000000000 | bytes 1000000 | tf_op jit(solution)/shard_map/pallas_call | solution.py:459
  44.6 7.5 %collective-permute-start.1 = (bf16[8,256,128]{2,1,0:T(8,128)(2,1)S(1)}, bf16[8,256,128]{2,1,0:T(8,128)(2,1)S(1)}, u32[]{:S(2)}, u32[]{:S(2)}) collective-permute-start(bf16[8,256,128]{2,1,0:T(8,128)(2,1)S(1)} %get-tuple-element.39), channel_id=1, source_target_pairs={{0,1},{1,0},{2,3},{3,2},{4,5},{5,4},{6,7},{7,6},{8,9},{9,8},{10,11... | collective-permute-start | bytes 1572872 | tf_op jit(solution)/shard_map/ppermute | solution.py:479
  52.2 1.4 hold.1.w1
  53.6 0.9 shard_map.157
  54.5 0.9 add_convert_fusion.1
  55.4 4.1 %all-to-all-start.2 = ((bf16[8,256,128]{2,1,0:T(8,128)(2,1)}), bf16[8,256,128]{2,1,0:T(8,128)(2,1)}, u32[]{:S(2)}, u32[]{:S(2)}) async-start(bf16[8,256,128]{2,1,0:T(8,128)(2,1)} %add_convert_fusion.1), calls=%async_computation.2 | async-start | bytes 1048576 | tf_op jit(solution)/shard_map/all_to_all | solution.py:475
  59.6 4.5 %collective-permute-start.3 = (bf16[6144,128]{1,0:T(8,128)(2,1)S(1)}, bf16[6144,128]{1,0:T(8,128)(2,1)}, u32[]{:S(2)}, u32[]{:S(2)}) collective-permute-start(bf16[6144,128]{1,0:T(8,128)(2,1)S(1)} %copy-done), channel_id=1, source_target_pairs={{0,2},{2,4},{4,6},{6,8},{8,10},{10,12},{12,14},{14,0},{1,15},{3,1}... | collective-permute-start | bytes 4718600 | tf_op jit(solution)/shard_map/ppermute | solution.py:542
  64.1 1.9 collective-permute-start.4
  66.0 11.6 %all-to-all-done.2.parts_ref = bf16[8,256,128]{2,1,0:T(8,128)(2,1)} async-done(((bf16[8,256,128]{2,1,0:T(8,128)(2,1)}), bf16[8,256,128]{2,1,0:T(8,128)(2,1)}, u32[]{:S(2)}, u32[]{:S(2)}) %all-to-all-start.2) | async-done | bytes 524320 | tf_op jit(solution)/shard_map/all_to_all | solution.py:475
  77.6 1.2 copy-done.2
  78.8 1.0 copy-done.9
  79.9 1.4 shard_map.158
  81.3 40.7 %all_to_all.31 = bf16[256,8,128]{2,1,0:T(8,128)(2,1)S(1)} all-to-all(bf16[256,8,128]{2,1,0:T(8,128)(2,1)S(1)} %bitcast.17), channel_id=1, replica_groups=mesh['z'=8,'x'=4,'y'=8,'c'=2] {'z','y','x'}, dimensions={0} | all-to-all | bytes 1048576 | tf_op jit(solution)/shard_map/all_to_all | solution.py:475
  122.0 2.8 %collective-permute-start.2 = (bf16[8,8,4,8,128]{4,3,2,1,0:T(8,128)(2,1)S(1)}, bf16[8,8,4,8,128]{4,3,2,1,0:T(8,128)(2,1)S(1)}, u32[]{:S(2)}, u32[]{:S(2)}) collective-permute-start(bf16[8,8,4,8,128]{4,3,2,1,0:T(8,128)(2,1)S(1)} %bitcast.14), channel_id=1, source_target_pairs={{0,1},{1,0},{2,3},{3,2},{4,5},{5,4},{6,7},{7,6},{8,9},{9,8},{10,11... | collective-permute-start | bytes 1572872 | tf_op jit(solution)/shard_map/ppermute | solution.py:479
  124.8 2.6 %shard_map.159 = (f32[4,256,256]{2,1,0:T(8,128)S(1)}, f32[256,128]{1,0:T(8,128)S(1)}) custom-call(s32[4]{0:T(128)S(1)} %pad_add_fusion.pos_ref, bf16[8,8,4,8,128]{4,3,2,1,0:T(8,128)(2,1)S(1)} %bitcast.15, f32[1,2048]{1,0:T(1,128)S(1)} %bitcast.19, bf16[6144,128]{1,0:T(8,128)(2,1)S(1)} %copy-done, bf16[6144,128]{1,0:T(8,128)(2,1)S(1)} %hold.1.w1, ...), custom_call_target="tpu_custom_call" | custom-call | flops 2000000000 | bytes 1000000 | tf_op jit(solution)/shard_map/pallas_call | solution.py:459
  127.5 3.0 %shard_map.160 = (bf16[8,8,4,8,128]{4,3,2,1,0:T(8,128)(2,1)S(1)}, bf16[256,512]{1,0:T(8,128)(2,1)S(1)}) custom-call(s32[4]{0:T(128)S(1)} %pad_add_fusion.pos_ref, bf16[8,8,4,8,128]{4,3,2,1,0:T(8,128)(2,1)S(1)} %collective-permute-done.2.other_ref, f32[1,2048]{1,0:T(1,128)S(1)} %bitcast.20, f32[4,256,256]{2,1,0:T(8,128)S(1)} %get-tuple-element.49.act_ref, ...), custom_call_target="tpu_custom_call" | custom-call | flops 2000000000 | bytes 1000000 | tf_op jit(solution)/shard_map/pallas_call | solution.py:459
  130.4 1.9 collective-permute-start.5
  132.4 0.6 shard_map.162
  132.9 2.3 %shard_map.161 = bf16[8,8,4,8,128]{4,3,2,1,0:T(8,128)(2,1)S(1)} custom-call(s32[4]{0:T(128)S(1)} %pad_add_fusion.pos_ref, bf16[256,512]{1,0:T(8,128)(2,1)S(1)} %get-tuple-element.52.hidden_ref, bf16[6144,128]{1,0:T(8,128)(2,1)S(1)} %copy-done, bf16[6144,128]{1,0:T(8,128)(2,1)S(1)} %hold.1.w1, bf16[6144,128]{1,0:T(8,128)(2,1)} %collective-permute-done.3.w2, ...), custom_call_target="tpu_custom_call" | custom-call | flops 2000000000 | bytes 1000000 | tf_op jit(solution)/shard_map/pallas_call | solution.py:459
  135.4 31.4 %all_to_all.32 = bf16[256,8,128]{2,1,0:T(8,128)(2,1)S(1)} all-to-all(bf16[256,8,128]{2,1,0:T(8,128)(2,1)S(1)} %bitcast.25), channel_id=1, replica_groups=mesh['z'=8,'x'=4,'y'=8,'c'=2] {'z','y','x'}, dimensions={0} | all-to-all | bytes 1048576 | tf_op jit(solution)/shard_map/all_to_all | solution.py:475
  166.8 0.4 shard_map.163
  167.2 18.2 %all_to_all.33.own_ref = bf16[8,256,128]{2,1,0:T(8,128)(2,1)S(1)} all-to-all(bf16[8,256,128]{2,1,0:T(8,128)(2,1)S(1)} %shard_map.163), channel_id=1, replica_groups=mesh['z'=8,'x'=4,'y'=8,'c'=2] {'y'}, dimensions={0} | all-to-all | bytes 1048576 | tf_op jit(solution)/shard_map/all_to_all | solution.py:475
  185.4 5.8 %collective-permute-start.6 = (bf16[8,256,128]{2,1,0:T(8,128)(2,1)S(1)}, bf16[8,256,128]{2,1,0:T(8,128)(2,1)S(1)}, u32[]{:S(2)}, u32[]{:S(2)}) collective-permute-start(bf16[8,256,128]{2,1,0:T(8,128)(2,1)S(1)} %all_to_all.33.own_ref), channel_id=1, source_target_pairs={{0,1},{1,0},{2,3},{3,2},{4,5},{5,4},{6,7},{7,6},{8,9},{9,8},{10,11... | collective-permute-start | bytes 1572872 | tf_op jit(solution)/shard_map/ppermute | solution.py:479
  191.3 1.4 shard_map.164.half_ref
  192.8 1.4 shard_map.165
  (31 shorter events, 0.4 us)
Async XLA Ops:
  2.4 39.6 %collective-permute-start = (bf16[6144,128]{1,0:T(8,128)(2,1)}, bf16[6144,128]{1,0:T(8,128)(2,1)}, u32[]{:S(2)}, u32[]{:S(2)}) collective-permute-start(bf16[6144,128]{1,0:T(8,128)(2,1)} %pack.1.w0), channel_id=1, source_target_pairs={{2,0},{4,2},{6,4},{8,6},{10,8},{12,10},{14,12},{0,14},{15,1},{1,3}... | collective-permute-start | bytes 4718600 | tf_op jit(solution)/shard_map/ppermute | solution.py:522
  12.8 8.9 %all-to-all-start = ((bf16[4,128,128]{2,1,0:T(8,128)(2,1)}), bf16[4,128,128]{2,1,0:T(8,128)(2,1)S(1)}, u32[]{:S(2)}, u32[]{:S(2)}) async-start(bf16[4,128,128]{2,1,0:T(8,128)(2,1)} %get-tuple-element.33), calls=%async_computation | async-start | bytes 262144 | tf_op jit(solution)/shard_map/all_to_all | solution.py:475
  16.9 25.1 %copy-start.3 = (bf16[128,2048]{1,0:T(8,128)(2,1)S(1)}, bf16[128,2048]{1,0:T(8,128)(2,1)}, u32[]{:S(2)}) copy-start(bf16[128,2048]{1,0:T(8,128)(2,1)} %w_ref.3) | copy-start | bytes 1572868
  16.9 25.1 %copy-start.4 = (s32[256,2]{0,1:T(2,128)S(1)}, s32[256,2]{0,1:T(2,128)}, u32[]{:S(2)}) copy-start(s32[256,2]{0,1:T(2,128)} %param.28) | copy-start | bytes 6148
  16.9 25.1 %copy-start.7 = (f32[128]{0:T(128)S(1)}, f32[128]{0:T(128)}, u32[]{:S(2)}) copy-start(f32[128]{0:T(128)} %param.22) | copy-start | bytes 1540
  16.9 25.1 %copy-start.10 = (f32[256,128]{1,0:T(8,128)S(1)}, f32[256,128]{1,0:T(8,128)}, u32[]{:S(2)}) copy-start(f32[256,128]{1,0:T(8,128)} %get-tuple-element.37.map_ref) | copy-start | bytes 393220
  16.9 25.1 %copy-start.11 = (f32[256,128]{1,0:T(8,128)S(1)}, f32[256,128]{1,0:T(8,128)}, u32[]{:S(2)}) copy-start(f32[256,128]{1,0:T(8,128)} %get-tuple-element.38.loc_ref) | copy-start | bytes 393220
  44.6 9.0 %copy-start.8 = (bf16[1024,256]{1,0:T(8,128)(2,1)}, bf16[1024,256]{1,0:T(8,128)(2,1)S(1)}, u32[]{:S(2)}) copy-start(bf16[1024,256]{1,0:T(8,128)(2,1)S(1)} %get-tuple-element.44.hot_ref) | copy-start | bytes 1572868
  44.6 9.9 %collective-permute-start.1 = (bf16[8,256,128]{2,1,0:T(8,128)(2,1)S(1)}, bf16[8,256,128]{2,1,0:T(8,128)(2,1)S(1)}, u32[]{:S(2)}, u32[]{:S(2)}) collective-permute-start(bf16[8,256,128]{2,1,0:T(8,128)(2,1)S(1)} %get-tuple-element.39), channel_id=1, source_target_pairs={{0,1},{1,0},{2,3},{3,2},{4,5},{5,4},{6,7},{7,6},{8,9},{9,8},{10,11... | collective-permute-start | bytes 1572872 | tf_op jit(solution)/shard_map/ppermute | solution.py:479
  54.5 5.1 %copy-start = (bf16[6144,128]{1,0:T(8,128)(2,1)S(1)}, bf16[6144,128]{1,0:T(8,128)(2,1)}, u32[]{:S(2)}) copy-start(bf16[6144,128]{1,0:T(8,128)(2,1)} %pack.1.w0) | copy-start | bytes 4718596
  54.5 23.1 %copy-start.1 = (f32[2048]{0:T(1024)S(1)}, f32[2048]{0:T(1024)}, u32[]{:S(2)}) copy-start(f32[2048]{0:T(1024)} %param.25) | copy-start | bytes 24580
  55.4 22.2 %all-to-all-start.2 = ((bf16[8,256,128]{2,1,0:T(8,128)(2,1)}), bf16[8,256,128]{2,1,0:T(8,128)(2,1)}, u32[]{:S(2)}, u32[]{:S(2)}) async-start(bf16[8,256,128]{2,1,0:T(8,128)(2,1)} %add_convert_fusion.1), calls=%async_computation.2 | async-start | bytes 1048576 | tf_op jit(solution)/shard_map/all_to_all | solution.py:475
  59.6 65.2 %collective-permute-start.3 = (bf16[6144,128]{1,0:T(8,128)(2,1)S(1)}, bf16[6144,128]{1,0:T(8,128)(2,1)}, u32[]{:S(2)}, u32[]{:S(2)}) collective-permute-start(bf16[6144,128]{1,0:T(8,128)(2,1)S(1)} %copy-done), channel_id=1, source_target_pairs={{0,2},{2,4},{4,6},{6,8},{8,10},{10,12},{12,14},{14,0},{1,15},{3,1}... | collective-permute-start | bytes 4718600 | tf_op jit(solution)/shard_map/ppermute | solution.py:542
  64.1 60.7 %collective-permute-start.4 = (bf16[6144,128]{1,0:T(8,128)(2,1)}, bf16[6144,128]{1,0:T(8,128)(2,1)}, u32[]{:S(2)}, u32[]{:S(2)}) collective-permute-start(bf16[6144,128]{1,0:T(8,128)(2,1)} %collective-permute-done.far_ref), channel_id=1, source_target_pairs={{2,0},{4,2},{6,4},{8,6},{10,8},{12,10},{14,12},{0,14},{15,1},{1,3}... | collective-permute-start | bytes 4718600 | tf_op jit(solution)/shard_map/ppermute | solution.py:548
  77.6 1.2 copy-start.2
  78.8 1.0 copy-start.9
  122.0 5.4 %collective-permute-start.2 = (bf16[8,8,4,8,128]{4,3,2,1,0:T(8,128)(2,1)S(1)}, bf16[8,8,4,8,128]{4,3,2,1,0:T(8,128)(2,1)S(1)}, u32[]{:S(2)}, u32[]{:S(2)}) collective-permute-start(bf16[8,8,4,8,128]{4,3,2,1,0:T(8,128)(2,1)S(1)} %bitcast.14), channel_id=1, source_target_pairs={{0,1},{1,0},{2,3},{3,2},{4,5},{5,4},{6,7},{7,6},{8,9},{9,8},{10,11... | collective-permute-start | bytes 1572872 | tf_op jit(solution)/shard_map/ppermute | solution.py:479
  127.4 4.9 %copy-start.5 = (f32[256,2]{0,1:T(2,128)S(1)}, f32[256,2]{0,1:T(2,128)}, u32[]{:S(2)}) copy-start(f32[256,2]{0,1:T(2,128)} %param.27) | copy-start | bytes 6148
  127.4 4.9 %copy-start.6 = (f32[256]{0:T(256)S(1)}, f32[256]{0:T(256)}, u32[]{:S(2)}) copy-start(f32[256]{0:T(256)} %param.26) | copy-start | bytes 3076
  130.4 4.9 %collective-permute-start.5 = (bf16[8,8,4,8,128]{4,3,2,1,0:T(8,128)(2,1)S(1)}, bf16[8,8,4,8,128]{4,3,2,1,0:T(8,128)(2,1)S(1)}, u32[]{:S(2)}, u32[]{:S(2)}) collective-permute-start(bf16[8,8,4,8,128]{4,3,2,1,0:T(8,128)(2,1)S(1)} %get-tuple-element.51), channel_id=1, source_target_pairs={{0,1},{1,0},{2,3},{3,2},{4,5},{5,4},{6,7},{7,6},{8,9},{9,8},{10,11... | collective-permute-start | bytes 1572872 | tf_op jit(solution)/shard_map/ppermute | solution.py:479
  185.4 7.4 %collective-permute-start.6 = (bf16[8,256,128]{2,1,0:T(8,128)(2,1)S(1)}, bf16[8,256,128]{2,1,0:T(8,128)(2,1)S(1)}, u32[]{:S(2)}, u32[]{:S(2)}) collective-permute-start(bf16[8,256,128]{2,1,0:T(8,128)(2,1)S(1)} %all_to_all.33.own_ref), channel_id=1, source_target_pairs={{0,1},{1,0},{2,3},{3,2},{4,5},{5,4},{6,7},{7,6},{8,9},{9,8},{10,11... | collective-permute-start | bytes 1572872 | tf_op jit(solution)/shard_map/ppermute | solution.py:479

commit v8 on v7

--- a/solution.py
+++ b/solution.py
@@ -31,6 +31,10 @@
     return dot(a_high, b_high, contract) + (
         dot(a_high, b_low, contract) + dot(a_low, b_high, contract)
     )
+
+
+def mm_one(a, b, contract=((1,), (0,))):
+    return dot(a.astype(BF16), b.astype(BF16), contract)
 
 
 def mm_exact(a, b, contract=((1,), (0,))):
@@ -213,15 +217,15 @@
             mm(jnp.concatenate([carried, p["value"]], axis=0), p["bar"], ((0,), (0,)))
         )
         locals_.append(
-            flat_heads(mm(p["read"], jnp.concatenate([carried, p["value"]], axis=0)))
-        )
-        reads.append(flat_heads(p["asked"] + mm(p["read_remove"], absorb)))
+            flat_heads(mm_one(p["read"], jnp.concatenate([carried, p["value"]], axis=0)))
+        )
+        reads.append(flat_heads(p["asked"] + mm_one(p["read_remove"], absorb)))
     map_ref[:SEG, :] = reads[0]
     loc_ref[:SEG, :] = locals_[0]
     run = jnp.concatenate([keeps[0], adds[0]], axis=0)
     for n in range(1, chunks):
         at = slice(n * SEG, (n + 1) * SEG)
-        both = mm(reads[n], run, ((1,), (1,)))
+        both = mm_one(reads[n], run, ((1,), (1,)))
         map_ref[at, :] = both[:, :W]
         loc_ref[at, :] = locals_[n] + both[:, W:]
         run = mm(run, keeps[n])

time: 195 us -> 195 us (level)
  no operation moved by 1% of the time
where the time goes in v8:
time: 195 us; the launch traced here: 194 us
  blocking collectives  110 us (56%)
  starting transfers between devices  36.6 us (19%)
  Pallas kernels  27.6 us (14%)
  waiting for transfers between devices  16.5 us (8%)
  local copies, waits for them, and re-layouts  2.31 us (1%)
    all_to_all x4, blocking collectives, exchange(): return lax.all_to_all(parts, axes, split_axis=0, concat_axis=0, tiled=True)  110 us
    pallas_call x10, Pallas kernels, call(): pl.pallas_call(kernel, out_shape=shapes if len(shapes) > 1 else shapes[0]...  21 us
    ppermute x4, starting transfers between devices, swap_cores(): return lax.ppermute(data, 'c', [(0, 1), (1, 0)])  18 us
    all_to_all x2, waiting for transfers between devices, exchange(): return lax.all_to_all(parts, axes, split_axis=0, concat_axis=0, tiled=True)  16.3 us
    all_to_all x2, starting transfers between devices, exchange(): return lax.all_to_all(parts, axes, split_axis=0, concat_axis=0, tiled=True)  8.17 us
    ppermute x1, starting transfers between devices, body(): weights.append(lax.ppermute(weights[0], TP, back))  4.47 us
    ppermute x1, starting transfers between devices, body(): weights.append(lax.ppermute(weights[-1], TP, ring))  4.02 us
  transfers between devices with their start and end apart: 9, of which 3 were waited for; matrix products, arithmetic and copies ran while one was open for 0% of the time, Pallas kernels for 9%

profile of v8, /device:TPU:1, one launch (start us, length us, event | category | flops | bytes accessed | tf_op | source)
XLA Modules:
  0.0 194.2 jit_solution(1112834124591358241)
XLA Ops:
  0.0 2.4 %pack.1.w0 = bf16[6144,128]{1,0:T(8,128)(2,1)} custom-call(bf16[1,2048,128]{2,1,0:T(8,128)(2,1)} %switch_ref.1, bf16[1,2048,128]{2,1,0:T(8,128)(2,1)} %expansion_ref.1, bf16[1,128,2048]{2,1,0:T(8,128)(2,1)} %contraction_ref.1), custom_call_target="tpu_custom_call" | custom-call | tf_op jit(solution)/shard_map/pack/pallas_call | solution.py:512
  2.4 4.0 %collective-permute-start = (bf16[6144,128]{1,0:T(8,128)(2,1)}, bf16[6144,128]{1,0:T(8,128)(2,1)}, u32[]{:S(2)}, u32[]{:S(2)}) collective-permute-start(bf16[6144,128]{1,0:T(8,128)(2,1)} %pack.1.w0), channel_id=1, source_target_pairs={{2,0},{4,2},{6,4},{8,6},{10,8},{12,10},{14,12},{0,14},{15,1},{1,3}... | collective-permute-start | bytes 4718600 | tf_op jit(solution)/shard_map/ppermute | solution.py:526
  6.4 6.2 %shard_map.154 = (bf16[4,128,128]{2,1,0:T(8,128)(2,1)}, f32[256,128]{1,0:T(8,128)}, f32[256,128]{1,0:T(8,128)}) custom-call(bf16[256,128]{1,0:T(8,128)(2,1)} %refs_0_.1, bf16[256,128]{1,0:T(8,128)(2,1)} %refs_1_.1, bf16[256,128]{1,0:T(8,128)(2,1)} %refs_2_.1, bf16[256,128]{1,0:T(8,128)(2,1)} %refs_3_.1, f32[256,128]{1,0:T(8,128)} %refs_4_.1, f32[2,256]{1,0:T(2,128)} %bitcast.26), custom_call_target="tpu_custom_call" | custom-call | flops 2000000000 | bytes 1000000 | tf_op jit(solution)/shard_map/pallas_call | solution.py:463
  12.6 4.0 %all-to-all-start = ((bf16[4,128,128]{2,1,0:T(8,128)(2,1)}), bf16[4,128,128]{2,1,0:T(8,128)(2,1)S(1)}, u32[]{:S(2)}, u32[]{:S(2)}) async-start(bf16[4,128,128]{2,1,0:T(8,128)(2,1)} %get-tuple-element.33), calls=%async_computation | async-start | bytes 262144 | tf_op jit(solution)/shard_map/all_to_all | solution.py:479
  16.7 4.7 %all-to-all-done.got_ref = bf16[4,128,128]{2,1,0:T(8,128)(2,1)S(1)} async-done(((bf16[4,128,128]{2,1,0:T(8,128)(2,1)}), bf16[4,128,128]{2,1,0:T(8,128)(2,1)S(1)}, u32[]{:S(2)}, u32[]{:S(2)}) %all-to-all-start) | async-done | bytes 131104 | tf_op jit(solution)/shard_map/all_to_all | solution.py:479
  21.5 1.0 shard_map.155
  22.5 19.3 %all_to_all.30.got_ref = bf16[8,128,128]{2,1,0:T(8,128)(2,1)S(1)} all-to-all(bf16[8,128,128]{2,1,0:T(8,128)(2,1)S(1)} %get-tuple-element.34), channel_id=1, replica_groups=mesh['z'=8,'x'=4,'y'=8,'c'=2] {'z'}, dimensions={0} | all-to-all | bytes 524288 | tf_op jit(solution)/shard_map/all_to_all | solution.py:479
  41.8 2.6 %shard_map.156 = (bf16[8,256,128]{2,1,0:T(8,128)(2,1)S(1)}, bf16[256,128]{1,0:T(8,128)(2,1)S(1)}, bf16[1024,256]{1,0:T(8,128)(2,1)S(1)}, f32[2,256]{1,0:T(2,128)S(1)}) custom-call(s32[4]{0:T(128)S(1)} %pad_add_fusion.pos_ref, bf16[8,128,128]{2,1,0:T(8,128)(2,1)S(1)} %all_to_all.30.got_ref, f32[256,128]{1,0:T(8,128)S(1)} %get-tuple-element.36.prefix_ref, ...), custom_call_target="tpu_custom_call" | custom-call | flops 2000000000 | bytes 1000000 | tf_op jit(solution)/shard_map/pallas_call | solution.py:463
  44.5 7.5 %collective-permute-start.1 = (bf16[8,256,128]{2,1,0:T(8,128)(2,1)S(1)}, bf16[8,256,128]{2,1,0:T(8,128)(2,1)S(1)}, u32[]{:S(2)}, u32[]{:S(2)}) collective-permute-start(bf16[8,256,128]{2,1,0:T(8,128)(2,1)S(1)} %get-tuple-element.39), channel_id=1, source_target_pairs={{0,1},{1,0},{2,3},{3,2},{4,5},{5,4},{6,7},{7,6},{8,9},{9,8},{10,11... | collective-permute-start | bytes 1572872 | tf_op jit(solution)/shard_map/ppermute | solution.py:483
  52.0 1.4 hold.1.w1
  53.4 0.9 shard_map.157
  54.3 0.9 add_convert_fusion.1
  55.2 4.1 %all-to-all-start.2 = ((bf16[8,256,128]{2,1,0:T(8,128)(2,1)}), bf16[8,256,128]{2,1,0:T(8,128)(2,1)}, u32[]{:S(2)}, u32[]{:S(2)}) async-start(bf16[8,256,128]{2,1,0:T(8,128)(2,1)} %add_convert_fusion.1), calls=%async_computation.2 | async-start | bytes 1048576 | tf_op jit(solution)/shard_map/all_to_all | solution.py:479
  59.4 4.5 %collective-permute-start.3 = (bf16[6144,128]{1,0:T(8,128)(2,1)S(1)}, bf16[6144,128]{1,0:T(8,128)(2,1)}, u32[]{:S(2)}, u32[]{:S(2)}) collective-permute-start(bf16[6144,128]{1,0:T(8,128)(2,1)S(1)} %copy-done), channel_id=1, source_target_pairs={{0,2},{2,4},{4,6},{6,8},{8,10},{10,12},{12,14},{14,0},{1,15},{3,1}... | collective-permute-start | bytes 4718600 | tf_op jit(solution)/shard_map/ppermute | solution.py:546
  63.9 1.9 collective-permute-start.4
  65.8 11.6 %all-to-all-done.2.parts_ref = bf16[8,256,128]{2,1,0:T(8,128)(2,1)} async-done(((bf16[8,256,128]{2,1,0:T(8,128)(2,1)}), bf16[8,256,128]{2,1,0:T(8,128)(2,1)}, u32[]{:S(2)}, u32[]{:S(2)}) %all-to-all-start.2) | async-done | bytes 524320 | tf_op jit(solution)/shard_map/all_to_all | solution.py:479
  77.4 1.2 copy-done.2
  78.7 1.0 copy-done.9
  79.7 1.4 shard_map.158
  81.1 40.7 %all_to_all.31 = bf16[256,8,128]{2,1,0:T(8,128)(2,1)S(1)} all-to-all(bf16[256,8,128]{2,1,0:T(8,128)(2,1)S(1)} %bitcast.17), channel_id=1, replica_groups=mesh['z'=8,'x'=4,'y'=8,'c'=2] {'z','y','x'}, dimensions={0} | all-to-all | bytes 1048576 | tf_op jit(solution)/shard_map/all_to_all | solution.py:479
  121.8 2.6 %collective-permute-start.2 = (bf16[8,8,4,8,128]{4,3,2,1,0:T(8,128)(2,1)S(1)}, bf16[8,8,4,8,128]{4,3,2,1,0:T(8,128)(2,1)S(1)}, u32[]{:S(2)}, u32[]{:S(2)}) collective-permute-start(bf16[8,8,4,8,128]{4,3,2,1,0:T(8,128)(2,1)S(1)} %bitcast.14), channel_id=1, source_target_pairs={{0,1},{1,0},{2,3},{3,2},{4,5},{5,4},{6,7},{7,6},{8,9},{9,8},{10,11... | collective-permute-start | bytes 1572872 | tf_op jit(solution)/shard_map/ppermute | solution.py:483
  124.4 2.6 %shard_map.159 = (f32[4,256,256]{2,1,0:T(8,128)S(1)}, f32[256,128]{1,0:T(8,128)S(1)}) custom-call(s32[4]{0:T(128)S(1)} %pad_add_fusion.pos_ref, bf16[8,8,4,8,128]{4,3,2,1,0:T(8,128)(2,1)S(1)} %bitcast.15, f32[1,2048]{1,0:T(1,128)S(1)} %bitcast.19, bf16[6144,128]{1,0:T(8,128)(2,1)S(1)} %copy-done, bf16[6144,128]{1,0:T(8,128)(2,1)S(1)} %hold.1.w1, ...), custom_call_target="tpu_custom_call" | custom-call | flops 2000000000 | bytes 1000000 | tf_op jit(solution)/shard_map/pallas_call | solution.py:463
  127.1 3.0 %shard_map.160 = (bf16[8,8,4,8,128]{4,3,2,1,0:T(8,128)(2,1)S(1)}, bf16[256,512]{1,0:T(8,128)(2,1)S(1)}) custom-call(s32[4]{0:T(128)S(1)} %pad_add_fusion.pos_ref, bf16[8,8,4,8,128]{4,3,2,1,0:T(8,128)(2,1)S(1)} %collective-permute-done.2.other_ref, f32[1,2048]{1,0:T(1,128)S(1)} %bitcast.20, f32[4,256,256]{2,1,0:T(8,128)S(1)} %get-tuple-element.49.act_ref, ...), custom_call_target="tpu_custom_call" | custom-call | flops 2000000000 | bytes 1000000 | tf_op jit(solution)/shard_map/pallas_call | solution.py:463
  130.1 2.1 %collective-permute-start.5 = (bf16[8,8,4,8,128]{4,3,2,1,0:T(8,128)(2,1)S(1)}, bf16[8,8,4,8,128]{4,3,2,1,0:T(8,128)(2,1)S(1)}, u32[]{:S(2)}, u32[]{:S(2)}) collective-permute-start(bf16[8,8,4,8,128]{4,3,2,1,0:T(8,128)(2,1)S(1)} %get-tuple-element.51), channel_id=1, source_target_pairs={{0,1},{1,0},{2,3},{3,2},{4,5},{5,4},{6,7},{7,6},{8,9},{9,8},{10,11... | collective-permute-start | bytes 1572872 | tf_op jit(solution)/shard_map/ppermute | solution.py:483
  132.2 0.6 shard_map.162
  132.7 2.3 %shard_map.161 = bf16[8,8,4,8,128]{4,3,2,1,0:T(8,128)(2,1)S(1)} custom-call(s32[4]{0:T(128)S(1)} %pad_add_fusion.pos_ref, bf16[256,512]{1,0:T(8,128)(2,1)S(1)} %get-tuple-element.52.hidden_ref, bf16[6144,128]{1,0:T(8,128)(2,1)S(1)} %copy-done, bf16[6144,128]{1,0:T(8,128)(2,1)S(1)} %hold.1.w1, bf16[6144,128]{1,0:T(8,128)(2,1)} %collective-permute-done.3.w2, ...), custom_call_target="tpu_custom_call" | custom-call | flops 2000000000 | bytes 1000000 | tf_op jit(solution)/shard_map/pallas_call | solution.py:463
  135.3 31.4 %all_to_all.32 = bf16[256,8,128]{2,1,0:T(8,128)(2,1)S(1)} all-to-all(bf16[256,8,128]{2,1,0:T(8,128)(2,1)S(1)} %bitcast.25), channel_id=1, replica_groups=mesh['z'=8,'x'=4,'y'=8,'c'=2] {'z','y','x'}, dimensions={0} | all-to-all | bytes 1048576 | tf_op jit(solution)/shard_map/all_to_all | solution.py:479
  166.6 0.4 shard_map.163
  167.1 18.2 %all_to_all.33.own_ref = bf16[8,256,128]{2,1,0:T(8,128)(2,1)S(1)} all-to-all(bf16[8,256,128]{2,1,0:T(8,128)(2,1)S(1)} %shard_map.163), channel_id=1, replica_groups=mesh['z'=8,'x'=4,'y'=8,'c'=2] {'y'}, dimensions={0} | all-to-all | bytes 1048576 | tf_op jit(solution)/shard_map/all_to_all | solution.py:479
  185.2 5.8 %collective-permute-start.6 = (bf16[8,256,128]{2,1,0:T(8,128)(2,1)S(1)}, bf16[8,256,128]{2,1,0:T(8,128)(2,1)S(1)}, u32[]{:S(2)}, u32[]{:S(2)}) collective-permute-start(bf16[8,256,128]{2,1,0:T(8,128)(2,1)S(1)} %all_to_all.33.own_ref), channel_id=1, source_target_pairs={{0,1},{1,0},{2,3},{3,2},{4,5},{5,4},{6,7},{7,6},{8,9},{9,8},{10,11... | collective-permute-start | bytes 1572872 | tf_op jit(solution)/shard_map/ppermute | solution.py:483
  191.1 1.4 shard_map.164.half_ref
  192.6 1.4 shard_map.165
  (31 shorter events, 0.4 us)
Async XLA Ops:
  2.4 39.4 %collective-permute-start = (bf16[6144,128]{1,0:T(8,128)(2,1)}, bf16[6144,128]{1,0:T(8,128)(2,1)}, u32[]{:S(2)}, u32[]{:S(2)}) collective-permute-start(bf16[6144,128]{1,0:T(8,128)(2,1)} %pack.1.w0), channel_id=1, source_target_pairs={{2,0},{4,2},{6,4},{8,6},{10,8},{12,10},{14,12},{0,14},{15,1},{1,3}... | collective-permute-start | bytes 4718600 | tf_op jit(solution)/shard_map/ppermute | solution.py:526
  12.6 8.9 %all-to-all-start = ((bf16[4,128,128]{2,1,0:T(8,128)(2,1)}), bf16[4,128,128]{2,1,0:T(8,128)(2,1)S(1)}, u32[]{:S(2)}, u32[]{:S(2)}) async-start(bf16[4,128,128]{2,1,0:T(8,128)(2,1)} %get-tuple-element.33), calls=%async_computation | async-start | bytes 262144 | tf_op jit(solution)/shard_map/all_to_all | solution.py:479
  16.7 25.1 %copy-start.3 = (bf16[128,2048]{1,0:T(8,128)(2,1)S(1)}, bf16[128,2048]{1,0:T(8,128)(2,1)}, u32[]{:S(2)}) copy-start(bf16[128,2048]{1,0:T(8,128)(2,1)} %w_ref.3) | copy-start | bytes 1572868
  16.7 25.1 %copy-start.4 = (s32[256,2]{0,1:T(2,128)S(1)}, s32[256,2]{0,1:T(2,128)}, u32[]{:S(2)}) copy-start(s32[256,2]{0,1:T(2,128)} %param.28) | copy-start | bytes 6148
  16.7 25.1 %copy-start.7 = (f32[128]{0:T(128)S(1)}, f32[128]{0:T(128)}, u32[]{:S(2)}) copy-start(f32[128]{0:T(128)} %param.22) | copy-start | bytes 1540
  16.7 25.1 %copy-start.10 = (f32[256,128]{1,0:T(8,128)S(1)}, f32[256,128]{1,0:T(8,128)}, u32[]{:S(2)}) copy-start(f32[256,128]{1,0:T(8,128)} %get-tuple-element.37.map_ref) | copy-start | bytes 393220
  16.7 25.1 %copy-start.11 = (f32[256,128]{1,0:T(8,128)S(1)}, f32[256,128]{1,0:T(8,128)}, u32[]{:S(2)}) copy-start(f32[256,128]{1,0:T(8,128)} %get-tuple-element.38.loc_ref) | copy-start | bytes 393220
  44.5 9.0 %copy-start.8 = (bf16[1024,256]{1,0:T(8,128)(2,1)}, bf16[1024,256]{1,0:T(8,128)(2,1)S(1)}, u32[]{:S(2)}) copy-start(bf16[1024,256]{1,0:T(8,128)(2,1)S(1)} %get-tuple-element.44.hot_ref) | copy-start | bytes 1572868
  44.5 9.8 %collective-permute-start.1 = (bf16[8,256,128]{2,1,0:T(8,128)(2,1)S(1)}, bf16[8,256,128]{2,1,0:T(8,128)(2,1)S(1)}, u32[]{:S(2)}, u32[]{:S(2)}) collective-permute-start(bf16[8,256,128]{2,1,0:T(8,128)(2,1)S(1)} %get-tuple-element.39), channel_id=1, source_target_pairs={{0,1},{1,0},{2,3},{3,2},{4,5},{5,4},{6,7},{7,6},{8,9},{9,8},{10,11... | collective-permute-start | bytes 1572872 | tf_op jit(solution)/shard_map/ppermute | solution.py:483
  54.3 5.1 %copy-start = (bf16[6144,128]{1,0:T(8,128)(2,1)S(1)}, bf16[6144,128]{1,0:T(8,128)(2,1)}, u32[]{:S(2)}) copy-start(bf16[6144,128]{1,0:T(8,128)(2,1)} %pack.1.w0) | copy-start | bytes 4718596
  54.3 23.1 %copy-start.1 = (f32[2048]{0:T(1024)S(1)}, f32[2048]{0:T(1024)}, u32[]{:S(2)}) copy-start(f32[2048]{0:T(1024)} %param.25) | copy-start | bytes 24580
  55.2 22.2 %all-to-all-start.2 = ((bf16[8,256,128]{2,1,0:T(8,128)(2,1)}), bf16[8,256,128]{2,1,0:T(8,128)(2,1)}, u32[]{:S(2)}, u32[]{:S(2)}) async-start(bf16[8,256,128]{2,1,0:T(8,128)(2,1)} %add_convert_fusion.1), calls=%async_computation.2 | async-start | bytes 1048576 | tf_op jit(solution)/shard_map/all_to_all | solution.py:479
  59.4 65.0 %collective-permute-start.3 = (bf16[6144,128]{1,0:T(8,128)(2,1)S(1)}, bf16[6144,128]{1,0:T(8,128)(2,1)}, u32[]{:S(2)}, u32[]{:S(2)}) collective-permute-start(bf16[6144,128]{1,0:T(8,128)(2,1)S(1)} %copy-done), channel_id=1, source_target_pairs={{0,2},{2,4},{4,6},{6,8},{8,10},{10,12},{12,14},{14,0},{1,15},{3,1}... | collective-permute-start | bytes 4718600 | tf_op jit(solution)/shard_map/ppermute | solution.py:546
  63.9 60.5 %collective-permute-start.4 = (bf16[6144,128]{1,0:T(8,128)(2,1)}, bf16[6144,128]{1,0:T(8,128)(2,1)}, u32[]{:S(2)}, u32[]{:S(2)}) collective-permute-start(bf16[6144,128]{1,0:T(8,128)(2,1)} %collective-permute-done.far_ref), channel_id=1, source_target_pairs={{2,0},{4,2},{6,4},{8,6},{10,8},{12,10},{14,12},{0,14},{15,1},{1,3}... | collective-permute-start | bytes 4718600 | tf_op jit(solution)/shard_map/ppermute | solution.py:552
  77.4 1.2 copy-start.2
  78.7 1.0 copy-start.9
  121.8 5.2 %collective-permute-start.2 = (bf16[8,8,4,8,128]{4,3,2,1,0:T(8,128)(2,1)S(1)}, bf16[8,8,4,8,128]{4,3,2,1,0:T(8,128)(2,1)S(1)}, u32[]{:S(2)}, u32[]{:S(2)}) collective-permute-start(bf16[8,8,4,8,128]{4,3,2,1,0:T(8,128)(2,1)S(1)} %bitcast.14), channel_id=1, source_target_pairs={{0,1},{1,0},{2,3},{3,2},{4,5},{5,4},{6,7},{7,6},{8,9},{9,8},{10,11... | collective-permute-start | bytes 1572872 | tf_op jit(solution)/shard_map/ppermute | solution.py:483
  127.1 5.1 %copy-start.5 = (f32[256,2]{0,1:T(2,128)S(1)}, f32[256,2]{0,1:T(2,128)}, u32[]{:S(2)}) copy-start(f32[256,2]{0,1:T(2,128)} %param.27) | copy-start | bytes 6148
  127.1 5.1 %copy-start.6 = (f32[256]{0:T(256)S(1)}, f32[256]{0:T(256)}, u32[]{:S(2)}) copy-start(f32[256]{0:T(256)} %param.26) | copy-start | bytes 3076
  130.1 5.1 %collective-permute-start.5 = (bf16[8,8,4,8,128]{4,3,2,1,0:T(8,128)(2,1)S(1)}, bf16[8,8,4,8,128]{4,3,2,1,0:T(8,128)(2,1)S(1)}, u32[]{:S(2)}, u32[]{:S(2)}) collective-permute-start(bf16[8,8,4,8,128]{4,3,2,1,0:T(8,128)(2,1)S(1)} %get-tuple-element.51), channel_id=1, source_target_pairs={{0,1},{1,0},{2,3},{3,2},{4,5},{5,4},{6,7},{7,6},{8,9},{9,8},{10,11... | collective-permute-start | bytes 1572872 | tf_op jit(solution)/shard_map/ppermute | solution.py:483
  185.2 7.4 %collective-permute-start.6 = (bf16[8,256,128]{2,1,0:T(8,128)(2,1)S(1)}, bf16[8,256,128]{2,1,0:T(8,128)(2,1)S(1)}, u32[]{:S(2)}, u32[]{:S(2)}) collective-permute-start(bf16[8,256,128]{2,1,0:T(8,128)(2,1)S(1)} %all_to_all.33.own_ref), channel_id=1, source_target_pairs={{0,1},{1,0},{2,3},{3,2},{4,5},{5,4},{6,7},{7,6},{8,9},{9,8},{10,11... | collective-permute-start | bytes 1572872 | tf_op jit(solution)/shard_map/ppermute | solution.py:483
